TPU v7x, 512 devices: a whole 4x4x16 slice. The times are simulated.
512 devices in a mesh: sp: 16 (over z), fs: 4 (over y), tp: 8 (over x, core).
Axes of the slice: x: 4, y: 4, z: 16, core: 2. Of those that a mesh axis runs over, the one named last changes fastest.
Arguments:
- input_layer_rows: bfloat16 [4, 4096, 2048], P('fs', 'sp'), may hold values from -6 to 6
- input_norm_gain: float32 [2048], replicated, may hold values from 0.1 to 1.9
- query_weight_attention: bfloat16 [2048, 1024], P(('sp', 'fs'), 'tp'), may hold values from -0.125 to 0.125
- key_weight_attention: bfloat16 [2048, 1024], P(('sp', 'fs'), 'tp'), may hold values from -0.125 to 0.125
- value_weight_attention: bfloat16 [2048, 1024], P(('sp', 'fs'), 'tp'), may hold values from -0.125 to 0.125
- query_weight_recurrent: bfloat16 [2048, 1024], P(('sp', 'fs'), 'tp'), may hold values from -0.125 to 0.125
- forget_weight_recurrent: bfloat16 [2048, 1024], P(('sp', 'fs'), 'tp'), may hold values from -0.125 to 0.125
- value_weight_recurrent: bfloat16 [2048, 1024], P(('sp', 'fs'), 'tp'), may hold values from -0.125 to 0.125
- gate_weight_recurrent: bfloat16 [2048, 1024], P(('sp', 'fs'), 'tp'), may hold values from -0.125 to 0.125
- output_weight_attention: bfloat16 [2048, 1024], P(('sp', 'fs'), 'tp'), may hold values from -0.125 to 0.125
- emitted_projection_linear_scan: bfloat16 [2048, 1024], P(('sp', 'fs'), 'tp'), may hold values from -0.125 to 0.125
- score_offset: float32 [8], P('tp'), as said below
- attention_norm_gain: float32 [1024], P('tp'), may hold values from 0.1 to 1.9
- recurrence_norm_gain: float32 [1024], P('tp'), may hold values from 0.1 to 1.9
- forget_floor: float32 [1024], P('tp'), may hold values from 0.1 to 0.5
- forget_offset: float32 [1024], P('tp'), as said below
- extra_log_decay: float32 [4, 4096, 1024], P('fs', 'sp', 'tp')
Outputs:
- layer_out: bfloat16 [4, 4096, 2048], P('fs', ('sp', 'tp'))
- row_log_total: float32 [4, 8, 4096], P('fs', 'tp', 'sp')
Inputs may be any that keep to these rules, and one draw needn't show every extreme that they name: `score_offset`: each head's offset lies between -ln(4096) - 2 and -ln(4096) + 0.5. `forget_offset`: each channel's offset lies between ln(256) - 3 and ln(4096) + 0.6.
All inputs are finite; a program needn't handle non-finite values.
Results may differ from a plain program's by a relative error of at most 0.015.
Values may be sent and summed in bfloat16 or wider, within the bound.
No kernel may reach another device: no remote copies, remote signals or barrier semaphores. Data moves between devices by JAX's collectives and lax.ppermute only.
A program may use at most 64 MiB of HBM per device.

v0:
```python
import jax
import jax.numpy as jnp
from jax import lax
from jax.experimental import pallas as pl
from jax.experimental.pallas import tpu as pltpu
from jax.sharding import PartitionSpec as P


HEAD = 128
ROWS = 32
TILE = 16
NEAR = 4

epsilon = 1e-06
log_floor = 0.05
F32 = jnp.float32
BF16 = jnp.bfloat16
INTERPRET = False


def vmem_call(kernel, outs, n_in, smem=(), hbm=(), scratch=(), mib=16):
    def space(k):
        return pltpu.SMEM if k in smem else pltpu.HBM if k in hbm else pltpu.VMEM

    return pl.pallas_call(
        kernel,
        out_shape=outs,
        in_specs=[pl.BlockSpec(memory_space=space(k)) for k in range(n_in)],
        out_specs=jax.tree.map(lambda _: pl.BlockSpec(memory_space=pltpu.VMEM), outs),
        scratch_shapes=list(scratch),
        compiler_params=pltpu.CompilerParams(vmem_limit_bytes=mib << 20),
        interpret=INTERPRET,
    )


def dot(a, b, dims=((1,), (0,))):
    return lax.dot_general(a, b, (dims, ((), ())), preferred_element_type=F32)


def parts(a):
    high = a.astype(BF16)
    return high, (a - high.astype(F32)).astype(BF16)


def dot_left(a, b, dims=((1,), (0,))):
    high, low = parts(a)
    return dot(high, b, dims) + dot(low, b, dims)


def dot_both(a, b, dims):
    a_high, a_low = parts(a)
    b_high, b_low = parts(b)
    return dot(a_high, b_high, dims) + (dot(a_high, b_low, dims) + dot(a_low, b_high, dims))


def start_kernel(x_hbm, gain_hbm, *refs):
    weights = refs[:9]
    slices_ref, packed_ref, own_ref, x_ref, gain_ref, arrived = refs[9:]
    copies = [
        pltpu.make_async_copy(x_hbm, x_ref, arrived.at[0]),
        pltpu.make_async_copy(gain_hbm, gain_ref, arrived.at[1]),
    ]
    for k in range(7):
        place = packed_ref.at[:, k * HEAD : (k + 1) * HEAD]
        copies.append(pltpu.make_async_copy(weights[k], place, arrived.at[2 + k]))
    for k in range(2):
        place = own_ref.at[k * ROWS : (k + 1) * ROWS]
        copies.append(pltpu.make_async_copy(weights[7 + k], place, arrived.at[9 + k]))
    for copy in copies:
        copy.start()
    for copy in copies:
        copy.wait()
    values = x_ref[...].astype(F32)
    square_mean = jnp.mean(values * values, axis=-1, keepdims=True)
    normed = (values * lax.rsqrt(square_mean + epsilon) * gain_ref[...]).astype(BF16)
    count = slices_ref.shape[0]
    wide = count * HEAD
    target = lax.broadcasted_iota(jnp.int32, (wide, wide), 1)
    source = lax.broadcasted_iota(jnp.int32, (wide, wide), 0)
    inside = target % HEAD
    wanted = (inside // ROWS) * (count * ROWS) + (target // HEAD) * ROWS + inside % ROWS
    pick = (source == wanted).astype(BF16)
    for b in range(x_ref.shape[1] // wide):
        moved = dot(normed[:, b * wide : (b + 1) * wide], pick).astype(BF16)
        for k in range(count):
            slices_ref[k, :, b * HEAD : (b + 1) * HEAD] = moved[:, k * HEAD : (k + 1) * HEAD]


def partial_kernel(rows_ref, weight_ref, out_ref):
    weight = weight_ref[...]
    for k in range(rows_ref.shape[0]):
        out_ref[k] = dot(rows_ref[k], weight).astype(BF16)


def local_recurrence_kernel(*refs):
    group_ref, products_ref, floor_ref, offset_ref, extra_hbm = refs[:5]
    own = refs[5:-7]
    message_ref, query_ref, inner_ref, query_decayed_ref, gate_ref, extra_ref, arrived = refs[-7:]
    copy = pltpu.make_async_copy(extra_hbm, extra_ref, arrived)
    copy.start()
    total = products_ref[0].astype(F32)
    for k in range(1, products_ref.shape[0]):
        total = total + products_ref[k].astype(F32)
    total = total.astype(BF16)
    columns = [total[:, k * HEAD : (k + 1) * HEAD] for k in range(7)]
    query_ref[...] = columns[2]
    query_b = columns[3].astype(F32)
    query = query_b / (1.0 + jnp.exp(-query_b))
    value = columns[5]
    gate_b = columns[6].astype(F32)
    gate_ref[...] = gate_b / (1.0 + jnp.exp(-gate_b))
    u = columns[4].astype(F32) + offset_ref[...]
    key = (1.0 - floor_ref[...]) / (1.0 + jnp.exp(u))
    copy.wait()
    log_forget = jnp.log(1.0 - key) + extra_ref[...]
    length = log_forget.shape[0]
    row = lax.broadcasted_iota(jnp.int32, (length, length), 0)
    col = lax.broadcasted_iota(jnp.int32, (length, length), 1)
    lower = (row >= col).astype(BF16)
    high = log_forget.astype(BF16)
    rest = log_forget - high.astype(F32)
    middle = rest.astype(BF16)
    low = (rest - middle.astype(F32)).astype(BF16)
    running = dot(lower, high) + (dot(lower, middle) + dot(lower, low))
    position = lax.broadcasted_iota(jnp.int32, (length, 1), 0)
    pairwise = jnp.where(row == col, dot_both(query, key, ((1,), (1,))), 0.0)
    half = 1
    while half < length:
        block = 2 * half
        if block >= 8:
            boundary = running.reshape(length // block, block, HEAD)[:, half - 1 : half]
            boundary = jnp.broadcast_to(boundary, (length // block, block, HEAD)).reshape(
                length, HEAD
            )
        else:
            tiles = running.reshape(length // 8, 8, HEAD)
            inside = lax.broadcasted_iota(jnp.int32, (1, 8, 1), 1) // block
            boundary = jnp.zeros_like(tiles)
            for k in range(8 // block):
                at = k * block + half - 1
                boundary = jnp.where(inside == k, tiles[:, at : at + 1], boundary)
            boundary = boundary.reshape(length, HEAD)
        second = (position // half) % 2 == 1
        after = jnp.where(second, query * jnp.exp(running - boundary), 0.0)
        before = jnp.where(second, 0.0, key * jnp.exp(boundary - running))
        chosen = (row // block == col // block) & (row // half != col // half) & (row > col)
        pairwise = jnp.where(chosen, dot_both(after, before, ((1,), (1,))), pairwise)
        half = block
    inner_ref[...] = dot_left(pairwise, value)
    final = running[length - 1 : length]
    query_decayed_ref[...] = query * jnp.exp(running)
    key_high, key_low = parts(key * jnp.exp(final - running))
    state = dot(value, key_high, ((0,), (0,))) + dot(value, key_low, ((0,), (0,)))
    at = 0
    vector = jnp.broadcast_to(jnp.exp(final), (TILE, HEAD)).astype(BF16)
    for piece in (columns[0], columns[1], state.astype(BF16), vector):
        message_ref[at : at + piece.shape[0]] = piece
        at += piece.shape[0]
    groups = len(own)
    for k in range(groups):
        slot = (group_ref[0] + groups - k) % groups
        start = pl.multiple_of(at + slot * 2 * ROWS, TILE)
        message_ref[pl.ds(start, 2 * ROWS)] = own[k][...]


def chain(message_ref, start, count):
    def step(k, carry):
        decay_all, state = carry
        decay = message_ref[k, start + HEAD : start + HEAD + TILE].astype(F32)[0:1]
        return decay * decay_all, decay * state + message_ref[k, start : start + HEAD].astype(F32)

    return lax.fori_loop(
        0, count, step, (jnp.ones((1, HEAD), F32), jnp.zeros((HEAD, HEAD), F32))
    )


def attend(query, message_ref, shift, k, ahead=None):
    length = query.shape[0]
    row = lax.broadcasted_iota(jnp.int32, (length, length), 0)
    col = lax.broadcasted_iota(jnp.int32, (length, length), 1)
    key = message_ref[k, 0:length]
    value = message_ref[k, length : 2 * length]
    scores = dot(query, key, ((1,), (1,))) * HEAD ** (-0.5) + shift
    softplus = jnp.maximum(scores, 0.0) + jnp.log(1.0 + jnp.exp(-jnp.abs(scores)))
    if ahead is not None:
        seen = row + ahead * length > col
        softplus = jnp.where(seen, softplus, 0.0)
    spent = dot_left(softplus, (row >= col).astype(BF16))
    weights = jnp.exp(scores - spent)
    if ahead is not None:
        weights = jnp.where(seen, weights, 0.0)
    return dot(weights.astype(BF16), value), spent[:, 0:1]


def attend_near(query, message_ref, shift, place=None):
    weighted, total = None, None
    for k in reversed(range(message_ref.shape[0])):
        ahead = None if place is None else place - k
        more, spent = attend(query, message_ref, shift, k, ahead)
        weighted = more if weighted is None else weighted + jnp.exp(-total) * more
        total = spent if total is None else total + spent
    return weighted, total


def as_row(total):
    return jnp.transpose(jnp.broadcast_to(total, (total.shape[0], HEAD)))[0:1]


def as_column(row):
    pieces = [
        jnp.transpose(jnp.broadcast_to(row[:, k : k + HEAD], (HEAD, HEAD)))[:, 0:1]
        for k in range(0, row.shape[1], HEAD)
    ]
    return jnp.concatenate(pieces, axis=0)


def far_kernel(group_ref, shift_ref, message_ref, *refs):
    count = len(refs) // 2
    shift = shift_ref[0]
    near = message_ref.shape[0]
    length = refs[0].shape[0]
    for j in range(count):
        out_ref = refs[count + j]
        wanted = group_ref[0] + j < count

        @pl.when(wanted)
        def _(query_ref=refs[j], out_ref=out_ref):
            weighted, total = attend_near(query_ref[...], message_ref, shift)
            out_ref[0:length] = weighted.astype(BF16)
            decay, state = chain(message_ref, 2 * length, near)
            high, low = parts(as_row(total))
            pieces = [
                piece[:, k * HEAD : (k + 1) * HEAD] for piece in (high, low) for k in range(2)
            ]
            index = lax.broadcasted_iota(jnp.int32, (TILE, HEAD), 0)
            vector = jnp.zeros((TILE, HEAD), F32)
            for k, piece in enumerate(pieces + [decay]):
                vector = jnp.where(index == k, piece.astype(F32), vector)
            out_ref[length : length + TILE] = vector.astype(BF16)
            out_ref[length + TILE : length + TILE + HEAD] = state.astype(BF16)

        @pl.when(jnp.logical_not(wanted))
        def _(out_ref=out_ref):
            out_ref[...] = jnp.zeros(out_ref.shape, BF16)


def final_kernel(
    place_ref,
    shift_ref,
    query_ref,
    message_ref,
    inner_ref,
    query_decayed_ref,
    gate_ref,
    gain_a_ref,
    gain_b_ref,
    weight_ref,
    *refs,
):
    far_refs, out_ref, total_ref = refs[:-2], refs[-2], refs[-1]
    place = place_ref[0]
    shift = shift_ref[0]
    query = query_ref[...]
    length = query.shape[0]
    incoming = jnp.zeros((HEAD, HEAD), F32)
    outside = jnp.zeros((length, HEAD), F32)
    outside_row = jnp.zeros((1, length), F32)
    for ref in reversed(far_refs):
        vector = ref[length : length + TILE].astype(F32)
        row = jnp.concatenate(
            [vector[k : k + 1] + vector[k + 2 : k + 3] for k in range(2)], axis=1
        )
        incoming = vector[4:5] * incoming + ref[
            length + TILE : length + TILE + HEAD
        ].astype(F32)
        outside = ref[0:length].astype(F32) + jnp.exp(-as_column(row)) * outside
        outside_row = outside_row + row
    decay, state = chain(message_ref, 2 * length, place)
    state = state + decay * incoming
    recurrent = inner_ref[...] + dot_both(query_decayed_ref[...], state, ((1,), (1,)))
    square_mean = jnp.mean(recurrent * recurrent, axis=-1, keepdims=True)
    mixed_b = (
        recurrent * lax.rsqrt(square_mean + epsilon) * gain_b_ref[...] * gate_ref[...]
    ).astype(BF16)
    weighted, total = attend_near(query, message_ref, shift, place)
    weighted = weighted + jnp.exp(-total) * outside
    total_row = as_row(total) + outside_row
    total_ref[...] = jnp.log(jnp.maximum(1.0 - jnp.exp(-total_row), log_floor))
    square_mean = jnp.mean(weighted * weighted, axis=-1, keepdims=True)
    mixed_a = (weighted * lax.rsqrt(square_mean + epsilon) * gain_a_ref[...]).astype(BF16)
    mixed = jnp.concatenate([mixed_a, mixed_b], axis=1)
    fs, near, groups = weight_ref.shape[:3]
    width = fs * ROWS
    for group in range(groups):
        for s in range(near):
            both = jnp.concatenate(
                [weight_ref[:, s, group, k].reshape(width, HEAD) for k in range(2)], axis=1
            )
            at = (group * near + s) * width
            out_ref[:, at : at + width] = dot(mixed, both, ((1,), (1,))).astype(BF16)


def over_fs(shard):
    size = lax.axis_size("fs")
    copies = jnp.broadcast_to(shard[None], (size, *shard.shape))
    return lax.all_to_all(copies, "fs", 0, 0, tiled=True)


def turned(array, axis, places):
    size = lax.axis_size(axis)
    return lax.ppermute(array, axis, [(k, (k + places) % size) for k in range(size)])


def on_device(
    input_layer_rows,
    input_norm_gain,
    query_weight_attention,
    key_weight_attention,
    value_weight_attention,
    query_weight_recurrent,
    forget_weight_recurrent,
    value_weight_recurrent,
    gate_weight_recurrent,
    output_weight_attention,
    emitted_projection_linear_scan,
    score_offset,
    attention_norm_gain,
    recurrence_norm_gain,
    forget_floor,
    forget_offset,
    extra_log_decay,
):
    x = input_layer_rows[0]
    tokens, width = x.shape
    sp, fs, tp = (lax.axis_size(name) for name in ("sp", "fs", "tp"))
    count = sp // NEAR
    rank = lax.axis_index("sp").astype(jnp.int32)
    group = (rank // NEAR).reshape(1)
    shape = jax.ShapeDtypeStruct

    slices, packed, out_own = vmem_call(
        start_kernel,
        (
            shape((fs, tokens, width // fs), BF16),
            shape((ROWS, 7 * HEAD), BF16),
            shape((2 * ROWS, HEAD), BF16),
        ),
        11,
        hbm=range(11),
        scratch=(
            pltpu.VMEM((tokens, width), BF16),
            pltpu.VMEM((1, width), F32),
            pltpu.SemaphoreType.DMA((11,)),
        ),
        mib=58,
    )(
        x,
        input_norm_gain.reshape(1, width),
        key_weight_attention,
        value_weight_attention,
        query_weight_attention,
        query_weight_recurrent,
        forget_weight_recurrent,
        value_weight_recurrent,
        gate_weight_recurrent,
        output_weight_attention,
        emitted_projection_linear_scan,
    )
    rows = lax.all_to_all(slices, "fs", 0, 0, tiled=True)
    out_slots = [out_own] + [turned(out_own, "sp", NEAR * k) for k in range(1, count)]
    column = lax.all_gather(packed, "sp", axis=0, tiled=True)
    products = vmem_call(partial_kernel, shape((fs, tokens, 7 * HEAD), BF16), 2)(rows, column)
    products = lax.all_to_all(products, "fs", 0, 0, tiled=True)

    small = shape((tokens, HEAD), F32)
    start = 2 * tokens + HEAD + TILE
    message, query, inner, query_decayed, gate = vmem_call(
        local_recurrence_kernel,
        (
            shape((start + count * 2 * ROWS, HEAD), BF16),
            shape((tokens, HEAD), BF16),
            small,
            small,
            small,
        ),
        5 + count,
        (0,),
        (4,),
        (pltpu.VMEM((tokens, HEAD), F32), pltpu.SemaphoreType.DMA(())),
    )(
        group,
        products,
        forget_floor.reshape(1, HEAD),
        forget_offset.reshape(1, HEAD),
        extra_log_decay[0],
        *out_slots,
    )
    queries = []
    for j in range(1, count):
        places = [(k, k - NEAR * j) for k in range(NEAR * j, sp)]
        queries.append(lax.ppermute(query, "sp", places))
    groups = [list(range(NEAR * k, NEAR * (k + 1))) for k in range(count)]
    gathered = lax.all_gather(message, "sp", axis_index_groups=groups)
    far = vmem_call(
        far_kernel,
        tuple(shape((tokens + TILE + HEAD, HEAD), BF16) for _ in queries),
        2 + count,
        (0, 1),
    )(group, score_offset, gathered, *queries)
    far = [
        lax.ppermute(far[j - 1], "sp", [(k, k + NEAR * j) for k in range(sp - NEAR * j)])
        for j in range(1, count)
    ]
    out_weights = over_fs(gathered[:, start:].reshape(NEAR, count, 2, ROWS, HEAD))
    projected, row_log_total = vmem_call(
        final_kernel,
        (shape((tokens, width), BF16), shape((1, tokens), F32)),
        9 + count,
        (0, 1),
    )(
        (rank % NEAR).reshape(1),
        score_offset,
        query,
        gathered,
        inner,
        query_decayed,
        gate,
        attention_norm_gain.reshape(1, HEAD),
        recurrence_norm_gain.reshape(1, HEAD),
        out_weights,
        *far,
    )
    tiles = lax.all_to_all(projected.reshape(tp, tokens // tp, width), "tp", 0, 0, tiled=True)
    layer_out = jnp.sum(tiles.astype(F32), axis=0).astype(BF16)
    return (layer_out[None], row_log_total[None])


def solution(mesh):
    weight = P(("sp", "fs"), "tp")
    return jax.shard_map(
        on_device,
        mesh=mesh,
        in_specs=(
            P("fs", "sp", None),
            P(),
            *(weight for _ in range(9)),
            *(P("tp") for _ in range(5)),
            P("fs", "sp", "tp"),
        ),
        out_specs=(P("fs", ("sp", "tp"), None), P("fs", "tp", "sp")),
        check_vma=False,
    )
```

profile of v0, /device:TPU:1, one launch (start us, length us, event | category | flops | bytes accessed | tf_op | source)
XLA Modules:
  0.0 166.7 jit_solution(3588435708147551692)
XLA Ops:
  0.6 3.3 %shard_map.176 = (bf16[4,256,512]{2,1,0:T(8,128)(2,1)}, bf16[32,896]{1,0:T(8,128)(2,1)}, bf16[64,128]{1,0:T(8,128)(2,1)}) custom-call(bf16[256,2048]{1,0:T(8,128)(2,1)} %bitcast.24, f32[1,2048]{1,0:T(1,128)} %bitcast.26, bf16[32,128]{1,0:T(8,128)(2,1)} %refs_0_.1, bf16[32,128]{1,0:T(8,128)(2,1)} %refs_1_.1, bf16[32,128]{1,0:T(8,128)(2,1)} %refs_2_.1, ...), custom_call_target="tpu_custom_call" | custom-call | tf_op jit(solution)/shard_map/pallas_call | solution.py:341
  4.0 0.0 copy-start.7
  4.0 5.2 %all-to-all-start = ((bf16[4,256,512]{2,1,0:T(8,128)(2,1)}), bf16[4,256,512]{2,1,0:T(8,128)(2,1)S(1)}, u32[]{:S(2)}, u32[]{:S(2)}) async-start(bf16[4,256,512]{2,1,0:T(8,128)(2,1)} %get-tuple-element.15), calls=%async_computation | async-start | bytes 2097152 | tf_op jit(solution)/shard_map/all_to_all | solution.py:369
  9.1 0.0 copy-done.7
  9.1 34.0 %all_gather.9.weight_ref = bf16[512,896]{1,0:T(8,128)(2,1)S(1)} all-gather(bf16[32,896]{1,0:T(8,128)(2,1)S(1)} %copy-done.7), channel_id=1, replica_groups=mesh['sp'=16,'fs'=4,'tp'=8] {'sp'}, dimensions={0}, use_global_device_ids=true | all-gather | bytes 974848 | tf_op jit(solution)/shard_map/all_gather | solution.py:371
  43.1 0.0 all-to-all-done.rows_ref
  43.1 1.3 shard_map.177
  44.4 0.0 copy-start
  44.4 1.3 copy-done
  45.6 0.0 copy-start.2
  45.6 0.0 copy-start.1
  45.6 0.0 copy-start.5
  45.7 0.0 copy-start.6
  45.7 4.8 %all-to-all-start.1 = ((bf16[4,256,896]{2,1,0:T(8,128)(2,1)}), bf16[4,256,896]{2,1,0:T(8,128)(2,1)S(1)}, u32[]{:S(2)}, u32[]{:S(2)}) async-start(bf16[4,256,896]{2,1,0:T(8,128)(2,1)} %copy-done), calls=%async_computation.1 | async-start | bytes 3670016 | tf_op jit(solution)/shard_map/all_to_all | solution.py:373
  50.5 0.0 copy-done.2
  50.5 2.9 %collective-permute-start = (bf16[64,128]{1,0:T(8,128)(2,1)S(1)}, bf16[64,128]{1,0:T(8,128)(2,1)S(1)}, u32[]{:S(2)}, u32[]{:S(2)}) collective-permute-start(bf16[64,128]{1,0:T(8,128)(2,1)S(1)} %copy-done.2), channel_id=1, source_target_pairs={{0,128},{32,160},{64,192},{96,224},{128,256},{160,288},{192,320},{... | collective-permute-start | bytes 49160 | tf_op jit(solution)/shard_map/ppermute | solution.py:311
  53.4 9.1 %collective-permute-start.1 = (bf16[64,128]{1,0:T(8,128)(2,1)S(1)}, bf16[64,128]{1,0:T(8,128)(2,1)S(1)}, u32[]{:S(2)}, u32[]{:S(2)}) collective-permute-start(bf16[64,128]{1,0:T(8,128)(2,1)S(1)} %copy-done.2), channel_id=1, source_target_pairs={{0,256},{32,288},{64,320},{96,352},{128,384},{160,416},{192,448},{... | collective-permute-start | bytes 49160 | tf_op jit(solution)/shard_map/ppermute | solution.py:311
  62.5 4.3 %collective-permute-start.2 = (bf16[64,128]{1,0:T(8,128)(2,1)S(1)}, bf16[64,128]{1,0:T(8,128)(2,1)S(1)}, u32[]{:S(2)}, u32[]{:S(2)}) collective-permute-start(bf16[64,128]{1,0:T(8,128)(2,1)S(1)} %copy-done.2), channel_id=1, source_target_pairs={{0,384},{32,416},{64,448},{96,480},{128,0},{160,32},{192,64},{224,... | collective-permute-start | bytes 49160 | tf_op jit(solution)/shard_map/ppermute | solution.py:311
  66.8 0.0 collective-permute-done.refs_6_
  66.8 0.0 collective-permute-done.1.refs_7_
  66.8 4.1 %collective-permute-done.2.refs_8_ = bf16[64,128]{1,0:T(8,128)(2,1)S(1)} collective-permute-done((bf16[64,128]{1,0:T(8,128)(2,1)S(1)}, bf16[64,128]{1,0:T(8,128)(2,1)S(1)}, u32[]{:S(2)}, u32[]{:S(2)}) %collective-permute-start.2) | collective-permute-done | bytes 16416 | tf_op jit(solution)/shard_map/ppermute | solution.py:311
  70.9 0.0 all-to-all-done.1.refs_1_
  70.9 0.0 copy-done.1
  70.9 0.0 copy-done.5
  70.9 0.0 copy-done.6
  70.9 2.3 %shard_map.178 = (bf16[912,128]{1,0:T(8,128)(2,1)S(1)}, bf16[256,128]{1,0:T(8,128)(2,1)S(1)}, f32[256,128]{1,0:T(8,128)S(1)}, f32[256,128]{1,0:T(8,128)S(1)}, f32[256,128]{1,0:T(8,128)S(1)}) custom-call(s32[1]{0:T(128)} %bitcast.1.refs_0_.group_ref, bf16[4,256,896]{2,1,0:T(8,128)(2,1)S(1)} %all-to-all-done.1.refs_1_, f32[1,128]{1,0:T(1,128)S(1)} %bitcast.21, ...), custom_call_target="tpu_custom_call" | custom-call | tf_op jit(solution)/shard_map/pallas_call | solution.py:377
  73.3 14.0 %all-gather = bf16[3648,128]{1,0:T(8,128)(2,1)S(1)} all-gather(bf16[912,128]{1,0:T(8,128)(2,1)S(1)} %get-tuple-element.19), channel_id=2, replica_groups={{0,32,64,96},{128,160,192,224},{256,288,320,352},{384,416,448,480},{1,3..., dimensions={0}, use_global_device_ids=true | all-gather | bytes 1167360 | tf_op jit(solution)/shard_map/all_gather | solution.py:403
  87.3 1.2 broadcast_in_dim.14
  88.6 0.0 copy-start.3
  88.6 0.0 copy-start.4
  88.6 4.0 %all-to-all-start.2 = ((bf16[4,4,4,2,32,128]{5,4,3,2,1,0:T(8,128)(2,1)}), bf16[4,4,4,2,32,128]{5,4,3,2,1,0:T(8,128)(2,1)S(1)}, u32[]{:S(2)}, u32[]{:S(2)}) async-start(bf16[4,4,4,2,32,128]{5,4,3,2,1,0:T(8,128)(2,1)} %broadcast_in_dim.14), calls=%async_computation.2 | async-start | bytes 2097152 | tf_op jit(solution)/shard_map/all_to_all | solution.py:306
  92.6 1.3 collective-permute-start.3
  93.9 1.3 collective-permute-start.4
  95.2 1.3 collective-permute-start.5
  97.1 5.2 %collective-permute-done.3.refs_0_ = bf16[256,128]{1,0:T(8,128)(2,1)S(1)} collective-permute-done((bf16[256,128]{1,0:T(8,128)(2,1)S(1)}, bf16[256,128]{1,0:T(8,128)(2,1)S(1)}, u32[]{:S(2)}, u32[]{:S(2)}) %collective-permute-start.3) | collective-permute-done | bytes 65568 | tf_op jit(solution)/shard_map/ppermute | solution.py:401
  102.3 5.5 %collective-permute-done.4.refs_1_ = bf16[256,128]{1,0:T(8,128)(2,1)S(1)} collective-permute-done((bf16[256,128]{1,0:T(8,128)(2,1)S(1)}, bf16[256,128]{1,0:T(8,128)(2,1)S(1)}, u32[]{:S(2)}, u32[]{:S(2)}) %collective-permute-start.4) | collective-permute-done | bytes 65568 | tf_op jit(solution)/shard_map/ppermute | solution.py:401
  107.8 2.1 %collective-permute-done.5.refs_2_ = bf16[256,128]{1,0:T(8,128)(2,1)S(1)} collective-permute-done((bf16[256,128]{1,0:T(8,128)(2,1)S(1)}, bf16[256,128]{1,0:T(8,128)(2,1)S(1)}, u32[]{:S(2)}, u32[]{:S(2)}) %collective-permute-start.5) | collective-permute-done | bytes 65568 | tf_op jit(solution)/shard_map/ppermute | solution.py:401
  109.9 5.2 %shard_map.179 = (bf16[400,128]{1,0:T(8,128)(2,1)S(1)}, bf16[400,128]{1,0:T(8,128)(2,1)S(1)}, bf16[400,128]{1,0:T(8,128)(2,1)S(1)}) custom-call(s32[1]{0:T(128)} %bitcast.1.refs_0_.group_ref, f32[1]{0:T(128)S(6)} %copy.19.shift_ref, bf16[4,912,128]{2,1,0:T(8,128)(2,1)S(1)} %bitcast.15, bf16[256,128]{1,0:T(8,128)(2,1)S(1)} %collective-permute-done.3.refs_0_, ...), custom_call_target="tpu_custom_call" | custom-call | tf_op jit(solution)/shard_map/pallas_call | solution.py:404
  115.1 4.1 %collective-permute-start.6 = (bf16[400,128]{1,0:T(8,128)(2,1)S(1)}, bf16[400,128]{1,0:T(8,128)(2,1)S(1)}, u32[]{:S(2)}, u32[]{:S(2)}) collective-permute-start(bf16[400,128]{1,0:T(8,128)(2,1)S(1)} %get-tuple-element.23), channel_id=1, source_target_pairs={{0,128},{32,160},{64,192},{96,224},{128,256},{160,288},{192,320},{... | collective-permute-start | bytes 307208 | tf_op jit(solution)/shard_map/ppermute | solution.py:411
  119.2 1.3 collective-permute-start.7
  120.5 1.3 collective-permute-start.8
  121.8 0.2 collective-permute-done.6.refs_0_
  122.0 3.1 %collective-permute-done.7.refs_1_ = bf16[400,128]{1,0:T(8,128)(2,1)S(1)} collective-permute-done((bf16[400,128]{1,0:T(8,128)(2,1)S(1)}, bf16[400,128]{1,0:T(8,128)(2,1)S(1)}, u32[]{:S(2)}, u32[]{:S(2)}) %collective-permute-start.7) | collective-permute-done | bytes 102432 | tf_op jit(solution)/shard_map/ppermute | solution.py:411
  125.1 3.0 %collective-permute-done.8.refs_2_ = bf16[400,128]{1,0:T(8,128)(2,1)S(1)} collective-permute-done((bf16[400,128]{1,0:T(8,128)(2,1)S(1)}, bf16[400,128]{1,0:T(8,128)(2,1)S(1)}, u32[]{:S(2)}, u32[]{:S(2)}) %collective-permute-start.8) | collective-permute-done | bytes 102432 | tf_op jit(solution)/shard_map/ppermute | solution.py:411
  128.1 0.0 all-to-all-done.2.weight_ref
  128.1 0.0 copy-done.3
  128.1 0.0 copy-done.4
  128.1 3.3 %shard_map.180 = (bf16[256,2048]{1,0:T(8,128)(2,1)S(1)}, f32[1,256]{1,0:T(1,128)}) custom-call(s32[1]{0:T(128)} %bitcast.place_ref, f32[1]{0:T(128)S(6)} %copy.19.shift_ref, bf16[256,128]{1,0:T(8,128)(2,1)S(1)} %get-tuple-element.18.query_ref, bf16[4,912,128]{2,1,0:T(8,128)(2,1)S(1)} %bitcast.16, f32[256,128]{1,0:T(8,128)S(1)} %get-tuple-element.20.inner_ref, ...), custom_call_target="tpu_custom_call" | custom-call | tf_op jit(solution)/shard_map/pallas_call | solution.py:415
  131.4 34.5 %all_to_all.20 = bf16[8,32,2048]{2,1,0:T(8,128)(2,1)S(1)} all-to-all(bf16[8,32,2048]{2,1,0:T(8,128)(2,1)S(1)} %bitcast.17), channel_id=1, replica_groups=mesh['sp'=16,'fs'=4,'tp'=8] {'tp'}, dimensions={0} | all-to-all | bytes 2097152 | tf_op jit(solution)/shard_map/all_to_all | solution.py:433
  165.9 0.8 reduce_sum.12
  (1 shorter events, 0.0 us)
Async XLA Ops:
  4.0 5.2 %copy-start.7 = (bf16[32,896]{1,0:T(8,128)(2,1)S(1)}, bf16[32,896]{1,0:T(8,128)(2,1)}, u32[]{:S(2)}) copy-start(bf16[32,896]{1,0:T(8,128)(2,1)} %get-tuple-element.16) | copy-start | bytes 172036
  4.0 39.2 %all-to-all-start = ((bf16[4,256,512]{2,1,0:T(8,128)(2,1)}), bf16[4,256,512]{2,1,0:T(8,128)(2,1)S(1)}, u32[]{:S(2)}, u32[]{:S(2)}) async-start(bf16[4,256,512]{2,1,0:T(8,128)(2,1)} %get-tuple-element.15), calls=%async_computation | async-start | bytes 2097152 | tf_op jit(solution)/shard_map/all_to_all | solution.py:369
  44.4 1.3 copy-start
  45.6 4.9 %copy-start.2 = (bf16[64,128]{1,0:T(8,128)(2,1)S(1)}, bf16[64,128]{1,0:T(8,128)(2,1)}, u32[]{:S(2)}) copy-start(bf16[64,128]{1,0:T(8,128)(2,1)} %get-tuple-element.17.refs_5_) | copy-start | bytes 49156
  45.6 25.3 %copy-start.1 = (f32[1,256,128]{2,1,0:T(8,128)S(1)}, f32[1,256,128]{2,1,0:T(8,128)}, u32[]{:S(2)}) copy-start(f32[1,256,128]{2,1,0:T(8,128)} %param.33) | copy-start | bytes 393220
  45.6 25.3 %copy-start.5 = (f32[128]{0:T(128)S(1)}, f32[128]{0:T(128)}, u32[]{:S(2)}) copy-start(f32[128]{0:T(128)} %param.31) | copy-start | bytes 1540
  45.7 25.3 %copy-start.6 = (f32[128]{0:T(128)S(1)}, f32[128]{0:T(128)}, u32[]{:S(2)}) copy-start(f32[128]{0:T(128)} %param.32) | copy-start | bytes 1540
  45.7 25.2 %all-to-all-start.1 = ((bf16[4,256,896]{2,1,0:T(8,128)(2,1)}), bf16[4,256,896]{2,1,0:T(8,128)(2,1)S(1)}, u32[]{:S(2)}, u32[]{:S(2)}) async-start(bf16[4,256,896]{2,1,0:T(8,128)(2,1)} %copy-done), calls=%async_computation.1 | async-start | bytes 3670016 | tf_op jit(solution)/shard_map/all_to_all | solution.py:373
  50.5 16.3 %collective-permute-start = (bf16[64,128]{1,0:T(8,128)(2,1)S(1)}, bf16[64,128]{1,0:T(8,128)(2,1)S(1)}, u32[]{:S(2)}, u32[]{:S(2)}) collective-permute-start(bf16[64,128]{1,0:T(8,128)(2,1)S(1)} %copy-done.2), channel_id=1, source_target_pairs={{0,128},{32,160},{64,192},{96,224},{128,256},{160,288},{192,320},{... | collective-permute-start | bytes 49160 | tf_op jit(solution)/shard_map/ppermute | solution.py:311
  53.4 13.4 %collective-permute-start.1 = (bf16[64,128]{1,0:T(8,128)(2,1)S(1)}, bf16[64,128]{1,0:T(8,128)(2,1)S(1)}, u32[]{:S(2)}, u32[]{:S(2)}) collective-permute-start(bf16[64,128]{1,0:T(8,128)(2,1)S(1)} %copy-done.2), channel_id=1, source_target_pairs={{0,256},{32,288},{64,320},{96,352},{128,384},{160,416},{192,448},{... | collective-permute-start | bytes 49160 | tf_op jit(solution)/shard_map/ppermute | solution.py:311
  62.5 8.4 %collective-permute-start.2 = (bf16[64,128]{1,0:T(8,128)(2,1)S(1)}, bf16[64,128]{1,0:T(8,128)(2,1)S(1)}, u32[]{:S(2)}, u32[]{:S(2)}) collective-permute-start(bf16[64,128]{1,0:T(8,128)(2,1)S(1)} %copy-done.2), channel_id=1, source_target_pairs={{0,384},{32,416},{64,448},{96,480},{128,0},{160,32},{192,64},{224,... | collective-permute-start | bytes 49160 | tf_op jit(solution)/shard_map/ppermute | solution.py:311
  88.6 39.6 %copy-start.3 = (f32[128]{0:T(128)S(1)}, f32[128]{0:T(128)}, u32[]{:S(2)}) copy-start(f32[128]{0:T(128)} %param.29) | copy-start | bytes 1540
  88.6 39.6 %copy-start.4 = (f32[128]{0:T(128)S(1)}, f32[128]{0:T(128)}, u32[]{:S(2)}) copy-start(f32[128]{0:T(128)} %param.30) | copy-start | bytes 1540
  88.6 39.6 %all-to-all-start.2 = ((bf16[4,4,4,2,32,128]{5,4,3,2,1,0:T(8,128)(2,1)}), bf16[4,4,4,2,32,128]{5,4,3,2,1,0:T(8,128)(2,1)S(1)}, u32[]{:S(2)}, u32[]{:S(2)}) async-start(bf16[4,4,4,2,32,128]{5,4,3,2,1,0:T(8,128)(2,1)} %broadcast_in_dim.14), calls=%async_computation.2 | async-start | bytes 2097152 | tf_op jit(solution)/shard_map/all_to_all | solution.py:306
  92.6 9.8 %collective-permute-start.3 = (bf16[256,128]{1,0:T(8,128)(2,1)S(1)}, bf16[256,128]{1,0:T(8,128)(2,1)S(1)}, u32[]{:S(2)}, u32[]{:S(2)}) collective-permute-start(bf16[256,128]{1,0:T(8,128)(2,1)S(1)} %get-tuple-element.18.query_ref), channel_id=1, source_target_pairs={{128,0},{160,32},{192,64},{224,96},{256,128},{288,160},{320,192},{... | collective-permute-start | bytes 196616 | tf_op jit(solution)/shard_map/ppermute | solution.py:401
  93.9 13.9 %collective-permute-start.4 = (bf16[256,128]{1,0:T(8,128)(2,1)S(1)}, bf16[256,128]{1,0:T(8,128)(2,1)S(1)}, u32[]{:S(2)}, u32[]{:S(2)}) collective-permute-start(bf16[256,128]{1,0:T(8,128)(2,1)S(1)} %get-tuple-element.18.query_ref), channel_id=1, source_target_pairs={{256,0},{288,32},{320,64},{352,96},{384,128},{416,160},{448,192},{... | collective-permute-start | bytes 196616 | tf_op jit(solution)/shard_map/ppermute | solution.py:401
  95.2 14.7 %collective-permute-start.5 = (bf16[256,128]{1,0:T(8,128)(2,1)S(1)}, bf16[256,128]{1,0:T(8,128)(2,1)S(1)}, u32[]{:S(2)}, u32[]{:S(2)}) collective-permute-start(bf16[256,128]{1,0:T(8,128)(2,1)S(1)} %get-tuple-element.18.query_ref), channel_id=1, source_target_pairs={{384,0},{416,32},{448,64},{480,96},{385,1},{417,33},{449,65},{481,... | collective-permute-start | bytes 196616 | tf_op jit(solution)/shard_map/ppermute | solution.py:401
  115.1 6.9 %collective-permute-start.6 = (bf16[400,128]{1,0:T(8,128)(2,1)S(1)}, bf16[400,128]{1,0:T(8,128)(2,1)S(1)}, u32[]{:S(2)}, u32[]{:S(2)}) collective-permute-start(bf16[400,128]{1,0:T(8,128)(2,1)S(1)} %get-tuple-element.23), channel_id=1, source_target_pairs={{0,128},{32,160},{64,192},{96,224},{128,256},{160,288},{192,320},{... | collective-permute-start | bytes 307208 | tf_op jit(solution)/shard_map/ppermute | solution.py:411
  119.2 5.9 %collective-permute-start.7 = (bf16[400,128]{1,0:T(8,128)(2,1)S(1)}, bf16[400,128]{1,0:T(8,128)(2,1)S(1)}, u32[]{:S(2)}, u32[]{:S(2)}) collective-permute-start(bf16[400,128]{1,0:T(8,128)(2,1)S(1)} %get-tuple-element.24), channel_id=1, source_target_pairs={{0,256},{32,288},{64,320},{96,352},{128,384},{160,416},{192,448},{... | collective-permute-start | bytes 307208 | tf_op jit(solution)/shard_map/ppermute | solution.py:411
  120.5 7.6 %collective-permute-start.8 = (bf16[400,128]{1,0:T(8,128)(2,1)S(1)}, bf16[400,128]{1,0:T(8,128)(2,1)S(1)}, u32[]{:S(2)}, u32[]{:S(2)}) collective-permute-start(bf16[400,128]{1,0:T(8,128)(2,1)S(1)} %get-tuple-element.25), channel_id=1, source_target_pairs={{0,384},{32,416},{64,448},{96,480},{1,385},{33,417},{65,449},{97,4... | collective-permute-start | bytes 307208 | tf_op jit(solution)/shard_map/ppermute | solution.py:411
where the time goes:
time: 167 us
  blocking collectives  82.5 us (49%)
  starting transfers between devices  40.8 us (24%)
  waiting for transfers between devices  23.2 us (14%)
  Pallas kernels  15.3 us (9%)
  local copies, waits for them, and re-layouts  2.55 us (2%)
    all_to_all x1, blocking collectives, on_device(): lax.all_to_all(projected.reshape(tp, tokens // tp, width), 'tp', 0, 0, ti...  34.5 us
    all_gather x1, blocking collectives, on_device(): column = lax.all_gather(packed, 'sp', axis=0, tiled=True)  34 us
    ppermute x3, starting transfers between devices, turned(): lax.ppermute(array, axis, [(k, (k + places) % size) for k in range(size)])  16.3 us
    all_gather x1, blocking collectives, on_device(): gathered = lax.all_gather(message, 'sp', axis_index_groups=groups)  14 us
    ppermute x3, waiting for transfers between devices, on_device(): queries.append(lax.ppermute(query, 'sp', places))  12.8 us
    ppermute x3, starting transfers between devices, on_device(): lax.ppermute(far[j - 1], 'sp', [(k, k + NEAR * j) for k in range(sp - NEA...  6.69 us
    ppermute x3, waiting for transfers between devices, on_device(): lax.ppermute(far[j - 1], 'sp', [(k, k + NEAR * j) for k in range(sp - NEA...  6.33 us
    pallas_call x1, Pallas kernels, on_device(): vmem_call(far_kernel, tuple((shape((tokens + TILE + HEAD, HEAD), BF16) fo...  5.16 us
  transfers between devices with their start and end apart: 12, of which 7 were waited for; matrix products, arithmetic and copies ran while one was open for 0% of the time, Pallas kernels for 3%

commit v1 on v0

--- a/solution.py
+++ b/solution.py
@@ -86,30 +86,44 @@
             slices_ref[k, :, b * HEAD : (b + 1) * HEAD] = moved[:, k * HEAD : (k + 1) * HEAD]
 
 
-def partial_kernel(rows_ref, weight_ref, out_ref):
+def partial_kernel(rows_ref, weight_ref, first_ref, second_ref):
+    cut = first_ref.shape[2]
     weight = weight_ref[...]
     for k in range(rows_ref.shape[0]):
-        out_ref[k] = dot(rows_ref[k], weight).astype(BF16)
-
-
-def local_recurrence_kernel(*refs):
-    group_ref, products_ref, floor_ref, offset_ref, extra_hbm = refs[:5]
-    own = refs[5:-7]
-    message_ref, query_ref, inner_ref, query_decayed_ref, gate_ref, extra_ref, arrived = refs[-7:]
-    copy = pltpu.make_async_copy(extra_hbm, extra_ref, arrived)
-    copy.start()
+        first_ref[k] = dot(rows_ref[k], weight[:, :cut]).astype(BF16)
+    for k in range(rows_ref.shape[0]):
+        second_ref[k] = dot(rows_ref[k], weight[:, cut:]).astype(BF16)
+
+
+def sum_of(products_ref):
     total = products_ref[0].astype(F32)
     for k in range(1, products_ref.shape[0]):
         total = total + products_ref[k].astype(F32)
-    total = total.astype(BF16)
-    columns = [total[:, k * HEAD : (k + 1) * HEAD] for k in range(7)]
-    query_ref[...] = columns[2]
-    query_b = columns[3].astype(F32)
+    return total.astype(BF16)
+
+
+def attention_inputs_kernel(products_ref, own_ref, far_ref, key_value_ref):
+    total = sum_of(products_ref)
+    length = total.shape[0]
+    key_value_ref[0:length] = total[:, 0:HEAD]
+    key_value_ref[length : 2 * length] = total[:, HEAD : 2 * HEAD]
+    far_ref[0:length] = total[:, 2 * HEAD :]
+    far_ref[length : length + 2 * ROWS] = own_ref[...]
+
+
+def local_recurrence_kernel(*refs):
+    products_ref, floor_ref, offset_ref, extra_hbm, key_value_ref, slots_ref = refs[:6]
+    message_ref, inner_ref, query_decayed_ref, gate_ref, extra_ref, arrived = refs[6:]
+    copy = pltpu.make_async_copy(extra_hbm, extra_ref, arrived)
+    copy.start()
+    total = sum_of(products_ref)
+    columns = [total[:, k * HEAD : (k + 1) * HEAD] for k in range(4)]
+    query_b = columns[0].astype(F32)
     query = query_b / (1.0 + jnp.exp(-query_b))
-    value = columns[5]
-    gate_b = columns[6].astype(F32)
+    value = columns[2]
+    gate_b = columns[3].astype(F32)
     gate_ref[...] = gate_b / (1.0 + jnp.exp(-gate_b))
-    u = columns[4].astype(F32) + offset_ref[...]
+    u = columns[1].astype(F32) + offset_ref[...]
     key = (1.0 - floor_ref[...]) / (1.0 + jnp.exp(u))
     copy.wait()
     log_forget = jnp.log(1.0 - key) + extra_ref[...]
@@ -153,14 +167,12 @@
     state = dot(value, key_high, ((0,), (0,))) + dot(value, key_low, ((0,), (0,)))
     at = 0
     vector = jnp.broadcast_to(jnp.exp(final), (TILE, HEAD)).astype(BF16)
-    for piece in (columns[0], columns[1], state.astype(BF16), vector):
+    for piece in (key_value_ref[...], state.astype(BF16), vector):
         message_ref[at : at + piece.shape[0]] = piece
         at += piece.shape[0]
-    groups = len(own)
-    for k in range(groups):
-        slot = (group_ref[0] + groups - k) % groups
-        start = pl.multiple_of(at + slot * 2 * ROWS, TILE)
-        message_ref[pl.ds(start, 2 * ROWS)] = own[k][...]
+    for k in range(slots_ref.shape[0]):
+        message_ref[at : at + 2 * ROWS] = slots_ref[k, slots_ref.shape[1] - 2 * ROWS :]
+        at += 2 * ROWS
 
 
 def chain(message_ref, start, count):
@@ -214,25 +226,26 @@
     return jnp.concatenate(pieces, axis=0)
 
 
-def far_kernel(group_ref, shift_ref, message_ref, *refs):
-    count = len(refs) // 2
+def far_kernel(group_ref, shift_ref, message_ref, query_ref, *out_refs):
+    count = query_ref.shape[0]
+    length = message_ref.shape[1] - count * 2 * ROWS - HEAD - TILE
+    length = length // 2
     shift = shift_ref[0]
     near = message_ref.shape[0]
-    length = refs[0].shape[0]
-    for j in range(count):
-        out_ref = refs[count + j]
-        wanted = group_ref[0] + j < count
+    index = lax.broadcasted_iota(jnp.int32, (TILE, HEAD), 0)
+    for j, out_ref in enumerate(out_refs):
+        wanted = group_ref[0] + j + 1 < count
 
         @pl.when(wanted)
-        def _(query_ref=refs[j], out_ref=out_ref):
-            weighted, total = attend_near(query_ref[...], message_ref, shift)
+        def _(j=j, out_ref=out_ref):
+            query = query_ref[group_ref[0] + j + 1, 0:length]
+            weighted, total = attend_near(query, message_ref, shift)
             out_ref[0:length] = weighted.astype(BF16)
             decay, state = chain(message_ref, 2 * length, near)
             high, low = parts(as_row(total))
             pieces = [
                 piece[:, k * HEAD : (k + 1) * HEAD] for piece in (high, low) for k in range(2)
             ]
-            index = lax.broadcasted_iota(jnp.int32, (TILE, HEAD), 0)
             vector = jnp.zeros((TILE, HEAD), F32)
             for k, piece in enumerate(pieces + [decay]):
                 vector = jnp.where(index == k, piece.astype(F32), vector)
@@ -244,11 +257,19 @@
             out_ref[...] = jnp.zeros(out_ref.shape, BF16)
 
 
+def near_kernel(place_ref, shift_ref, query_ref, message_ref, weighted_ref, total_ref):
+    place = place_ref[0]
+    length = weighted_ref.shape[0]
+    weighted, total = attend_near(query_ref[0:length], message_ref, shift_ref[0], place)
+    weighted_ref[...] = weighted
+    total_ref[...] = jnp.broadcast_to(total, total_ref.shape)
+
+
 def final_kernel(
     place_ref,
-    shift_ref,
-    query_ref,
     message_ref,
+    weighted_ref,
+    spent_ref,
     inner_ref,
     query_decayed_ref,
     gate_ref,
@@ -258,10 +279,7 @@
     *refs,
 ):
     far_refs, out_ref, total_ref = refs[:-2], refs[-2], refs[-1]
-    place = place_ref[0]
-    shift = shift_ref[0]
-    query = query_ref[...]
-    length = query.shape[0]
+    length = weighted_ref.shape[0]
     incoming = jnp.zeros((HEAD, HEAD), F32)
     outside = jnp.zeros((length, HEAD), F32)
     outside_row = jnp.zeros((1, length), F32)
@@ -275,16 +293,16 @@
         ].astype(F32)
         outside = ref[0:length].astype(F32) + jnp.exp(-as_column(row)) * outside
         outside_row = outside_row + row
-    decay, state = chain(message_ref, 2 * length, place)
+    decay, state = chain(message_ref, 2 * length, place_ref[0])
     state = state + decay * incoming
     recurrent = inner_ref[...] + dot_both(query_decayed_ref[...], state, ((1,), (1,)))
     square_mean = jnp.mean(recurrent * recurrent, axis=-1, keepdims=True)
     mixed_b = (
         recurrent * lax.rsqrt(square_mean + epsilon) * gain_b_ref[...] * gate_ref[...]
     ).astype(BF16)
-    weighted, total = attend_near(query, message_ref, shift, place)
-    weighted = weighted + jnp.exp(-total) * outside
-    total_row = as_row(total) + outside_row
+    total = spent_ref[...]
+    weighted = weighted_ref[...] + jnp.exp(-total) * outside
+    total_row = jnp.transpose(total)[0:1] + outside_row
     total_ref[...] = jnp.log(jnp.maximum(1.0 - jnp.exp(-total_row), log_floor))
     square_mean = jnp.mean(weighted * weighted, axis=-1, keepdims=True)
     mixed_a = (weighted * lax.rsqrt(square_mean + epsilon) * gain_a_ref[...]).astype(BF16)
@@ -300,15 +318,8 @@
             out_ref[:, at : at + width] = dot(mixed, both, ((1,), (1,))).astype(BF16)
 
 
-def over_fs(shard):
-    size = lax.axis_size("fs")
-    copies = jnp.broadcast_to(shard[None], (size, *shard.shape))
-    return lax.all_to_all(copies, "fs", 0, 0, tiled=True)
-
-
-def turned(array, axis, places):
-    size = lax.axis_size(axis)
-    return lax.ppermute(array, axis, [(k, (k + places) % size) for k in range(size)])
+def copies(array, size):
+    return jnp.broadcast_to(array[None], (size, *array.shape))
 
 
 def on_device(
@@ -367,68 +378,80 @@
         emitted_projection_linear_scan,
     )
     rows = lax.all_to_all(slices, "fs", 0, 0, tiled=True)
-    out_slots = [out_own] + [turned(out_own, "sp", NEAR * k) for k in range(1, count)]
     column = lax.all_gather(packed, "sp", axis=0, tiled=True)
-    products = vmem_call(partial_kernel, shape((fs, tokens, 7 * HEAD), BF16), 2)(rows, column)
-    products = lax.all_to_all(products, "fs", 0, 0, tiled=True)
+    first, second = vmem_call(
+        partial_kernel,
+        tuple(shape((fs, tokens, columns * HEAD), BF16) for columns in (3, 4)),
+        2,
+    )(rows, column)
+    first = lax.all_to_all(first, "fs", 0, 0, tiled=True)
+    own, key_value = vmem_call(
+        attention_inputs_kernel,
+        (shape((tokens + 2 * ROWS, HEAD), BF16), shape((2 * tokens, HEAD), BF16)),
+        2,
+    )(first, out_own)
+    second, _ = lax.optimization_barrier((second, own))
+    second = lax.all_to_all(second, "fs", 0, 0, tiled=True)
+    strided = [list(range(k, sp, NEAR)) for k in range(NEAR)]
+    across = lax.all_gather(own, "sp", axis_index_groups=strided)
 
     small = shape((tokens, HEAD), F32)
     start = 2 * tokens + HEAD + TILE
-    message, query, inner, query_decayed, gate = vmem_call(
+    message, inner, query_decayed, gate = vmem_call(
         local_recurrence_kernel,
-        (
-            shape((start + count * 2 * ROWS, HEAD), BF16),
-            shape((tokens, HEAD), BF16),
-            small,
-            small,
-            small,
-        ),
-        5 + count,
-        (0,),
-        (4,),
+        (shape((start + count * 2 * ROWS, HEAD), BF16), small, small, small),
+        6,
+        (),
+        (3,),
         (pltpu.VMEM((tokens, HEAD), F32), pltpu.SemaphoreType.DMA(())),
     )(
-        group,
-        products,
+        second,
         forget_floor.reshape(1, HEAD),
         forget_offset.reshape(1, HEAD),
         extra_log_decay[0],
-        *out_slots,
-    )
-    queries = []
-    for j in range(1, count):
-        places = [(k, k - NEAR * j) for k in range(NEAR * j, sp)]
-        queries.append(lax.ppermute(query, "sp", places))
+        key_value,
+        across,
+    )
     groups = [list(range(NEAR * k, NEAR * (k + 1))) for k in range(count)]
     gathered = lax.all_gather(message, "sp", axis_index_groups=groups)
+    out_weights = lax.all_to_all(
+        copies(gathered[:, start:].reshape(NEAR, count, 2, ROWS, HEAD), fs),
+        "fs",
+        0,
+        0,
+        tiled=True,
+    )
     far = vmem_call(
         far_kernel,
-        tuple(shape((tokens + TILE + HEAD, HEAD), BF16) for _ in queries),
-        2 + count,
+        tuple(shape((tokens + TILE + HEAD, HEAD), BF16) for _ in range(count - 1)),
+        4,
         (0, 1),
-    )(group, score_offset, gathered, *queries)
-    far = [
-        lax.ppermute(far[j - 1], "sp", [(k, k + NEAR * j) for k in range(sp - NEAR * j)])
-        for j in range(1, count)
-    ]
-    out_weights = over_fs(gathered[:, start:].reshape(NEAR, count, 2, ROWS, HEAD))
+    )(group, score_offset, gathered, across)
+    outside = []
+    for j in range(1, count):
+        places = [(k, k + NEAR * j) for k in range(sp - NEAR * j)]
+        outside.append(lax.ppermute(far[j - 1], "sp", places))
+    place = (rank % NEAR).reshape(1)
+    weighted, spent = vmem_call(near_kernel, (small, small), 4, (0, 1))(
+        place, score_offset, own, gathered
+    )
     projected, row_log_total = vmem_call(
         final_kernel,
         (shape((tokens, width), BF16), shape((1, tokens), F32)),
         9 + count,
-        (0, 1),
+        (0,),
     )(
-        (rank % NEAR).reshape(1),
-        score_offset,
-        query,
+        place,
         gathered,
+        weighted,
+        spent,
         inner,
         query_decayed,
         gate,
         attention_norm_gain.reshape(1, HEAD),
         recurrence_norm_gain.reshape(1, HEAD),
         out_weights,
-        *far,
+        *outside,
     )
     tiles = lax.all_to_all(projected.reshape(tp, tokens // tp, width), "tp", 0, 0, tiled=True)
     layer_out = jnp.sum(tiles.astype(F32), axis=0).astype(BF16)

time: 167 us -> 160 us (0.958)
  blocking collectives: 82.5 us -> 114 us
  starting transfers between devices: 40.8 us -> 19.7 us
  waiting for transfers between devices: 23.2 us -> 4.91 us
    ppermute x9 -> x3, starting transfers between devices: 26.8 us -> 7.31 us  [on_device(): outside.append(lax.ppermute(far[j - 1], 'sp', places))]
    ppermute x9 -> x3, waiting for transfers between devices: 23.2 us -> 4.9 us  [on_device(): outside.append(lax.ppermute(far[j - 1], 'sp', places))]
    all_gather x0 -> x1, blocking collectives: none -> 17.7 us  [on_device(): across = lax.all_gather(own, 'sp', axis_index_groups=strided)]
    all_to_all x0 -> x1, blocking collectives: none -> 13 us  [on_device(): first = lax.all_to_all(first, 'fs', 0, 0, tiled=True)]
    pallas_call x1 -> x3, Pallas kernels: 1.25 us -> 4.01 us  [the longest x1 2.24 us: on_device(): vmem_call(partial_kernel, tuple((shape((fs, tokens, columns * HEAD), BF16...]
  transfers between devices with their start and end apart: 12 -> 6, of which waited for: 7 -> 1; matrix products, arithmetic and copies ran while one was open for 0% -> 0% of each run, Pallas kernels for 3% -> 4%
where the time goes in v1:
time: 160 us
  blocking collectives  114 us (71%)
  starting transfers between devices  19.7 us (12%)
  Pallas kernels  16.4 us (10%)
  waiting for transfers between devices  4.91 us (3%)
  local copies, waits for them, and re-layouts  2.61 us (2%)
    all_to_all x1, blocking collectives, on_device(): lax.all_to_all(projected.reshape(tp, tokens // tp, width), 'tp', 0, 0, ti...  34.8 us
    all_gather x1, blocking collectives, on_device(): column = lax.all_gather(packed, 'sp', axis=0, tiled=True)  34 us
    all_gather x1, blocking collectives, on_device(): across = lax.all_gather(own, 'sp', axis_index_groups=strided)  17.7 us
    all_gather x1, blocking collectives, on_device(): gathered = lax.all_gather(message, 'sp', axis_index_groups=groups)  14.3 us
    all_to_all x1, blocking collectives, on_device(): first = lax.all_to_all(first, 'fs', 0, 0, tiled=True)  13 us
    ppermute x3, starting transfers between devices, on_device(): outside.append(lax.ppermute(far[j - 1], 'sp', places))  7.31 us
    pallas_call x1, Pallas kernels, on_device(): vmem_call(far_kernel, tuple((shape((tokens + TILE + HEAD, HEAD), BF16) fo...  5.16 us
    all_to_all x1, starting transfers between devices, on_device(): rows = lax.all_to_all(slices, 'fs', 0, 0, tiled=True)  5.15 us
  transfers between devices with their start and end apart: 6, of which 1 were waited for; matrix products, arithmetic and copies ran while one was open for 0% of the time, Pallas kernels for 4%

profile of v1, /device:TPU:1, one launch (start us, length us, event | category | flops | bytes accessed | tf_op | source)
XLA Modules:
  0.0 159.7 jit_solution(11349360661250619448)
XLA Ops:
  0.6 3.3 %shard_map.176 = (bf16[4,256,512]{2,1,0:T(8,128)(2,1)}, bf16[32,896]{1,0:T(8,128)(2,1)}, bf16[64,128]{1,0:T(8,128)(2,1)}) custom-call(bf16[256,2048]{1,0:T(8,128)(2,1)} %bitcast.28, f32[1,2048]{1,0:T(1,128)} %bitcast.30, bf16[32,128]{1,0:T(8,128)(2,1)} %refs_0_.1, bf16[32,128]{1,0:T(8,128)(2,1)} %refs_1_.1, bf16[32,128]{1,0:T(8,128)(2,1)} %refs_2_.1, ...), custom_call_target="tpu_custom_call" | custom-call | tf_op jit(solution)/shard_map/pallas_call | solution.py:352
  4.0 0.0 copy-start.6
  4.0 5.2 %all-to-all-start = ((bf16[4,256,512]{2,1,0:T(8,128)(2,1)}), bf16[4,256,512]{2,1,0:T(8,128)(2,1)S(1)}, u32[]{:S(2)}, u32[]{:S(2)}) async-start(bf16[4,256,512]{2,1,0:T(8,128)(2,1)} %get-tuple-element.21), calls=%async_computation | async-start | bytes 2097152 | tf_op jit(solution)/shard_map/all_to_all | solution.py:380
  9.1 0.0 copy-done.6
  9.1 34.0 %all_gather.15.weight_ref = bf16[512,896]{1,0:T(8,128)(2,1)S(1)} all-gather(bf16[32,896]{1,0:T(8,128)(2,1)S(1)} %copy-done.6), channel_id=1, replica_groups=mesh['sp'=16,'fs'=4,'tp'=8] {'sp'}, dimensions={0}, use_global_device_ids=true | all-gather | bytes 974848 | tf_op jit(solution)/shard_map/all_gather | solution.py:381
  43.1 0.0 all-to-all-done.rows_ref
  43.1 2.2 %shard_map.177 = (bf16[4,256,384]{2,1,0:T(8,128)(2,1)S(1)}, bf16[4,256,512]{2,1,0:T(8,128)(2,1)}) custom-call(bf16[4,256,512]{2,1,0:T(8,128)(2,1)S(1)} %all-to-all-done.rows_ref, bf16[512,896]{1,0:T(8,128)(2,1)S(1)} %all_gather.15.weight_ref), custom_call_target="tpu_custom_call" | custom-call | tf_op jit(solution)/shard_map/pallas_call | solution.py:382
  45.4 0.0 copy-start.1
  45.4 13.0 %all_to_all.25.products_ref = bf16[4,256,384]{2,1,0:T(8,128)(2,1)S(1)} all-to-all(bf16[4,256,384]{2,1,0:T(8,128)(2,1)S(1)} %get-tuple-element.24), channel_id=1, replica_groups=mesh['sp'=16,'fs'=4,'tp'=8] {'fs'}, dimensions={0} | all-to-all | bytes 1572864 | tf_op jit(solution)/shard_map/all_to_all | solution.py:387
  58.3 0.0 copy-done.1
  58.3 0.1 shard_map.178
  58.4 3.5 %all-to-all-start.2 = ((bf16[4,256,512]{2,1,0:T(8,128)(2,1)}), bf16[4,256,512]{2,1,0:T(8,128)(2,1)S(1)}, u32[]{:S(2)}, u32[]{:S(2)}) async-start(bf16[4,256,512]{2,1,0:T(8,128)(2,1)} %get-tuple-element.27), calls=%async_computation.2 | async-start | bytes 2097152 | tf_op jit(solution)/shard_map/all_to_all | solution.py:394
  62.0 0.0 copy-start
  62.0 17.7 %all-gather = bf16[1280,128]{1,0:T(8,128)(2,1)S(1)} all-gather(bf16[320,128]{1,0:T(8,128)(2,1)S(1)} %get-tuple-element.26.query_ref), channel_id=2, replica_groups={{0,128,256,384},{32,160,288,416},{64,192,320,448},{96,224,352,480},{1,1..., dimensions={0}, use_global_device_ids=true | all-gather | bytes 409600 | tf_op jit(solution)/shard_map/all_gather | solution.py:396
  79.6 0.0 all-to-all-done.2.refs_0_
  79.6 0.0 copy-start.2
  79.6 0.0 copy-start.3
  79.6 0.0 copy-done
  79.7 0.6 copy-done.2
  80.3 0.0 copy-done.3
  80.3 2.2 %shard_map.179 = (bf16[912,128]{1,0:T(8,128)(2,1)S(1)}, f32[256,128]{1,0:T(8,128)S(1)}, f32[256,128]{1,0:T(8,128)S(1)}, f32[256,128]{1,0:T(8,128)S(1)}) custom-call(bf16[4,256,512]{2,1,0:T(8,128)(2,1)S(1)} %all-to-all-done.2.refs_0_, f32[1,128]{1,0:T(1,128)S(1)} %bitcast.23, f32[1,128]{1,0:T(1,128)S(1)} %bitcast.24, f32[256,128]{1,0:T(8,128)S(1)} %bitcast.22, ...), custom_call_target="tpu_custom_call" | custom-call | tf_op jit(solution)/shard_map/pallas_call | solution.py:400
  82.5 14.3 %all-gather.1 = bf16[3648,128]{1,0:T(8,128)(2,1)S(1)} all-gather(bf16[912,128]{1,0:T(8,128)(2,1)S(1)} %get-tuple-element.29), channel_id=3, replica_groups={{0,32,64,96},{128,160,192,224},{256,288,320,352},{384,416,448,480},{1,3..., dimensions={0}, use_global_device_ids=true | all-gather | bytes 1167360 | tf_op jit(solution)/shard_map/all_gather | solution.py:416
  96.8 1.2 broadcast_in_dim.14
  98.1 3.7 %all-to-all-start.3 = ((bf16[4,4,4,2,32,128]{5,4,3,2,1,0:T(8,128)(2,1)}), bf16[4,4,4,2,32,128]{5,4,3,2,1,0:T(8,128)(2,1)S(1)}, u32[]{:S(2)}, u32[]{:S(2)}) async-start(bf16[4,4,4,2,32,128]{5,4,3,2,1,0:T(8,128)(2,1)} %broadcast_in_dim.14), calls=%async_computation.3 | async-start | bytes 2097152 | tf_op jit(solution)/shard_map/all_to_all | solution.py:417
  102.4 5.2 %shard_map.181 = (bf16[400,128]{1,0:T(8,128)(2,1)S(1)}, bf16[400,128]{1,0:T(8,128)(2,1)S(1)}, bf16[400,128]{1,0:T(8,128)(2,1)S(1)}) custom-call(s32[1]{0:T(128)} %bitcast.11.group_ref, f32[1]{0:T(128)S(6)} %copy.19.shift_ref, bf16[4,912,128]{2,1,0:T(8,128)(2,1)S(1)} %bitcast.16, bf16[4,320,128]{2,1,0:T(8,128)(2,1)S(1)} %bitcast.20), custom_call_target="tpu_custom_call" | custom-call | tf_op jit(solution)/shard_map/pallas_call | solution.py:424
  107.6 2.4 %collective-permute-start = (bf16[400,128]{1,0:T(8,128)(2,1)S(1)}, bf16[400,128]{1,0:T(8,128)(2,1)S(1)}, u32[]{:S(2)}, u32[]{:S(2)}) collective-permute-start(bf16[400,128]{1,0:T(8,128)(2,1)S(1)} %get-tuple-element.35), channel_id=1, source_target_pairs={{0,128},{32,160},{64,192},{96,224},{128,256},{160,288},{192,320},{... | collective-permute-start | bytes 307208 | tf_op jit(solution)/shard_map/ppermute | solution.py:433
  110.0 3.6 %collective-permute-start.1 = (bf16[400,128]{1,0:T(8,128)(2,1)S(1)}, bf16[400,128]{1,0:T(8,128)(2,1)S(1)}, u32[]{:S(2)}, u32[]{:S(2)}) collective-permute-start(bf16[400,128]{1,0:T(8,128)(2,1)S(1)} %get-tuple-element.36), channel_id=1, source_target_pairs={{0,256},{32,288},{64,320},{96,352},{128,384},{160,416},{192,448},{... | collective-permute-start | bytes 307208 | tf_op jit(solution)/shard_map/ppermute | solution.py:433
  113.6 1.3 collective-permute-start.2
  115.0 1.7 %shard_map.180 = (f32[256,128]{1,0:T(8,128)S(1)}, f32[256,128]{1,0:T(8,128)S(1)}) custom-call(s32[1]{0:T(128)} %bitcast.place_ref, f32[1]{0:T(128)S(6)} %copy.19.shift_ref, bf16[320,128]{1,0:T(8,128)(2,1)S(1)} %get-tuple-element.26.query_ref, bf16[4,912,128]{2,1,0:T(8,128)(2,1)S(1)} %bitcast.17), custom_call_target="tpu_custom_call" | custom-call | tf_op jit(solution)/shard_map/pallas_call | solution.py:435
  116.6 0.0 collective-permute-done.refs_0_
  116.6 0.0 collective-permute-done.1.refs_1_
  116.6 4.9 %collective-permute-done.2.refs_2_ = bf16[400,128]{1,0:T(8,128)(2,1)S(1)} collective-permute-done((bf16[400,128]{1,0:T(8,128)(2,1)S(1)}, bf16[400,128]{1,0:T(8,128)(2,1)S(1)}, u32[]{:S(2)}, u32[]{:S(2)}) %collective-permute-start.2) | collective-permute-done | bytes 102432 | tf_op jit(solution)/shard_map/ppermute | solution.py:433
  121.5 0.0 all-to-all-done.3.weight_ref
  121.5 0.0 copy-start.4
  121.5 0.0 copy-start.5
  121.5 0.7 copy-done.4
  122.2 0.0 copy-done.5
  122.2 1.8 %shard_map.182 = (bf16[256,2048]{1,0:T(8,128)(2,1)S(1)}, f32[1,256]{1,0:T(1,128)}) custom-call(s32[1]{0:T(128)} %bitcast.place_ref, bf16[4,912,128]{2,1,0:T(8,128)(2,1)S(1)} %bitcast.18, f32[256,128]{1,0:T(8,128)S(1)} %get-tuple-element.30.weighted_ref, f32[256,128]{1,0:T(8,128)S(1)} %get-tuple-element.31.spent_ref, ...), custom_call_target="tpu_custom_call" | custom-call | tf_op jit(solution)/shard_map/pallas_call | solution.py:438
  124.0 34.8 %all_to_all.26 = bf16[8,32,2048]{2,1,0:T(8,128)(2,1)S(1)} all-to-all(bf16[8,32,2048]{2,1,0:T(8,128)(2,1)S(1)} %bitcast.21), channel_id=1, replica_groups=mesh['sp'=16,'fs'=4,'tp'=8] {'tp'}, dimensions={0} | all-to-all | bytes 2097152 | tf_op jit(solution)/shard_map/all_to_all | solution.py:456
  158.8 0.8 reduce_sum.12
  (1 shorter events, 0.0 us)
Async XLA Ops:
  4.0 5.2 %copy-start.6 = (bf16[32,896]{1,0:T(8,128)(2,1)S(1)}, bf16[32,896]{1,0:T(8,128)(2,1)}, u32[]{:S(2)}) copy-start(bf16[32,896]{1,0:T(8,128)(2,1)} %get-tuple-element.22) | copy-start | bytes 172036
  4.0 39.2 %all-to-all-start = ((bf16[4,256,512]{2,1,0:T(8,128)(2,1)}), bf16[4,256,512]{2,1,0:T(8,128)(2,1)S(1)}, u32[]{:S(2)}, u32[]{:S(2)}) async-start(bf16[4,256,512]{2,1,0:T(8,128)(2,1)} %get-tuple-element.21), calls=%async_computation | async-start | bytes 2097152 | tf_op jit(solution)/shard_map/all_to_all | solution.py:380
  45.4 13.0 %copy-start.1 = (bf16[64,128]{1,0:T(8,128)(2,1)S(1)}, bf16[64,128]{1,0:T(8,128)(2,1)}, u32[]{:S(2)}) copy-start(bf16[64,128]{1,0:T(8,128)(2,1)} %get-tuple-element.25.own_ref) | copy-start | bytes 49156
  58.4 21.2 %all-to-all-start.2 = ((bf16[4,256,512]{2,1,0:T(8,128)(2,1)}), bf16[4,256,512]{2,1,0:T(8,128)(2,1)S(1)}, u32[]{:S(2)}, u32[]{:S(2)}) async-start(bf16[4,256,512]{2,1,0:T(8,128)(2,1)} %get-tuple-element.27), calls=%async_computation.2 | async-start | bytes 2097152 | tf_op jit(solution)/shard_map/all_to_all | solution.py:394
  62.0 17.7 %copy-start = (f32[1,256,128]{2,1,0:T(8,128)S(1)}, f32[1,256,128]{2,1,0:T(8,128)}, u32[]{:S(2)}) copy-start(f32[1,256,128]{2,1,0:T(8,128)} %param.33) | copy-start | bytes 393220
  79.6 0.7 copy-start.2
  79.6 0.7 copy-start.3
  98.1 23.5 %all-to-all-start.3 = ((bf16[4,4,4,2,32,128]{5,4,3,2,1,0:T(8,128)(2,1)}), bf16[4,4,4,2,32,128]{5,4,3,2,1,0:T(8,128)(2,1)S(1)}, u32[]{:S(2)}, u32[]{:S(2)}) async-start(bf16[4,4,4,2,32,128]{5,4,3,2,1,0:T(8,128)(2,1)} %broadcast_in_dim.14), calls=%async_computation.3 | async-start | bytes 2097152 | tf_op jit(solution)/shard_map/all_to_all | solution.py:417
  107.6 9.0 %collective-permute-start = (bf16[400,128]{1,0:T(8,128)(2,1)S(1)}, bf16[400,128]{1,0:T(8,128)(2,1)S(1)}, u32[]{:S(2)}, u32[]{:S(2)}) collective-permute-start(bf16[400,128]{1,0:T(8,128)(2,1)S(1)} %get-tuple-element.35), channel_id=1, source_target_pairs={{0,128},{32,160},{64,192},{96,224},{128,256},{160,288},{192,320},{... | collective-permute-start | bytes 307208 | tf_op jit(solution)/shard_map/ppermute | solution.py:433
  110.0 6.6 %collective-permute-start.1 = (bf16[400,128]{1,0:T(8,128)(2,1)S(1)}, bf16[400,128]{1,0:T(8,128)(2,1)S(1)}, u32[]{:S(2)}, u32[]{:S(2)}) collective-permute-start(bf16[400,128]{1,0:T(8,128)(2,1)S(1)} %get-tuple-element.36), channel_id=1, source_target_pairs={{0,256},{32,288},{64,320},{96,352},{128,384},{160,416},{192,448},{... | collective-permute-start | bytes 307208 | tf_op jit(solution)/shard_map/ppermute | solution.py:433
  113.6 7.9 %collective-permute-start.2 = (bf16[400,128]{1,0:T(8,128)(2,1)S(1)}, bf16[400,128]{1,0:T(8,128)(2,1)S(1)}, u32[]{:S(2)}, u32[]{:S(2)}) collective-permute-start(bf16[400,128]{1,0:T(8,128)(2,1)S(1)} %get-tuple-element.37), channel_id=1, source_target_pairs={{0,384},{32,416},{64,448},{96,480},{1,385},{33,417},{65,449},{97,4... | collective-permute-start | bytes 307208 | tf_op jit(solution)/shard_map/ppermute | solution.py:433
  121.5 0.7 copy-start.4
  121.5 0.7 copy-start.5

commit v2 on v1

--- a/solution.py
+++ b/solution.py
@@ -1,3 +1,5 @@
+import functools
+
 import jax
 import jax.numpy as jnp
 from jax import lax
@@ -61,7 +63,7 @@
         pltpu.make_async_copy(gain_hbm, gain_ref, arrived.at[1]),
     ]
     for k in range(7):
-        place = packed_ref.at[:, k * HEAD : (k + 1) * HEAD]
+        place = packed_ref.at[k * ROWS : (k + 1) * ROWS]
         copies.append(pltpu.make_async_copy(weights[k], place, arrived.at[2 + k]))
     for k in range(2):
         place = own_ref.at[k * ROWS : (k + 1) * ROWS]
@@ -86,13 +88,15 @@
             slices_ref[k, :, b * HEAD : (b + 1) * HEAD] = moved[:, k * HEAD : (k + 1) * HEAD]
 
 
-def partial_kernel(rows_ref, weight_ref, first_ref, second_ref):
-    cut = first_ref.shape[2]
-    weight = weight_ref[...]
+def partial_kernel(first, rows_ref, weight_ref, out_ref):
+    sp = weight_ref.shape[0]
+    pieces = [
+        weight_ref[:, k * ROWS : (k + 1) * ROWS].reshape(sp * ROWS, HEAD)
+        for k in range(first, first + out_ref.shape[2] // HEAD)
+    ]
+    weight = jnp.concatenate(pieces, axis=1)
     for k in range(rows_ref.shape[0]):
-        first_ref[k] = dot(rows_ref[k], weight[:, :cut]).astype(BF16)
-    for k in range(rows_ref.shape[0]):
-        second_ref[k] = dot(rows_ref[k], weight[:, cut:]).astype(BF16)
+        out_ref[k] = dot(rows_ref[k], weight).astype(BF16)
 
 
 def sum_of(products_ref):
@@ -226,35 +230,30 @@
     return jnp.concatenate(pieces, axis=0)
 
 
-def far_kernel(group_ref, shift_ref, message_ref, query_ref, *out_refs):
+def far_kernel(places, group_ref, shift_ref, message_ref, query_ref, out_ref):
     count = query_ref.shape[0]
-    length = message_ref.shape[1] - count * 2 * ROWS - HEAD - TILE
-    length = length // 2
-    shift = shift_ref[0]
     near = message_ref.shape[0]
-    index = lax.broadcasted_iota(jnp.int32, (TILE, HEAD), 0)
-    for j, out_ref in enumerate(out_refs):
-        wanted = group_ref[0] + j + 1 < count
-
-        @pl.when(wanted)
-        def _(j=j, out_ref=out_ref):
-            query = query_ref[group_ref[0] + j + 1, 0:length]
-            weighted, total = attend_near(query, message_ref, shift)
-            out_ref[0:length] = weighted.astype(BF16)
-            decay, state = chain(message_ref, 2 * length, near)
-            high, low = parts(as_row(total))
-            pieces = [
-                piece[:, k * HEAD : (k + 1) * HEAD] for piece in (high, low) for k in range(2)
-            ]
-            vector = jnp.zeros((TILE, HEAD), F32)
-            for k, piece in enumerate(pieces + [decay]):
-                vector = jnp.where(index == k, piece.astype(F32), vector)
-            out_ref[length : length + TILE] = vector.astype(BF16)
-            out_ref[length + TILE : length + TILE + HEAD] = state.astype(BF16)
-
-        @pl.when(jnp.logical_not(wanted))
-        def _(out_ref=out_ref):
-            out_ref[...] = jnp.zeros(out_ref.shape, BF16)
+    length = out_ref.shape[0] - TILE - HEAD
+    wanted = group_ref[0] + places < count
+
+    @pl.when(wanted)
+    def _():
+        query = query_ref[group_ref[0] + places, 0:length]
+        weighted, total = attend_near(query, message_ref, shift_ref[0])
+        out_ref[0:length] = weighted.astype(BF16)
+        decay, state = chain(message_ref, 2 * length, near)
+        high, low = parts(as_row(total))
+        pieces = [piece[:, k * HEAD : (k + 1) * HEAD] for piece in (high, low) for k in range(2)]
+        index = lax.broadcasted_iota(jnp.int32, (TILE, HEAD), 0)
+        vector = jnp.zeros((TILE, HEAD), F32)
+        for k, piece in enumerate(pieces + [decay]):
+            vector = jnp.where(index == k, piece.astype(F32), vector)
+        out_ref[length : length + TILE] = vector.astype(BF16)
+        out_ref[length + TILE : length + TILE + HEAD] = state.astype(BF16)
+
+    @pl.when(jnp.logical_not(wanted))
+    def _():
+        out_ref[...] = jnp.zeros(out_ref.shape, BF16)
 
 
 def near_kernel(place_ref, shift_ref, query_ref, message_ref, weighted_ref, total_ref):
@@ -353,7 +352,7 @@
         start_kernel,
         (
             shape((fs, tokens, width // fs), BF16),
-            shape((ROWS, 7 * HEAD), BF16),
+            shape((7 * ROWS, HEAD), BF16),
             shape((2 * ROWS, HEAD), BF16),
         ),
         11,
@@ -378,11 +377,12 @@
         emitted_projection_linear_scan,
     )
     rows = lax.all_to_all(slices, "fs", 0, 0, tiled=True)
-    column = lax.all_gather(packed, "sp", axis=0, tiled=True)
-    first, second = vmem_call(
-        partial_kernel,
-        tuple(shape((fs, tokens, columns * HEAD), BF16) for columns in (3, 4)),
-        2,
+    column = lax.all_gather(packed, "sp")
+    first = vmem_call(
+        functools.partial(partial_kernel, 0), shape((fs, tokens, 3 * HEAD), BF16), 2
+    )(rows, column)
+    second = vmem_call(
+        functools.partial(partial_kernel, 3), shape((fs, tokens, 4 * HEAD), BF16), 2
     )(rows, column)
     first = lax.all_to_all(first, "fs", 0, 0, tiled=True)
     own, key_value = vmem_call(
@@ -421,16 +421,16 @@
         0,
         tiled=True,
     )
-    far = vmem_call(
-        far_kernel,
-        tuple(shape((tokens + TILE + HEAD, HEAD), BF16) for _ in range(count - 1)),
-        4,
-        (0, 1),
-    )(group, score_offset, gathered, across)
     outside = []
     for j in range(1, count):
+        far = vmem_call(
+            functools.partial(far_kernel, j),
+            shape((tokens + TILE + HEAD, HEAD), BF16),
+            4,
+            (0, 1),
+        )(group, score_offset, gathered, across)
         places = [(k, k + NEAR * j) for k in range(sp - NEAR * j)]
-        outside.append(lax.ppermute(far[j - 1], "sp", places))
+        outside.append(lax.ppermute(far, "sp", places))
     place = (rank % NEAR).reshape(1)
     weighted, spent = vmem_call(near_kernel, (small, small), 4, (0, 1))(
         place, score_offset, own, gathered

time: 160 us -> 160 us (level)
  blocking collectives: 114 us -> 101 us
  waiting for transfers between devices: 4.91 us -> 11.5 us
  starting transfers between devices: 19.7 us -> 24.4 us
    all_to_all x1 -> x0, blocking collectives: 13 us -> none  [on_device(): first = lax.all_to_all(first, 'fs', 0, 0, tiled=True)]
    all_to_all x0 -> x1, waiting for transfers between devices: none -> 6.63 us  [on_device(): first = lax.all_to_all(first, 'fs', 0, 0, tiled=True)]
    all_to_all x0 -> x1, starting transfers between devices: none -> 4.7 us  [on_device(): first = lax.all_to_all(first, 'fs', 0, 0, tiled=True)]
    pallas_call x3 -> x6, Pallas kernels: 10.7 us -> 11.8 us  [the longest x3 5.14 us: on_device(): vmem_call(functools.partial(far_kernel, j), shape((tokens + TILE + HEAD,...]
  transfers between devices with their start and end apart: 6 -> 7, of which waited for: 1 -> 2; matrix products, arithmetic and copies ran while one was open for 0% -> 0% of each run, Pallas kernels for 4% -> 5%
where the time goes in v2:
time: 160 us; the launch traced here: 159 us
  blocking collectives  101 us (63%)
  starting transfers between devices  24.4 us (15%)
  Pallas kernels  17.5 us (11%)
  waiting for transfers between devices  11.5 us (7%)
  local copies, waits for them, and re-layouts  2.61 us (2%)
    all_to_all x1, blocking collectives, on_device(): lax.all_to_all(projected.reshape(tp, tokens // tp, width), 'tp', 0, 0, ti...  34.8 us
    all_gather x1, blocking collectives, on_device(): column = lax.all_gather(packed, 'sp')  34 us
    all_gather x1, blocking collectives, on_device(): across = lax.all_gather(own, 'sp', axis_index_groups=strided)  17.7 us
    all_gather x1, blocking collectives, on_device(): gathered = lax.all_gather(message, 'sp', axis_index_groups=groups)  14.3 us
    ppermute x3, starting transfers between devices, on_device(): outside.append(lax.ppermute(far, 'sp', places))  7.26 us
    all_to_all x1, waiting for transfers between devices, on_device(): first = lax.all_to_all(first, 'fs', 0, 0, tiled=True)  6.63 us
    all_to_all x1, starting transfers between devices, on_device(): rows = lax.all_to_all(slices, 'fs', 0, 0, tiled=True)  5.15 us
    pallas_call x3, Pallas kernels, on_device(): vmem_call(functools.partial(far_kernel, j), shape((tokens + TILE + HEAD,...  5.14 us
  transfers between devices with their start and end apart: 7, of which 2 were waited for; matrix products, arithmetic and copies ran while one was open for 0% of the time, Pallas kernels for 5%

profile of v2, /device:TPU:1, one launch (start us, length us, event | category | flops | bytes accessed | tf_op | source)
XLA Modules:
  0.0 159.1 jit_solution(534262421702853167)
XLA Ops:
  0.6 3.3 %shard_map.176 = (bf16[4,256,512]{2,1,0:T(8,128)(2,1)}, bf16[224,128]{1,0:T(8,128)(2,1)}, bf16[64,128]{1,0:T(8,128)(2,1)}) custom-call(bf16[256,2048]{1,0:T(8,128)(2,1)} %bitcast.35, f32[1,2048]{1,0:T(1,128)} %bitcast.37, bf16[32,128]{1,0:T(8,128)(2,1)} %refs_0_.1, bf16[32,128]{1,0:T(8,128)(2,1)} %refs_1_.1, bf16[32,128]{1,0:T(8,128)(2,1)} %refs_2_.1, ...), custom_call_target="tpu_custom_call" | custom-call | tf_op jit(solution)/shard_map/pallas_call | solution.py:351
  4.0 0.0 copy-start.6
  4.0 5.2 %all-to-all-start = ((bf16[4,256,512]{2,1,0:T(8,128)(2,1)}), bf16[4,256,512]{2,1,0:T(8,128)(2,1)S(1)}, u32[]{:S(2)}, u32[]{:S(2)}) async-start(bf16[4,256,512]{2,1,0:T(8,128)(2,1)} %get-tuple-element.16), calls=%async_computation | async-start | bytes 2097152 | tf_op jit(solution)/shard_map/all_to_all | solution.py:379
  9.1 0.0 copy-done.6
  9.1 34.0 %all-gather = bf16[3584,128]{1,0:T(8,128)(2,1)S(1)} all-gather(bf16[224,128]{1,0:T(8,128)(2,1)S(1)} %copy-done.6), channel_id=2, replica_groups=mesh['sp'=16,'fs'=4,'tp'=8] {'sp'}, dimensions={0}, use_global_device_ids=true | all-gather | bytes 974848 | tf_op jit(solution)/shard_map/all_gather | solution.py:380
  43.1 0.0 all-to-all-done.rows_ref
  43.1 1.6 %shard_map.178 = bf16[4,256,384]{2,1,0:T(8,128)(2,1)} custom-call(bf16[4,256,512]{2,1,0:T(8,128)(2,1)S(1)} %all-to-all-done.rows_ref, bf16[16,224,128]{2,1,0:T(8,128)(2,1)S(1)} %bitcast.22), custom_call_target="tpu_custom_call" | custom-call | tf_op jit(solution)/shard_map/pallas_call | solution.py:381
  44.7 4.7 %all-to-all-start.1 = ((bf16[4,256,384]{2,1,0:T(8,128)(2,1)}), bf16[4,256,384]{2,1,0:T(8,128)(2,1)S(1)}, u32[]{:S(2)}, u32[]{:S(2)}) async-start(bf16[4,256,384]{2,1,0:T(8,128)(2,1)} %shard_map.178), calls=%async_computation.1 | async-start | bytes 1572864 | tf_op jit(solution)/shard_map/all_to_all | solution.py:387
  49.4 0.0 copy-start.1
  49.4 1.7 %shard_map.177 = bf16[4,256,512]{2,1,0:T(8,128)(2,1)} custom-call(bf16[4,256,512]{2,1,0:T(8,128)(2,1)S(1)} %all-to-all-done.rows_ref, bf16[16,224,128]{2,1,0:T(8,128)(2,1)S(1)} %bitcast.23), custom_call_target="tpu_custom_call" | custom-call | tf_op jit(solution)/shard_map/pallas_call | solution.py:384
  51.1 6.6 %all-to-all-done.1.products_ref = bf16[4,256,384]{2,1,0:T(8,128)(2,1)S(1)} async-done(((bf16[4,256,384]{2,1,0:T(8,128)(2,1)}), bf16[4,256,384]{2,1,0:T(8,128)(2,1)S(1)}, u32[]{:S(2)}, u32[]{:S(2)}) %all-to-all-start.1) | async-done | bytes 786464 | tf_op jit(solution)/shard_map/all_to_all | solution.py:387
  57.8 0.0 copy-done.1
  57.8 0.1 shard_map.179
  57.9 3.5 %all-to-all-start.2 = ((bf16[4,256,512]{2,1,0:T(8,128)(2,1)}), bf16[4,256,512]{2,1,0:T(8,128)(2,1)S(1)}, u32[]{:S(2)}, u32[]{:S(2)}) async-start(bf16[4,256,512]{2,1,0:T(8,128)(2,1)} %shard_map.177), calls=%async_computation.2 | async-start | bytes 2097152 | tf_op jit(solution)/shard_map/all_to_all | solution.py:394
  61.4 0.0 copy-start
  61.4 17.7 %all-gather.1 = bf16[1280,128]{1,0:T(8,128)(2,1)S(1)} all-gather(bf16[320,128]{1,0:T(8,128)(2,1)S(1)} %get-tuple-element.19.query_ref), channel_id=3, replica_groups={{0,128,256,384},{32,160,288,416},{64,192,320,448},{96,224,352,480},{1,1..., dimensions={0}, use_global_device_ids=true | all-gather | bytes 409600 | tf_op jit(solution)/shard_map/all_gather | solution.py:396
  79.1 0.0 all-to-all-done.2.refs_0_
  79.1 0.0 copy-start.2
  79.1 0.0 copy-start.3
  79.1 0.0 copy-done
  79.1 0.6 copy-done.2
  79.7 0.0 copy-done.3
  79.7 2.1 %shard_map.180 = (bf16[912,128]{1,0:T(8,128)(2,1)S(1)}, f32[256,128]{1,0:T(8,128)S(1)}, f32[256,128]{1,0:T(8,128)S(1)}, f32[256,128]{1,0:T(8,128)S(1)}) custom-call(bf16[4,256,512]{2,1,0:T(8,128)(2,1)S(1)} %all-to-all-done.2.refs_0_, f32[1,128]{1,0:T(1,128)S(1)} %bitcast.30, f32[1,128]{1,0:T(1,128)S(1)} %bitcast.31, f32[256,128]{1,0:T(8,128)S(1)} %bitcast.29, ...), custom_call_target="tpu_custom_call" | custom-call | tf_op jit(solution)/shard_map/pallas_call | solution.py:400
  81.9 14.3 %all-gather.2 = bf16[3648,128]{1,0:T(8,128)(2,1)S(1)} all-gather(bf16[912,128]{1,0:T(8,128)(2,1)S(1)} %get-tuple-element.22), channel_id=4, replica_groups={{0,32,64,96},{128,160,192,224},{256,288,320,352},{384,416,448,480},{1,3..., dimensions={0}, use_global_device_ids=true | all-gather | bytes 1167360 | tf_op jit(solution)/shard_map/all_gather | solution.py:416
  96.3 1.2 broadcast_in_dim.14
  97.5 3.8 %all-to-all-start.3 = ((bf16[4,4,4,2,32,128]{5,4,3,2,1,0:T(8,128)(2,1)}), bf16[4,4,4,2,32,128]{5,4,3,2,1,0:T(8,128)(2,1)S(1)}, u32[]{:S(2)}, u32[]{:S(2)}) async-start(bf16[4,4,4,2,32,128]{5,4,3,2,1,0:T(8,128)(2,1)} %broadcast_in_dim.14), calls=%async_computation.3 | async-start | bytes 2097152 | tf_op jit(solution)/shard_map/all_to_all | solution.py:417
  102.0 1.7 %shard_map.184 = bf16[400,128]{1,0:T(8,128)(2,1)S(1)} custom-call(s32[1]{0:T(128)} %bitcast.12.group_ref, f32[1]{0:T(128)S(6)} %copy.19.shift_ref, bf16[4,912,128]{2,1,0:T(8,128)(2,1)S(1)} %bitcast.17, bf16[4,320,128]{2,1,0:T(8,128)(2,1)S(1)} %bitcast.25), custom_call_target="tpu_custom_call" | custom-call | tf_op jit(solution)/shard_map/pallas_call | solution.py:426
  103.7 1.7 %shard_map.183 = bf16[400,128]{1,0:T(8,128)(2,1)S(1)} custom-call(s32[1]{0:T(128)} %bitcast.12.group_ref, f32[1]{0:T(128)S(6)} %copy.19.shift_ref, bf16[4,912,128]{2,1,0:T(8,128)(2,1)S(1)} %bitcast.18, bf16[4,320,128]{2,1,0:T(8,128)(2,1)S(1)} %bitcast.26), custom_call_target="tpu_custom_call" | custom-call | tf_op jit(solution)/shard_map/pallas_call | solution.py:426
  105.4 1.7 %shard_map.182 = bf16[400,128]{1,0:T(8,128)(2,1)S(1)} custom-call(s32[1]{0:T(128)} %bitcast.12.group_ref, f32[1]{0:T(128)S(6)} %copy.19.shift_ref, bf16[4,912,128]{2,1,0:T(8,128)(2,1)S(1)} %bitcast.19, bf16[4,320,128]{2,1,0:T(8,128)(2,1)S(1)} %bitcast.27), custom_call_target="tpu_custom_call" | custom-call | tf_op jit(solution)/shard_map/pallas_call | solution.py:426
  107.1 2.3 %collective-permute-start = (bf16[400,128]{1,0:T(8,128)(2,1)S(1)}, bf16[400,128]{1,0:T(8,128)(2,1)S(1)}, u32[]{:S(2)}, u32[]{:S(2)}) collective-permute-start(bf16[400,128]{1,0:T(8,128)(2,1)S(1)} %shard_map.182), channel_id=1, source_target_pairs={{0,128},{32,160},{64,192},{96,224},{128,256},{160,288},{192,320},{... | collective-permute-start | bytes 307208 | tf_op jit(solution)/shard_map/ppermute | solution.py:433
  109.5 3.6 %collective-permute-start.1 = (bf16[400,128]{1,0:T(8,128)(2,1)S(1)}, bf16[400,128]{1,0:T(8,128)(2,1)S(1)}, u32[]{:S(2)}, u32[]{:S(2)}) collective-permute-start(bf16[400,128]{1,0:T(8,128)(2,1)S(1)} %shard_map.183), channel_id=1, source_target_pairs={{0,256},{32,288},{64,320},{96,352},{128,384},{160,416},{192,448},{... | collective-permute-start | bytes 307208 | tf_op jit(solution)/shard_map/ppermute | solution.py:433
  113.1 1.3 collective-permute-start.2
  114.4 1.7 %shard_map.181 = (f32[256,128]{1,0:T(8,128)S(1)}, f32[256,128]{1,0:T(8,128)S(1)}) custom-call(s32[1]{0:T(128)} %bitcast.place_ref, f32[1]{0:T(128)S(6)} %copy.19.shift_ref, bf16[320,128]{1,0:T(8,128)(2,1)S(1)} %get-tuple-element.19.query_ref, bf16[4,912,128]{2,1,0:T(8,128)(2,1)S(1)} %bitcast.20), custom_call_target="tpu_custom_call" | custom-call | tf_op jit(solution)/shard_map/pallas_call | solution.py:435
  116.1 0.0 collective-permute-done.refs_0_
  116.1 0.0 collective-permute-done.1.refs_1_
  116.1 4.9 %collective-permute-done.2.refs_2_ = bf16[400,128]{1,0:T(8,128)(2,1)S(1)} collective-permute-done((bf16[400,128]{1,0:T(8,128)(2,1)S(1)}, bf16[400,128]{1,0:T(8,128)(2,1)S(1)}, u32[]{:S(2)}, u32[]{:S(2)}) %collective-permute-start.2) | collective-permute-done | bytes 102432 | tf_op jit(solution)/shard_map/ppermute | solution.py:433
  121.0 0.0 all-to-all-done.3.weight_ref
  121.0 0.0 copy-start.4
  121.0 0.0 copy-start.5
  121.0 0.7 copy-done.4
  121.7 0.0 copy-done.5
  121.7 1.8 %shard_map.185 = (bf16[256,2048]{1,0:T(8,128)(2,1)S(1)}, f32[1,256]{1,0:T(1,128)}) custom-call(s32[1]{0:T(128)} %bitcast.place_ref, bf16[4,912,128]{2,1,0:T(8,128)(2,1)S(1)} %bitcast.21, f32[256,128]{1,0:T(8,128)S(1)} %get-tuple-element.23.weighted_ref, f32[256,128]{1,0:T(8,128)S(1)} %get-tuple-element.24.spent_ref, ...), custom_call_target="tpu_custom_call" | custom-call | tf_op jit(solution)/shard_map/pallas_call | solution.py:438
  123.5 34.8 %all_to_all.25 = bf16[8,32,2048]{2,1,0:T(8,128)(2,1)S(1)} all-to-all(bf16[8,32,2048]{2,1,0:T(8,128)(2,1)S(1)} %bitcast.28), channel_id=1, replica_groups=mesh['sp'=16,'fs'=4,'tp'=8] {'tp'}, dimensions={0} | all-to-all | bytes 2097152 | tf_op jit(solution)/shard_map/all_to_all | solution.py:456
  158.3 0.8 reduce_sum.12
  (1 shorter events, 0.0 us)
Async XLA Ops:
  4.0 5.2 %copy-start.6 = (bf16[224,128]{1,0:T(8,128)(2,1)S(1)}, bf16[224,128]{1,0:T(8,128)(2,1)}, u32[]{:S(2)}) copy-start(bf16[224,128]{1,0:T(8,128)(2,1)} %get-tuple-element.17) | copy-start | bytes 172036
  4.0 39.2 %all-to-all-start = ((bf16[4,256,512]{2,1,0:T(8,128)(2,1)}), bf16[4,256,512]{2,1,0:T(8,128)(2,1)S(1)}, u32[]{:S(2)}, u32[]{:S(2)}) async-start(bf16[4,256,512]{2,1,0:T(8,128)(2,1)} %get-tuple-element.16), calls=%async_computation | async-start | bytes 2097152 | tf_op jit(solution)/shard_map/all_to_all | solution.py:379
  44.7 13.0 %all-to-all-start.1 = ((bf16[4,256,384]{2,1,0:T(8,128)(2,1)}), bf16[4,256,384]{2,1,0:T(8,128)(2,1)S(1)}, u32[]{:S(2)}, u32[]{:S(2)}) async-start(bf16[4,256,384]{2,1,0:T(8,128)(2,1)} %shard_map.178), calls=%async_computation.1 | async-start | bytes 1572864 | tf_op jit(solution)/shard_map/all_to_all | solution.py:387
  49.4 8.3 %copy-start.1 = (bf16[64,128]{1,0:T(8,128)(2,1)S(1)}, bf16[64,128]{1,0:T(8,128)(2,1)}, u32[]{:S(2)}) copy-start(bf16[64,128]{1,0:T(8,128)(2,1)} %get-tuple-element.18.own_ref) | copy-start | bytes 49156
  57.9 21.2 %all-to-all-start.2 = ((bf16[4,256,512]{2,1,0:T(8,128)(2,1)}), bf16[4,256,512]{2,1,0:T(8,128)(2,1)S(1)}, u32[]{:S(2)}, u32[]{:S(2)}) async-start(bf16[4,256,512]{2,1,0:T(8,128)(2,1)} %shard_map.177), calls=%async_computation.2 | async-start | bytes 2097152 | tf_op jit(solution)/shard_map/all_to_all | solution.py:394
  61.4 17.7 %copy-start = (f32[1,256,128]{2,1,0:T(8,128)S(1)}, f32[1,256,128]{2,1,0:T(8,128)}, u32[]{:S(2)}) copy-start(f32[1,256,128]{2,1,0:T(8,128)} %param.33) | copy-start | bytes 393220
  79.1 0.7 copy-start.2
  79.1 0.7 copy-start.3
  97.5 23.5 %all-to-all-start.3 = ((bf16[4,4,4,2,32,128]{5,4,3,2,1,0:T(8,128)(2,1)}), bf16[4,4,4,2,32,128]{5,4,3,2,1,0:T(8,128)(2,1)S(1)}, u32[]{:S(2)}, u32[]{:S(2)}) async-start(bf16[4,4,4,2,32,128]{5,4,3,2,1,0:T(8,128)(2,1)} %broadcast_in_dim.14), calls=%async_computation.3 | async-start | bytes 2097152 | tf_op jit(solution)/shard_map/all_to_all | solution.py:417
  107.1 9.0 %collective-permute-start = (bf16[400,128]{1,0:T(8,128)(2,1)S(1)}, bf16[400,128]{1,0:T(8,128)(2,1)S(1)}, u32[]{:S(2)}, u32[]{:S(2)}) collective-permute-start(bf16[400,128]{1,0:T(8,128)(2,1)S(1)} %shard_map.182), channel_id=1, source_target_pairs={{0,128},{32,160},{64,192},{96,224},{128,256},{160,288},{192,320},{... | collective-permute-start | bytes 307208 | tf_op jit(solution)/shard_map/ppermute | solution.py:433
  109.5 6.6 %collective-permute-start.1 = (bf16[400,128]{1,0:T(8,128)(2,1)S(1)}, bf16[400,128]{1,0:T(8,128)(2,1)S(1)}, u32[]{:S(2)}, u32[]{:S(2)}) collective-permute-start(bf16[400,128]{1,0:T(8,128)(2,1)S(1)} %shard_map.183), channel_id=1, source_target_pairs={{0,256},{32,288},{64,320},{96,352},{128,384},{160,416},{192,448},{... | collective-permute-start | bytes 307208 | tf_op jit(solution)/shard_map/ppermute | solution.py:433
  113.1 7.9 %collective-permute-start.2 = (bf16[400,128]{1,0:T(8,128)(2,1)S(1)}, bf16[400,128]{1,0:T(8,128)(2,1)S(1)}, u32[]{:S(2)}, u32[]{:S(2)}) collective-permute-start(bf16[400,128]{1,0:T(8,128)(2,1)S(1)} %shard_map.184), channel_id=1, source_target_pairs={{0,384},{32,416},{64,448},{96,480},{1,385},{33,417},{65,449},{97,4... | collective-permute-start | bytes 307208 | tf_op jit(solution)/shard_map/ppermute | solution.py:433
  121.0 0.7 copy-start.4
  121.0 0.7 copy-start.5

commit v3 on v1

--- a/solution.py
+++ b/solution.py
@@ -1,3 +1,5 @@
+import functools
+
 import jax
 import jax.numpy as jnp
 from jax import lax
@@ -61,7 +63,7 @@
         pltpu.make_async_copy(gain_hbm, gain_ref, arrived.at[1]),
     ]
     for k in range(7):
-        place = packed_ref.at[:, k * HEAD : (k + 1) * HEAD]
+        place = packed_ref.at[k * ROWS : (k + 1) * ROWS]
         copies.append(pltpu.make_async_copy(weights[k], place, arrived.at[2 + k]))
     for k in range(2):
         place = own_ref.at[k * ROWS : (k + 1) * ROWS]
@@ -86,13 +88,19 @@
             slices_ref[k, :, b * HEAD : (b + 1) * HEAD] = moved[:, k * HEAD : (k + 1) * HEAD]
 
 
-def partial_kernel(rows_ref, weight_ref, first_ref, second_ref):
-    cut = first_ref.shape[2]
-    weight = weight_ref[...]
+def partial_kernel(first, rows_ref, weight_ref, *refs):
+    vectors = refs[: (len(refs) - 1) // 2]
+    out_ref = refs[len(vectors)]
+    for k, ref in enumerate(refs[len(vectors) + 1 :]):
+        ref[...] = vectors[k][...]
+    sp = weight_ref.shape[0]
+    pieces = [
+        weight_ref[:, k * ROWS : (k + 1) * ROWS].reshape(sp * ROWS, HEAD)
+        for k in range(first, first + out_ref.shape[2] // HEAD)
+    ]
+    weight = jnp.concatenate(pieces, axis=1)
     for k in range(rows_ref.shape[0]):
-        first_ref[k] = dot(rows_ref[k], weight[:, :cut]).astype(BF16)
-    for k in range(rows_ref.shape[0]):
-        second_ref[k] = dot(rows_ref[k], weight[:, cut:]).astype(BF16)
+        out_ref[k] = dot(rows_ref[k], weight).astype(BF16)
 
 
 def sum_of(products_ref):
@@ -102,28 +110,25 @@
     return total.astype(BF16)
 
 
-def attention_inputs_kernel(products_ref, own_ref, far_ref, key_value_ref):
-    total = sum_of(products_ref)
-    length = total.shape[0]
-    key_value_ref[0:length] = total[:, 0:HEAD]
-    key_value_ref[length : 2 * length] = total[:, HEAD : 2 * HEAD]
-    far_ref[0:length] = total[:, 2 * HEAD :]
+def attention_inputs_kernel(products_ref, own_ref, far_ref):
+    length = products_ref.shape[1]
+    far_ref[0:length] = sum_of(products_ref)
     far_ref[length : length + 2 * ROWS] = own_ref[...]
 
 
 def local_recurrence_kernel(*refs):
-    products_ref, floor_ref, offset_ref, extra_hbm, key_value_ref, slots_ref = refs[:6]
-    message_ref, inner_ref, query_decayed_ref, gate_ref, extra_ref, arrived = refs[6:]
+    products_ref, floor_ref, offset_ref, extra_hbm, slots_ref = refs[:5]
+    message_ref, inner_ref, query_decayed_ref, gate_ref, extra_ref, arrived = refs[5:]
     copy = pltpu.make_async_copy(extra_hbm, extra_ref, arrived)
     copy.start()
     total = sum_of(products_ref)
-    columns = [total[:, k * HEAD : (k + 1) * HEAD] for k in range(4)]
-    query_b = columns[0].astype(F32)
+    columns = [total[:, k * HEAD : (k + 1) * HEAD] for k in range(6)]
+    query_b = columns[2].astype(F32)
     query = query_b / (1.0 + jnp.exp(-query_b))
-    value = columns[2]
-    gate_b = columns[3].astype(F32)
+    value = columns[4]
+    gate_b = columns[5].astype(F32)
     gate_ref[...] = gate_b / (1.0 + jnp.exp(-gate_b))
-    u = columns[1].astype(F32) + offset_ref[...]
+    u = columns[3].astype(F32) + offset_ref[...]
     key = (1.0 - floor_ref[...]) / (1.0 + jnp.exp(u))
     copy.wait()
     log_forget = jnp.log(1.0 - key) + extra_ref[...]
@@ -167,7 +172,7 @@
     state = dot(value, key_high, ((0,), (0,))) + dot(value, key_low, ((0,), (0,)))
     at = 0
     vector = jnp.broadcast_to(jnp.exp(final), (TILE, HEAD)).astype(BF16)
-    for piece in (key_value_ref[...], state.astype(BF16), vector):
+    for piece in (columns[0], columns[1], state.astype(BF16), vector):
         message_ref[at : at + piece.shape[0]] = piece
         at += piece.shape[0]
     for k in range(slots_ref.shape[0]):
@@ -353,7 +358,7 @@
         start_kernel,
         (
             shape((fs, tokens, width // fs), BF16),
-            shape((ROWS, 7 * HEAD), BF16),
+            shape((7 * ROWS, HEAD), BF16),
             shape((2 * ROWS, HEAD), BF16),
         ),
         11,
@@ -367,9 +372,9 @@
     )(
         x,
         input_norm_gain.reshape(1, width),
+        query_weight_attention,
         key_weight_attention,
         value_weight_attention,
-        query_weight_attention,
         query_weight_recurrent,
         forget_weight_recurrent,
         value_weight_recurrent,
@@ -378,18 +383,27 @@
         emitted_projection_linear_scan,
     )
     rows = lax.all_to_all(slices, "fs", 0, 0, tiled=True)
-    column = lax.all_gather(packed, "sp", axis=0, tiled=True)
-    first, second = vmem_call(
-        partial_kernel,
-        tuple(shape((fs, tokens, columns * HEAD), BF16) for columns in (3, 4)),
-        2,
+    column = lax.all_gather(packed, "sp")
+    first = vmem_call(
+        functools.partial(partial_kernel, 0), shape((fs, tokens, HEAD), BF16), 2
     )(rows, column)
+    vector = shape((1, HEAD), F32)
+    second, floor, offset, gain_a, gain_b = vmem_call(
+        functools.partial(partial_kernel, 1),
+        (shape((fs, tokens, 6 * HEAD), BF16), vector, vector, vector, vector),
+        6,
+    )(
+        rows,
+        column,
+        forget_floor.reshape(1, HEAD),
+        forget_offset.reshape(1, HEAD),
+        attention_norm_gain.reshape(1, HEAD),
+        recurrence_norm_gain.reshape(1, HEAD),
+    )
     first = lax.all_to_all(first, "fs", 0, 0, tiled=True)
-    own, key_value = vmem_call(
-        attention_inputs_kernel,
-        (shape((tokens + 2 * ROWS, HEAD), BF16), shape((2 * tokens, HEAD), BF16)),
-        2,
-    )(first, out_own)
+    own = vmem_call(attention_inputs_kernel, shape((tokens + 2 * ROWS, HEAD), BF16), 2)(
+        first, out_own
+    )
     second, _ = lax.optimization_barrier((second, own))
     second = lax.all_to_all(second, "fs", 0, 0, tiled=True)
     strided = [list(range(k, sp, NEAR)) for k in range(NEAR)]
@@ -400,16 +414,15 @@
     message, inner, query_decayed, gate = vmem_call(
         local_recurrence_kernel,
         (shape((start + count * 2 * ROWS, HEAD), BF16), small, small, small),
-        6,
+        5,
         (),
         (3,),
         (pltpu.VMEM((tokens, HEAD), F32), pltpu.SemaphoreType.DMA(())),
     )(
         second,
-        forget_floor.reshape(1, HEAD),
-        forget_offset.reshape(1, HEAD),
+        floor,
+        offset,
         extra_log_decay[0],
-        key_value,
         across,
     )
     groups = [list(range(NEAR * k, NEAR * (k + 1))) for k in range(count)]
@@ -448,8 +461,8 @@
         inner,
         query_decayed,
         gate,
-        attention_norm_gain.reshape(1, HEAD),
-        recurrence_norm_gain.reshape(1, HEAD),
+        gain_a,
+        gain_b,
         out_weights,
         *outside,
     )

time: 160 us -> 156 us (0.975)
  blocking collectives: 114 us -> 102 us
  starting transfers between devices: 19.7 us -> 24 us
  waiting for transfers between devices: 4.91 us -> 8.19 us
    all_to_all x1 -> x0, blocking collectives: 13 us -> none  [on_device(): first = lax.all_to_all(first, 'fs', 0, 0, tiled=True)]
    all_to_all x0 -> x1, starting transfers between devices: none -> 4.83 us  [on_device(): first = lax.all_to_all(first, 'fs', 0, 0, tiled=True)]
    all_to_all x0 -> x1, waiting for transfers between devices: none -> 3.35 us  [on_device(): first = lax.all_to_all(first, 'fs', 0, 0, tiled=True)]
    pallas_call x3 -> x4, Pallas kernels: 5.65 us -> 6.62 us  [the longest x1 3.31 us: on_device(): vmem_call(start_kernel, (shape((fs, tokens, width // fs), BF16), shape((7...]
  transfers between devices with their start and end apart: 6 -> 7, of which waited for: 1 -> 2; matrix products, arithmetic and copies ran while one was open for 0% -> 0% of each run, Pallas kernels for 4% -> 6%
where the time goes in v3:
time: 156 us; the launch traced here: 155 us
  blocking collectives  102 us (65%)
  starting transfers between devices  24 us (15%)
  Pallas kernels  17.6 us (11%)
  waiting for transfers between devices  8.19 us (5%)
    all_to_all x1, blocking collectives, on_device(): lax.all_to_all(projected.reshape(tp, tokens // tp, width), 'tp', 0, 0, ti...  35 us
    all_gather x1, blocking collectives, on_device(): column = lax.all_gather(packed, 'sp')  34 us
    all_gather x1, blocking collectives, on_device(): across = lax.all_gather(own, 'sp', axis_index_groups=strided)  18.5 us
    all_gather x1, blocking collectives, on_device(): gathered = lax.all_gather(message, 'sp', axis_index_groups=groups)  14.3 us
    ppermute x3, starting transfers between devices, on_device(): outside.append(lax.ppermute(far[j - 1], 'sp', places))  6.82 us
    pallas_call x1, Pallas kernels, on_device(): vmem_call(far_kernel, tuple((shape((tokens + TILE + HEAD, HEAD), BF16) fo...  5.16 us
    all_to_all x1, starting transfers between devices, on_device(): rows = lax.all_to_all(slices, 'fs', 0, 0, tiled=True)  5.15 us
    ppermute x3, waiting for transfers between devices, on_device(): outside.append(lax.ppermute(far[j - 1], 'sp', places))  4.84 us
  transfers between devices with their start and end apart: 7, of which 2 were waited for; matrix products, arithmetic and copies ran while one was open for 0% of the time, Pallas kernels for 6%

profile of v3, /device:TPU:1, one launch (start us, length us, event | category | flops | bytes accessed | tf_op | source)
XLA Modules:
  0.0 155.2 jit_solution(6285015388858301150)
XLA Ops:
  0.6 3.3 %shard_map.176 = (bf16[4,256,512]{2,1,0:T(8,128)(2,1)}, bf16[224,128]{1,0:T(8,128)(2,1)}, bf16[64,128]{1,0:T(8,128)(2,1)}) custom-call(bf16[256,2048]{1,0:T(8,128)(2,1)} %bitcast.31, f32[1,2048]{1,0:T(1,128)} %bitcast.33, bf16[32,128]{1,0:T(8,128)(2,1)} %refs_0_.1, bf16[32,128]{1,0:T(8,128)(2,1)} %refs_1_.1, bf16[32,128]{1,0:T(8,128)(2,1)} %refs_2_.1, ...), custom_call_target="tpu_custom_call" | custom-call | tf_op jit(solution)/shard_map/pallas_call | solution.py:357
  3.9 0.0 copy-start.6
  4.0 5.2 %all-to-all-start = ((bf16[4,256,512]{2,1,0:T(8,128)(2,1)}), bf16[4,256,512]{2,1,0:T(8,128)(2,1)S(1)}, u32[]{:S(2)}, u32[]{:S(2)}) async-start(bf16[4,256,512]{2,1,0:T(8,128)(2,1)} %get-tuple-element.22), calls=%async_computation | async-start | bytes 2097152 | tf_op jit(solution)/shard_map/all_to_all | solution.py:385
  9.1 0.0 copy-done.6
  9.1 34.0 %all-gather = bf16[3584,128]{1,0:T(8,128)(2,1)S(1)} all-gather(bf16[224,128]{1,0:T(8,128)(2,1)S(1)} %copy-done.6), channel_id=2, replica_groups=mesh['sp'=16,'fs'=4,'tp'=8] {'sp'}, dimensions={0}, use_global_device_ids=true | all-gather | bytes 974848 | tf_op jit(solution)/shard_map/all_gather | solution.py:386
  43.1 0.0 copy-start.2
  43.1 0.0 copy-start.3
  43.1 0.0 copy-start.4
  43.1 0.0 copy-start.5
  43.1 0.0 all-to-all-done.rows_ref
  43.1 1.1 shard_map.178
  44.2 0.0 copy-start.1
  44.2 4.8 %all-to-all-start.1 = ((bf16[4,256,128]{2,1,0:T(8,128)(2,1)}), bf16[4,256,128]{2,1,0:T(8,128)(2,1)S(1)}, u32[]{:S(2)}, u32[]{:S(2)}) async-start(bf16[4,256,128]{2,1,0:T(8,128)(2,1)} %shard_map.178), calls=%async_computation.1 | async-start | bytes 524288 | tf_op jit(solution)/shard_map/all_to_all | solution.py:403
  49.1 0.0 copy-done.2
  49.1 0.0 copy-done.3
  49.1 0.0 copy-done.4
  49.1 0.0 copy-done.5
  49.1 2.2 %shard_map.177 = (bf16[4,256,768]{2,1,0:T(8,128)(2,1)}, f32[1,128]{1,0:T(1,128)S(1)}, f32[1,128]{1,0:T(1,128)S(1)}, f32[1,128]{1,0:T(1,128)S(1)}, f32[1,128]{1,0:T(1,128)S(1)}) custom-call(bf16[4,256,512]{2,1,0:T(8,128)(2,1)S(1)} %all-to-all-done.rows_ref, bf16[16,224,128]{2,1,0:T(8,128)(2,1)S(1)} %bitcast.21, f32[1,128]{1,0:T(1,128)S(1)} %bitcast.26, ...), custom_call_target="tpu_custom_call" | custom-call | tf_op jit(solution)/shard_map/pallas_call | solution.py:391
  51.3 3.3 %all-to-all-done.1.products_ref = bf16[4,256,128]{2,1,0:T(8,128)(2,1)S(1)} async-done(((bf16[4,256,128]{2,1,0:T(8,128)(2,1)}), bf16[4,256,128]{2,1,0:T(8,128)(2,1)S(1)}, u32[]{:S(2)}, u32[]{:S(2)}) %all-to-all-start.1) | async-done | bytes 262176 | tf_op jit(solution)/shard_map/all_to_all | solution.py:403
  54.6 0.0 copy-done.1
  54.7 0.0 copy-start
  54.7 3.7 %all-to-all-start.2 = ((bf16[4,256,768]{2,1,0:T(8,128)(2,1)}), bf16[4,256,768]{2,1,0:T(8,128)(2,1)S(1)}, u32[]{:S(2)}, u32[]{:S(2)}) async-start(bf16[4,256,768]{2,1,0:T(8,128)(2,1)} %get-tuple-element.26), calls=%async_computation.2 | async-start | bytes 3145728 | tf_op jit(solution)/shard_map/all_to_all | solution.py:408
  58.4 18.5 %all-gather.1 = bf16[1280,128]{1,0:T(8,128)(2,1)S(1)} all-gather(bf16[320,128]{1,0:T(8,128)(2,1)S(1)} %shard_map.179.query_ref), channel_id=3, replica_groups={{0,128,256,384},{32,160,288,416},{64,192,320,448},{96,224,352,480},{1,1..., dimensions={0}, use_global_device_ids=true | all-gather | bytes 409600 | tf_op jit(solution)/shard_map/all_gather | solution.py:410
  76.9 0.0 all-to-all-done.2.refs_0_
  76.9 0.0 copy-done
  76.9 2.3 %shard_map.180 = (bf16[912,128]{1,0:T(8,128)(2,1)S(1)}, f32[256,128]{1,0:T(8,128)S(1)}, f32[256,128]{1,0:T(8,128)S(1)}, f32[256,128]{1,0:T(8,128)S(1)}) custom-call(bf16[4,256,768]{2,1,0:T(8,128)(2,1)S(1)} %all-to-all-done.2.refs_0_, f32[1,128]{1,0:T(1,128)S(1)} %get-tuple-element.27.refs_1_, f32[1,128]{1,0:T(1,128)S(1)} %get-tuple-element.28.refs_2_, ...), custom_call_target="tpu_custom_call" | custom-call | tf_op jit(solution)/shard_map/pallas_call | solution.py:414
  79.2 14.3 %all-gather.2 = bf16[3648,128]{1,0:T(8,128)(2,1)S(1)} all-gather(bf16[912,128]{1,0:T(8,128)(2,1)S(1)} %get-tuple-element.29), channel_id=4, replica_groups={{0,32,64,96},{128,160,192,224},{256,288,320,352},{384,416,448,480},{1,3..., dimensions={0}, use_global_device_ids=true | all-gather | bytes 1167360 | tf_op jit(solution)/shard_map/all_gather | solution.py:429
  93.5 1.2 broadcast_in_dim.14
  94.8 3.5 %all-to-all-start.3 = ((bf16[4,4,4,2,32,128]{5,4,3,2,1,0:T(8,128)(2,1)}), bf16[4,4,4,2,32,128]{5,4,3,2,1,0:T(8,128)(2,1)S(1)}, u32[]{:S(2)}, u32[]{:S(2)}) async-start(bf16[4,4,4,2,32,128]{5,4,3,2,1,0:T(8,128)(2,1)} %broadcast_in_dim.14), calls=%async_computation.3 | async-start | bytes 2097152 | tf_op jit(solution)/shard_map/all_to_all | solution.py:430
  99.0 5.2 %shard_map.182 = (bf16[400,128]{1,0:T(8,128)(2,1)S(1)}, bf16[400,128]{1,0:T(8,128)(2,1)S(1)}, bf16[400,128]{1,0:T(8,128)(2,1)S(1)}) custom-call(s32[1]{0:T(128)} %bitcast.12.group_ref, f32[1]{0:T(128)S(6)} %copy.19.shift_ref, bf16[4,912,128]{2,1,0:T(8,128)(2,1)S(1)} %bitcast.17, bf16[4,320,128]{2,1,0:T(8,128)(2,1)S(1)} %bitcast.23), custom_call_target="tpu_custom_call" | custom-call | tf_op jit(solution)/shard_map/pallas_call | solution.py:437
  104.1 2.0 %collective-permute-start = (bf16[400,128]{1,0:T(8,128)(2,1)S(1)}, bf16[400,128]{1,0:T(8,128)(2,1)S(1)}, u32[]{:S(2)}, u32[]{:S(2)}) collective-permute-start(bf16[400,128]{1,0:T(8,128)(2,1)S(1)} %get-tuple-element.37), channel_id=1, source_target_pairs={{0,128},{32,160},{64,192},{96,224},{128,256},{160,288},{192,320},{... | collective-permute-start | bytes 307208 | tf_op jit(solution)/shard_map/ppermute | solution.py:446
  106.2 3.5 %collective-permute-start.1 = (bf16[400,128]{1,0:T(8,128)(2,1)S(1)}, bf16[400,128]{1,0:T(8,128)(2,1)S(1)}, u32[]{:S(2)}, u32[]{:S(2)}) collective-permute-start(bf16[400,128]{1,0:T(8,128)(2,1)S(1)} %get-tuple-element.38), channel_id=1, source_target_pairs={{0,256},{32,288},{64,320},{96,352},{128,384},{160,416},{192,448},{... | collective-permute-start | bytes 307208 | tf_op jit(solution)/shard_map/ppermute | solution.py:446
  109.7 1.3 collective-permute-start.2
  111.0 1.7 %shard_map.181 = (f32[256,128]{1,0:T(8,128)S(1)}, f32[256,128]{1,0:T(8,128)S(1)}) custom-call(s32[1]{0:T(128)} %bitcast.place_ref, f32[1]{0:T(128)S(6)} %copy.19.shift_ref, bf16[320,128]{1,0:T(8,128)(2,1)S(1)} %shard_map.179.query_ref, bf16[4,912,128]{2,1,0:T(8,128)(2,1)S(1)} %bitcast.18), custom_call_target="tpu_custom_call" | custom-call | tf_op jit(solution)/shard_map/pallas_call | solution.py:448
  112.7 0.0 collective-permute-done.refs_0_
  112.7 0.0 collective-permute-done.1.refs_1_
  112.7 4.8 %collective-permute-done.2.refs_2_ = bf16[400,128]{1,0:T(8,128)(2,1)S(1)} collective-permute-done((bf16[400,128]{1,0:T(8,128)(2,1)S(1)}, bf16[400,128]{1,0:T(8,128)(2,1)S(1)}, u32[]{:S(2)}, u32[]{:S(2)}) %collective-permute-start.2) | collective-permute-done | bytes 102432 | tf_op jit(solution)/shard_map/ppermute | solution.py:446
  117.5 0.0 all-to-all-done.3.weight_ref
  117.5 1.8 %shard_map.183 = (bf16[256,2048]{1,0:T(8,128)(2,1)S(1)}, f32[1,256]{1,0:T(1,128)}) custom-call(s32[1]{0:T(128)} %bitcast.place_ref, bf16[4,912,128]{2,1,0:T(8,128)(2,1)S(1)} %bitcast.19, f32[256,128]{1,0:T(8,128)S(1)} %get-tuple-element.30.weighted_ref, f32[256,128]{1,0:T(8,128)S(1)} %get-tuple-element.31.spent_ref, ...), custom_call_target="tpu_custom_call" | custom-call | tf_op jit(solution)/shard_map/pallas_call | solution.py:451
  119.4 35.0 %all_to_all.25 = bf16[8,32,2048]{2,1,0:T(8,128)(2,1)S(1)} all-to-all(bf16[8,32,2048]{2,1,0:T(8,128)(2,1)S(1)} %bitcast.24), channel_id=1, replica_groups=mesh['sp'=16,'fs'=4,'tp'=8] {'tp'}, dimensions={0} | all-to-all | bytes 2097152 | tf_op jit(solution)/shard_map/all_to_all | solution.py:469
  154.3 0.8 reduce_sum.12
  (2 shorter events, 0.1 us)
Async XLA Ops:
  3.9 5.2 %copy-start.6 = (bf16[224,128]{1,0:T(8,128)(2,1)S(1)}, bf16[224,128]{1,0:T(8,128)(2,1)}, u32[]{:S(2)}) copy-start(bf16[224,128]{1,0:T(8,128)(2,1)} %get-tuple-element.23) | copy-start | bytes 172036
  4.0 39.2 %all-to-all-start = ((bf16[4,256,512]{2,1,0:T(8,128)(2,1)}), bf16[4,256,512]{2,1,0:T(8,128)(2,1)S(1)}, u32[]{:S(2)}, u32[]{:S(2)}) async-start(bf16[4,256,512]{2,1,0:T(8,128)(2,1)} %get-tuple-element.22), calls=%async_computation | async-start | bytes 2097152 | tf_op jit(solution)/shard_map/all_to_all | solution.py:385
  43.1 6.0 %copy-start.2 = (f32[128]{0:T(128)S(1)}, f32[128]{0:T(128)}, u32[]{:S(2)}) copy-start(f32[128]{0:T(128)} %param.31) | copy-start | bytes 1540
  43.1 6.0 %copy-start.3 = (f32[128]{0:T(128)S(1)}, f32[128]{0:T(128)}, u32[]{:S(2)}) copy-start(f32[128]{0:T(128)} %param.32) | copy-start | bytes 1540
  43.1 6.0 %copy-start.4 = (f32[128]{0:T(128)S(1)}, f32[128]{0:T(128)}, u32[]{:S(2)}) copy-start(f32[128]{0:T(128)} %param.29) | copy-start | bytes 1540
  43.1 6.0 %copy-start.5 = (f32[128]{0:T(128)S(1)}, f32[128]{0:T(128)}, u32[]{:S(2)}) copy-start(f32[128]{0:T(128)} %param.30) | copy-start | bytes 1540
  44.2 10.4 %copy-start.1 = (bf16[64,128]{1,0:T(8,128)(2,1)S(1)}, bf16[64,128]{1,0:T(8,128)(2,1)}, u32[]{:S(2)}) copy-start(bf16[64,128]{1,0:T(8,128)(2,1)} %get-tuple-element.25.own_ref) | copy-start | bytes 49156
  44.2 10.4 %all-to-all-start.1 = ((bf16[4,256,128]{2,1,0:T(8,128)(2,1)}), bf16[4,256,128]{2,1,0:T(8,128)(2,1)S(1)}, u32[]{:S(2)}, u32[]{:S(2)}) async-start(bf16[4,256,128]{2,1,0:T(8,128)(2,1)} %shard_map.178), calls=%async_computation.1 | async-start | bytes 524288 | tf_op jit(solution)/shard_map/all_to_all | solution.py:403
  54.7 22.3 %copy-start = (f32[1,256,128]{2,1,0:T(8,128)S(1)}, f32[1,256,128]{2,1,0:T(8,128)}, u32[]{:S(2)}) copy-start(f32[1,256,128]{2,1,0:T(8,128)} %param.33) | copy-start | bytes 393220
  54.7 22.3 %all-to-all-start.2 = ((bf16[4,256,768]{2,1,0:T(8,128)(2,1)}), bf16[4,256,768]{2,1,0:T(8,128)(2,1)S(1)}, u32[]{:S(2)}, u32[]{:S(2)}) async-start(bf16[4,256,768]{2,1,0:T(8,128)(2,1)} %get-tuple-element.26), calls=%async_computation.2 | async-start | bytes 3145728 | tf_op jit(solution)/shard_map/all_to_all | solution.py:408
  94.8 22.7 %all-to-all-start.3 = ((bf16[4,4,4,2,32,128]{5,4,3,2,1,0:T(8,128)(2,1)}), bf16[4,4,4,2,32,128]{5,4,3,2,1,0:T(8,128)(2,1)S(1)}, u32[]{:S(2)}, u32[]{:S(2)}) async-start(bf16[4,4,4,2,32,128]{5,4,3,2,1,0:T(8,128)(2,1)} %broadcast_in_dim.14), calls=%async_computation.3 | async-start | bytes 2097152 | tf_op jit(solution)/shard_map/all_to_all | solution.py:430
  104.1 8.5 %collective-permute-start = (bf16[400,128]{1,0:T(8,128)(2,1)S(1)}, bf16[400,128]{1,0:T(8,128)(2,1)S(1)}, u32[]{:S(2)}, u32[]{:S(2)}) collective-permute-start(bf16[400,128]{1,0:T(8,128)(2,1)S(1)} %get-tuple-element.37), channel_id=1, source_target_pairs={{0,128},{32,160},{64,192},{96,224},{128,256},{160,288},{192,320},{... | collective-permute-start | bytes 307208 | tf_op jit(solution)/shard_map/ppermute | solution.py:446
  106.2 6.5 %collective-permute-start.1 = (bf16[400,128]{1,0:T(8,128)(2,1)S(1)}, bf16[400,128]{1,0:T(8,128)(2,1)S(1)}, u32[]{:S(2)}, u32[]{:S(2)}) collective-permute-start(bf16[400,128]{1,0:T(8,128)(2,1)S(1)} %get-tuple-element.38), channel_id=1, source_target_pairs={{0,256},{32,288},{64,320},{96,352},{128,384},{160,416},{192,448},{... | collective-permute-start | bytes 307208 | tf_op jit(solution)/shard_map/ppermute | solution.py:446
  109.7 7.8 %collective-permute-start.2 = (bf16[400,128]{1,0:T(8,128)(2,1)S(1)}, bf16[400,128]{1,0:T(8,128)(2,1)S(1)}, u32[]{:S(2)}, u32[]{:S(2)}) collective-permute-start(bf16[400,128]{1,0:T(8,128)(2,1)S(1)} %get-tuple-element.39), channel_id=1, source_target_pairs={{0,384},{32,416},{64,448},{96,480},{1,385},{33,417},{65,449},{97,4... | collective-permute-start | bytes 307208 | tf_op jit(solution)/shard_map/ppermute | solution.py:446

commit v4 on v3

--- a/solution.py
+++ b/solution.py
@@ -28,7 +28,12 @@
         kernel,
         out_shape=outs,
         in_specs=[pl.BlockSpec(memory_space=space(k)) for k in range(n_in)],
-        out_specs=jax.tree.map(lambda _: pl.BlockSpec(memory_space=pltpu.VMEM), outs),
+        out_specs=jax.tree.map(
+            lambda out: pl.BlockSpec(
+                memory_space=pltpu.SMEM if out.dtype == jnp.int32 else pltpu.VMEM
+            ),
+            outs,
+        ),
         scratch_shapes=list(scratch),
         compiler_params=pltpu.CompilerParams(vmem_limit_bytes=mib << 20),
         interpret=INTERPRET,
@@ -92,7 +97,11 @@
     vectors = refs[: (len(refs) - 1) // 2]
     out_ref = refs[len(vectors)]
     for k, ref in enumerate(refs[len(vectors) + 1 :]):
-        ref[...] = vectors[k][...]
+        if ref.dtype == jnp.int32:
+            for n in range(ref.shape[0]):
+                ref[n] = vectors[k][n]
+        else:
+            ref[...] = vectors[k][...]
     sp = weight_ref.shape[0]
     pieces = [
         weight_ref[:, k * ROWS : (k + 1) * ROWS].reshape(sp * ROWS, HEAD)
@@ -231,7 +240,7 @@
     return jnp.concatenate(pieces, axis=0)
 
 
-def far_kernel(group_ref, shift_ref, message_ref, query_ref, *out_refs):
+def far_kernel(places_ref, shift_ref, message_ref, query_ref, *out_refs):
     count = query_ref.shape[0]
     length = message_ref.shape[1] - count * 2 * ROWS - HEAD - TILE
     length = length // 2
@@ -239,11 +248,11 @@
     near = message_ref.shape[0]
     index = lax.broadcasted_iota(jnp.int32, (TILE, HEAD), 0)
     for j, out_ref in enumerate(out_refs):
-        wanted = group_ref[0] + j + 1 < count
+        wanted = places_ref[0] + j + 1 < count
 
         @pl.when(wanted)
         def _(j=j, out_ref=out_ref):
-            query = query_ref[group_ref[0] + j + 1, 0:length]
+            query = query_ref[places_ref[0] + j + 1, 0:length]
             weighted, total = attend_near(query, message_ref, shift)
             out_ref[0:length] = weighted.astype(BF16)
             decay, state = chain(message_ref, 2 * length, near)
@@ -262,28 +271,31 @@
             out_ref[...] = jnp.zeros(out_ref.shape, BF16)
 
 
-def near_kernel(place_ref, shift_ref, query_ref, message_ref, weighted_ref, total_ref):
-    place = place_ref[0]
+def near_kernel(
+    places_ref, shift_ref, query_ref, message_ref, weighted_ref, total_ref, decay_ref, state_ref
+):
+    place = places_ref[1]
     length = weighted_ref.shape[0]
     weighted, total = attend_near(query_ref[0:length], message_ref, shift_ref[0], place)
     weighted_ref[...] = weighted
     total_ref[...] = jnp.broadcast_to(total, total_ref.shape)
-
-
-def final_kernel(
-    place_ref,
-    message_ref,
+    decay_ref[...], state_ref[...] = chain(message_ref, 2 * length, place)
+
+
+def mixed_kernel(
+    places_ref,
     weighted_ref,
     spent_ref,
+    decay_ref,
+    state_ref,
     inner_ref,
     query_decayed_ref,
     gate_ref,
     gain_a_ref,
     gain_b_ref,
-    weight_ref,
     *refs,
 ):
-    far_refs, out_ref, total_ref = refs[:-2], refs[-2], refs[-1]
+    far_refs, (keep_ref, give_ref, total_ref) = refs[:-3], refs[-3:]
     length = weighted_ref.shape[0]
     incoming = jnp.zeros((HEAD, HEAD), F32)
     outside = jnp.zeros((length, HEAD), F32)
@@ -298,8 +310,7 @@
         ].astype(F32)
         outside = ref[0:length].astype(F32) + jnp.exp(-as_column(row)) * outside
         outside_row = outside_row + row
-    decay, state = chain(message_ref, 2 * length, place_ref[0])
-    state = state + decay * incoming
+    state = state_ref[...] + decay_ref[...] * incoming
     recurrent = inner_ref[...] + dot_both(query_decayed_ref[...], state, ((1,), (1,)))
     square_mean = jnp.mean(recurrent * recurrent, axis=-1, keepdims=True)
     mixed_b = (
@@ -312,15 +323,32 @@
     square_mean = jnp.mean(weighted * weighted, axis=-1, keepdims=True)
     mixed_a = (weighted * lax.rsqrt(square_mean + epsilon) * gain_a_ref[...]).astype(BF16)
     mixed = jnp.concatenate([mixed_a, mixed_b], axis=1)
-    fs, near, groups = weight_ref.shape[:3]
+    blocks = mixed.reshape(keep_ref.shape[0], 2, *keep_ref.shape[1:])
+    first = places_ref[2] == 0
+    keep_ref[...] = jnp.where(first, blocks[:, 0], blocks[:, 1])
+    give_ref[...] = jnp.where(first, blocks[:, 1], blocks[:, 0])
+
+
+def project_out_kernel(keep_ref, other_ref, own_ref, pair_ref, out_ref):
+    chips, rows, depth = keep_ref.shape
+    mixed = jnp.concatenate(
+        [ref[...].reshape(chips * rows, depth) for ref in (keep_ref, other_ref)], axis=1
+    )
+    fs, near, groups = own_ref.shape[:3]
     width = fs * ROWS
     for group in range(groups):
         for s in range(near):
             both = jnp.concatenate(
-                [weight_ref[:, s, group, k].reshape(width, HEAD) for k in range(2)], axis=1
+                [
+                    ref[:, s, group, k].reshape(width, HEAD)
+                    for ref in (own_ref, pair_ref)
+                    for k in range(2)
+                ],
+                axis=1,
             )
             at = (group * near + s) * width
-            out_ref[:, at : at + width] = dot(mixed, both, ((1,), (1,))).astype(BF16)
+            piece = dot(mixed, both, ((1,), (1,))).astype(BF16)
+            out_ref[:, :, at : at + width] = piece.reshape(chips, rows, width)
 
 
 def copies(array, size):
@@ -351,7 +379,6 @@
     sp, fs, tp = (lax.axis_size(name) for name in ("sp", "fs", "tp"))
     count = sp // NEAR
     rank = lax.axis_index("sp").astype(jnp.int32)
-    group = (rank // NEAR).reshape(1)
     shape = jax.ShapeDtypeStruct
 
     slices, packed, out_own = vmem_call(
@@ -388,13 +415,22 @@
         functools.partial(partial_kernel, 0), shape((fs, tokens, HEAD), BF16), 2
     )(rows, column)
     vector = shape((1, HEAD), F32)
-    second, floor, offset, gain_a, gain_b = vmem_call(
+    second, places, floor, offset, gain_a, gain_b = vmem_call(
         functools.partial(partial_kernel, 1),
-        (shape((fs, tokens, 6 * HEAD), BF16), vector, vector, vector, vector),
-        6,
+        (
+            shape((fs, tokens, 6 * HEAD), BF16),
+            shape((3,), jnp.int32),
+            vector,
+            vector,
+            vector,
+            vector,
+        ),
+        7,
+        (2,),
     )(
         rows,
         column,
+        jnp.stack((rank // NEAR, rank % NEAR, lax.axis_index("tp").astype(jnp.int32) % 2)),
         forget_floor.reshape(1, HEAD),
         forget_offset.reshape(1, HEAD),
         attention_norm_gain.reshape(1, HEAD),
@@ -439,34 +475,41 @@
         tuple(shape((tokens + TILE + HEAD, HEAD), BF16) for _ in range(count - 1)),
         4,
         (0, 1),
-    )(group, score_offset, gathered, across)
+    )(places, score_offset, gathered, across)
     outside = []
     for j in range(1, count):
-        places = [(k, k + NEAR * j) for k in range(sp - NEAR * j)]
-        outside.append(lax.ppermute(far[j - 1], "sp", places))
-    place = (rank % NEAR).reshape(1)
-    weighted, spent = vmem_call(near_kernel, (small, small), 4, (0, 1))(
-        place, score_offset, own, gathered
-    )
-    projected, row_log_total = vmem_call(
-        final_kernel,
-        (shape((tokens, width), BF16), shape((1, tokens), F32)),
+        moves = [(k, k + NEAR * j) for k in range(sp - NEAR * j)]
+        outside.append(lax.ppermute(far[j - 1], "sp", moves))
+    weighted, spent, decay, state = vmem_call(
+        near_kernel, (small, small, vector, shape((HEAD, HEAD), F32)), 4, (0, 1)
+    )(places, score_offset, own, gathered)
+    pairs = [(k, k ^ 1) for k in range(tp)]
+    out_other = lax.ppermute(out_weights, "tp", pairs)
+    half_rows = (tp // 2, tokens // tp, 2 * HEAD)
+    keep, give, row_log_total = vmem_call(
+        mixed_kernel,
+        (shape(half_rows, BF16), shape(half_rows, BF16), shape((1, tokens), F32)),
         9 + count,
         (0,),
     )(
-        place,
-        gathered,
+        places,
         weighted,
         spent,
+        decay,
+        state,
         inner,
         query_decayed,
         gate,
         gain_a,
         gain_b,
-        out_weights,
         *outside,
     )
-    tiles = lax.all_to_all(projected.reshape(tp, tokens // tp, width), "tp", 0, 0, tiled=True)
+    other = lax.ppermute(give, "tp", pairs)
+    projected = vmem_call(
+        project_out_kernel, shape((tp // 2, tokens // tp, width), BF16), 4
+    )(keep, other, out_weights, out_other)
+    chips = [list(range(k, tp, 2)) for k in range(2)]
+    tiles = lax.all_to_all(projected, "tp", 0, 0, tiled=True, axis_index_groups=chips)
     layer_out = jnp.sum(tiles.astype(F32), axis=0).astype(BF16)
     return (layer_out[None], row_log_total[None])
 

time: 156 us -> 172 us (1.10)
  starting transfers between devices: 24 us -> 40.9 us
  blocking collectives: 102 us -> 93.2 us
  waiting for transfers between devices: 8.19 us -> 15.6 us
  Pallas kernels: 17.6 us -> 19.5 us
    ppermute x3 -> x5, starting transfers between devices: 6.82 us -> 27.2 us  [the longest x1 17.3 us: on_device(): out_other = lax.ppermute(out_weights, 'tp', pairs)]
    all_to_all x1 -> x2, blocking collectives: 35 us -> 26.3 us  [the longest x1 13.5 us: on_device(): lax.all_to_all(projected, 'tp', 0, 0, tiled=True, axis_index_groups=chips)]
    ppermute x3 -> x5, waiting for transfers between devices: 4.84 us -> 12.9 us  [the longest x3 12 us: on_device(): outside.append(lax.ppermute(far[j - 1], 'sp', moves))]
    all_to_all x1 -> x0, starting transfers between devices: 3.51 us -> none  [on_device(): lax.all_to_all(copies(gathered[:, start:].reshape(NEAR, count, 2, ROWS, H...]
    pallas_call x2 -> x3, Pallas kernels: 3.5 us -> 4.38 us  [the longest x1 2.21 us: on_device(): vmem_call(near_kernel, (small, small, vector, shape((HEAD, HEAD), F32)),...]
  transfers between devices with their start and end apart: 7 -> 8, of which waited for: 2 -> 3; matrix products, arithmetic and copies ran while one was open for 0% -> 0% of each run, Pallas kernels for 6% -> 7%
where the time goes in v4:
time: 172 us
  blocking collectives  93.2 us (54%)
  starting transfers between devices  40.9 us (24%)
  Pallas kernels  19.5 us (11%)
  waiting for transfers between devices  15.6 us (9%)
    all_gather x1, blocking collectives, on_device(): column = lax.all_gather(packed, 'sp')  34 us
    all_gather x1, blocking collectives, on_device(): across = lax.all_gather(own, 'sp', axis_index_groups=strided)  18.5 us
    ppermute x1, starting transfers between devices, on_device(): out_other = lax.ppermute(out_weights, 'tp', pairs)  17.3 us
    all_gather x1, blocking collectives, on_device(): gathered = lax.all_gather(message, 'sp', axis_index_groups=groups)  14.3 us
    all_to_all x1, blocking collectives, on_device(): lax.all_to_all(projected, 'tp', 0, 0, tiled=True, axis_index_groups=chips)  13.5 us
    all_to_all x1, blocking collectives, on_device(): lax.all_to_all(copies(gathered[:, start:].reshape(NEAR, count, 2, ROWS, H...  12.9 us
    ppermute x3, waiting for transfers between devices, on_device(): outside.append(lax.ppermute(far[j - 1], 'sp', moves))  12 us
    ppermute x3, starting transfers between devices, on_device(): outside.append(lax.ppermute(far[j - 1], 'sp', moves))  7.56 us
  transfers between devices with their start and end apart: 8, of which 3 were waited for; matrix products, arithmetic and copies ran while one was open for 0% of the time, Pallas kernels for 7%

profile of v4, /device:TPU:1, one launch (start us, length us, event | category | flops | bytes accessed | tf_op | source)
XLA Modules:
  0.0 171.8 jit_solution(5457804497144645157)
XLA Ops:
  0.6 3.3 %shard_map.176 = (bf16[4,256,512]{2,1,0:T(8,128)(2,1)}, bf16[224,128]{1,0:T(8,128)(2,1)}, bf16[64,128]{1,0:T(8,128)(2,1)}) custom-call(bf16[256,2048]{1,0:T(8,128)(2,1)} %bitcast.29, f32[1,2048]{1,0:T(1,128)} %bitcast.31, bf16[32,128]{1,0:T(8,128)(2,1)} %refs_0_.1, bf16[32,128]{1,0:T(8,128)(2,1)} %refs_1_.1, bf16[32,128]{1,0:T(8,128)(2,1)} %refs_2_.1, ...), custom_call_target="tpu_custom_call" | custom-call | tf_op jit(solution)/shard_map/pallas_call | solution.py:384
  3.9 0.0 copy-start.6
  4.0 5.2 %all-to-all-start = ((bf16[4,256,512]{2,1,0:T(8,128)(2,1)}), bf16[4,256,512]{2,1,0:T(8,128)(2,1)S(1)}, u32[]{:S(2)}, u32[]{:S(2)}) async-start(bf16[4,256,512]{2,1,0:T(8,128)(2,1)} %get-tuple-element.26), calls=%async_computation | async-start | bytes 2097152 | tf_op jit(solution)/shard_map/all_to_all | solution.py:412
  9.1 0.0 copy-done.6
  9.1 34.0 %all-gather = bf16[3584,128]{1,0:T(8,128)(2,1)S(1)} all-gather(bf16[224,128]{1,0:T(8,128)(2,1)S(1)} %copy-done.6), channel_id=2, replica_groups=mesh['sp'=16,'fs'=4,'tp'=8] {'sp'}, dimensions={0}, use_global_device_ids=true | all-gather | bytes 974848 | tf_op jit(solution)/shard_map/all_gather | solution.py:413
  43.1 0.0 copy-start.2
  43.1 0.0 copy-start.3
  43.1 0.0 copy-start.4
  43.1 0.0 copy-start.5
  43.1 0.0 all-to-all-done.rows_ref
  43.1 1.1 shard_map.178
  44.2 0.0 copy-start.1
  44.2 4.8 %all-to-all-start.1 = ((bf16[4,256,128]{2,1,0:T(8,128)(2,1)}), bf16[4,256,128]{2,1,0:T(8,128)(2,1)S(1)}, u32[]{:S(2)}, u32[]{:S(2)}) async-start(bf16[4,256,128]{2,1,0:T(8,128)(2,1)} %shard_map.178), calls=%async_computation.1 | async-start | bytes 524288 | tf_op jit(solution)/shard_map/all_to_all | solution.py:439
  49.1 0.1 pad_add_fusion.refs_0_
  49.2 0.0 copy-done.2
  49.2 0.0 copy-done.3
  49.2 0.0 copy-done.4
  49.2 0.0 copy-done.5
  49.2 2.7 %shard_map.177 = (bf16[4,256,768]{2,1,0:T(8,128)(2,1)}, s32[3]{0:T(128)S(1)}, f32[1,128]{1,0:T(1,128)S(1)}, f32[1,128]{1,0:T(1,128)S(1)}, f32[1,128]{1,0:T(1,128)S(1)}, /*index=5*/f32[1,128]{1,0:T(1,128)S(1)}) custom-call(bf16[4,256,512]{2,1,0:T(8,128)(2,1)S(1)} %all-to-all-done.rows_ref, bf16[16,224,128]{2,1,0:T(8,128)(2,1)S(1)} %bitcast.20, ...), custom_call_target="tpu_custom_call" | custom-call | tf_op jit(solution)/shard_map/pallas_call | solution.py:418
  51.9 2.7 %all-to-all-done.1.products_ref = bf16[4,256,128]{2,1,0:T(8,128)(2,1)S(1)} async-done(((bf16[4,256,128]{2,1,0:T(8,128)(2,1)}), bf16[4,256,128]{2,1,0:T(8,128)(2,1)S(1)}, u32[]{:S(2)}, u32[]{:S(2)}) %all-to-all-start.1) | async-done | bytes 262176 | tf_op jit(solution)/shard_map/all_to_all | solution.py:439
  54.6 0.0 copy-done.1
  54.7 0.0 copy-start
  54.7 3.7 %all-to-all-start.2 = ((bf16[4,256,768]{2,1,0:T(8,128)(2,1)}), bf16[4,256,768]{2,1,0:T(8,128)(2,1)S(1)}, u32[]{:S(2)}, u32[]{:S(2)}) async-start(bf16[4,256,768]{2,1,0:T(8,128)(2,1)} %get-tuple-element.31), calls=%async_computation.2 | async-start | bytes 3145728 | tf_op jit(solution)/shard_map/all_to_all | solution.py:444
  58.4 18.5 %all-gather.1 = bf16[1280,128]{1,0:T(8,128)(2,1)S(1)} all-gather(bf16[320,128]{1,0:T(8,128)(2,1)S(1)} %shard_map.179.query_ref), channel_id=3, replica_groups={{0,128,256,384},{32,160,288,416},{64,192,320,448},{96,224,352,480},{1,1..., dimensions={0}, use_global_device_ids=true | all-gather | bytes 409600 | tf_op jit(solution)/shard_map/all_gather | solution.py:446
  76.9 0.0 all-to-all-done.2.refs_0_
  76.9 0.0 copy-done
  76.9 2.3 %shard_map.180 = (bf16[912,128]{1,0:T(8,128)(2,1)S(1)}, f32[256,128]{1,0:T(8,128)S(1)}, f32[256,128]{1,0:T(8,128)S(1)}, f32[256,128]{1,0:T(8,128)S(1)}) custom-call(bf16[4,256,768]{2,1,0:T(8,128)(2,1)S(1)} %all-to-all-done.2.refs_0_, f32[1,128]{1,0:T(1,128)S(1)} %get-tuple-element.32.refs_1_, f32[1,128]{1,0:T(1,128)S(1)} %get-tuple-element.33.refs_2_, ...), custom_call_target="tpu_custom_call" | custom-call | tf_op jit(solution)/shard_map/pallas_call | solution.py:450
  79.2 14.3 %all-gather.2 = bf16[3648,128]{1,0:T(8,128)(2,1)S(1)} all-gather(bf16[912,128]{1,0:T(8,128)(2,1)S(1)} %get-tuple-element.34), channel_id=4, replica_groups={{0,32,64,96},{128,160,192,224},{256,288,320,352},{384,416,448,480},{1,3..., dimensions={0}, use_global_device_ids=true | all-gather | bytes 1167360 | tf_op jit(solution)/shard_map/all_gather | solution.py:465
  93.5 0.2 broadcast_in_dim.14
  93.8 12.9 %all_to_all.25.own_ref = bf16[4,4,4,2,32,128]{5,4,3,2,1,0:T(8,128)(2,1)S(1)} all-to-all(bf16[4,4,4,2,32,128]{5,4,3,2,1,0:T(8,128)(2,1)S(1)} %broadcast_in_dim.14), channel_id=1, replica_groups=mesh['sp'=16,'fs'=4,'tp'=8] {'fs'}, dimensions={0} | all-to-all | bytes 2097152 | tf_op jit(solution)/shard_map/all_to_all | solution.py:466
  106.7 17.3 %collective-permute-start.4 = (bf16[4,4,4,2,32,128]{5,4,3,2,1,0:T(8,128)(2,1)S(1)}, bf16[4,4,4,2,32,128]{5,4,3,2,1,0:T(8,128)(2,1)S(1)}, u32[]{:S(2)}, u32[]{:S(2)}) collective-permute-start(bf16[4,4,4,2,32,128]{5,4,3,2,1,0:T(8,128)(2,1)S(1)} %all_to_all.25.own_ref), channel_id=1, source_target_pairs={{0,1},{1,0},{2,3},{3,2},{4,5},{5,4},{6,7},{7,6},{8,9},{9,8},{10,11... | collective-permute-start | bytes 3145736 | tf_op jit(solution)/shard_map/ppermute | solution.py:487
  124.6 5.7 %shard_map.182 = (bf16[400,128]{1,0:T(8,128)(2,1)S(1)}, bf16[400,128]{1,0:T(8,128)(2,1)S(1)}, bf16[400,128]{1,0:T(8,128)(2,1)S(1)}) custom-call(s32[3]{0:T(128)S(1)} %get-tuple-element.28.places_ref, f32[1]{0:T(128)S(6)} %copy.19.shift_ref, bf16[4,912,128]{2,1,0:T(8,128)(2,1)S(1)} %bitcast.17, bf16[4,320,128]{2,1,0:T(8,128)(2,1)S(1)} %bitcast.22), custom_call_target="tpu_custom_call" | custom-call | tf_op jit(solution)/shard_map/pallas_call | solution.py:473
  130.3 2.7 %collective-permute-start = (bf16[400,128]{1,0:T(8,128)(2,1)S(1)}, bf16[400,128]{1,0:T(8,128)(2,1)S(1)}, u32[]{:S(2)}, u32[]{:S(2)}) collective-permute-start(bf16[400,128]{1,0:T(8,128)(2,1)S(1)} %get-tuple-element.44), channel_id=1, source_target_pairs={{0,128},{32,160},{64,192},{96,224},{128,256},{160,288},{192,320},{... | collective-permute-start | bytes 307208 | tf_op jit(solution)/shard_map/ppermute | solution.py:482
  133.0 3.5 %collective-permute-start.1 = (bf16[400,128]{1,0:T(8,128)(2,1)S(1)}, bf16[400,128]{1,0:T(8,128)(2,1)S(1)}, u32[]{:S(2)}, u32[]{:S(2)}) collective-permute-start(bf16[400,128]{1,0:T(8,128)(2,1)S(1)} %get-tuple-element.45), channel_id=1, source_target_pairs={{0,256},{32,288},{64,320},{96,352},{128,384},{160,416},{192,448},{... | collective-permute-start | bytes 307208 | tf_op jit(solution)/shard_map/ppermute | solution.py:482
  136.6 1.3 collective-permute-start.2
  137.9 2.2 %shard_map.181 = (f32[256,128]{1,0:T(8,128)S(1)}, f32[256,128]{1,0:T(8,128)S(1)}, f32[1,128]{1,0:T(1,128)S(1)}, f32[128,128]{1,0:T(8,128)S(1)}) custom-call(s32[3]{0:T(128)S(1)} %get-tuple-element.28.places_ref, f32[1]{0:T(128)S(6)} %copy.19.shift_ref, bf16[320,128]{1,0:T(8,128)(2,1)S(1)} %shard_map.179.query_ref, bf16[4,912,128]{2,1,0:T(8,128)(2,1)S(1)} %bitcast.18), custom_call_target="tpu_custom_call" | custom-call | tf_op jit(solution)/shard_map/pallas_call | solution.py:483
  140.1 0.0 collective-permute-done.refs_0_
  140.1 0.0 collective-permute-done.1.refs_1_
  140.1 12.0 %collective-permute-done.2.refs_2_ = bf16[400,128]{1,0:T(8,128)(2,1)S(1)} collective-permute-done((bf16[400,128]{1,0:T(8,128)(2,1)S(1)}, bf16[400,128]{1,0:T(8,128)(2,1)S(1)}, u32[]{:S(2)}, u32[]{:S(2)}) %collective-permute-start.2) | collective-permute-done | bytes 102432 | tf_op jit(solution)/shard_map/ppermute | solution.py:482
  152.1 1.5 shard_map.183
  153.6 2.4 %collective-permute-start.3 = (bf16[4,32,256]{2,1,0:T(8,128)(2,1)S(1)}, bf16[4,32,256]{2,1,0:T(8,128)(2,1)S(1)}, u32[]{:S(2)}, u32[]{:S(2)}) collective-permute-start(bf16[4,32,256]{2,1,0:T(8,128)(2,1)S(1)} %get-tuple-element.48), channel_id=1, source_target_pairs={{0,1},{1,0},{2,3},{3,2},{4,5},{5,4},{6,7},{7,6},{8,9},{9,8},{10,11... | collective-permute-start | bytes 196616 | tf_op jit(solution)/shard_map/ppermute | solution.py:507
  156.0 0.9 collective-permute-done.3.other_ref
  156.8 0.0 collective-permute-done.4.pair_ref
  156.8 0.7 shard_map.184
  157.6 13.5 %all_to_all.26 = bf16[4,32,2048]{2,1,0:T(8,128)(2,1)S(1)} all-to-all(bf16[4,32,2048]{2,1,0:T(8,128)(2,1)S(1)} %shard_map.184), channel_id=1, replica_groups={{0,2,4,6},{1,3,5,7},{8,10,12,14},{9,11,13,15},{16,18,20,22},{17,19,21,2..., dimensions={0} | all-to-all | bytes 1048576 | tf_op jit(solution)/shard_map/all_to_all | solution.py:512
  171.0 0.7 reduce_sum.12
  (2 shorter events, 0.1 us)
Async XLA Ops:
  3.9 5.2 %copy-start.6 = (bf16[224,128]{1,0:T(8,128)(2,1)S(1)}, bf16[224,128]{1,0:T(8,128)(2,1)}, u32[]{:S(2)}) copy-start(bf16[224,128]{1,0:T(8,128)(2,1)} %get-tuple-element.27) | copy-start | bytes 172036
  4.0 39.2 %all-to-all-start = ((bf16[4,256,512]{2,1,0:T(8,128)(2,1)}), bf16[4,256,512]{2,1,0:T(8,128)(2,1)S(1)}, u32[]{:S(2)}, u32[]{:S(2)}) async-start(bf16[4,256,512]{2,1,0:T(8,128)(2,1)} %get-tuple-element.26), calls=%async_computation | async-start | bytes 2097152 | tf_op jit(solution)/shard_map/all_to_all | solution.py:412
  43.1 6.1 %copy-start.2 = (f32[128]{0:T(128)S(1)}, f32[128]{0:T(128)}, u32[]{:S(2)}) copy-start(f32[128]{0:T(128)} %param.31) | copy-start | bytes 1540
  43.1 6.1 %copy-start.3 = (f32[128]{0:T(128)S(1)}, f32[128]{0:T(128)}, u32[]{:S(2)}) copy-start(f32[128]{0:T(128)} %param.32) | copy-start | bytes 1540
  43.1 6.1 %copy-start.4 = (f32[128]{0:T(128)S(1)}, f32[128]{0:T(128)}, u32[]{:S(2)}) copy-start(f32[128]{0:T(128)} %param.29) | copy-start | bytes 1540
  43.1 6.1 %copy-start.5 = (f32[128]{0:T(128)S(1)}, f32[128]{0:T(128)}, u32[]{:S(2)}) copy-start(f32[128]{0:T(128)} %param.30) | copy-start | bytes 1540
  44.2 10.4 %copy-start.1 = (bf16[64,128]{1,0:T(8,128)(2,1)S(1)}, bf16[64,128]{1,0:T(8,128)(2,1)}, u32[]{:S(2)}) copy-start(bf16[64,128]{1,0:T(8,128)(2,1)} %get-tuple-element.29.own_ref) | copy-start | bytes 49156
  44.2 10.4 %all-to-all-start.1 = ((bf16[4,256,128]{2,1,0:T(8,128)(2,1)}), bf16[4,256,128]{2,1,0:T(8,128)(2,1)S(1)}, u32[]{:S(2)}, u32[]{:S(2)}) async-start(bf16[4,256,128]{2,1,0:T(8,128)(2,1)} %shard_map.178), calls=%async_computation.1 | async-start | bytes 524288 | tf_op jit(solution)/shard_map/all_to_all | solution.py:439
  54.7 22.3 %copy-start = (f32[1,256,128]{2,1,0:T(8,128)S(1)}, f32[1,256,128]{2,1,0:T(8,128)}, u32[]{:S(2)}) copy-start(f32[1,256,128]{2,1,0:T(8,128)} %param.33) | copy-start | bytes 393220
  54.7 22.3 %all-to-all-start.2 = ((bf16[4,256,768]{2,1,0:T(8,128)(2,1)}), bf16[4,256,768]{2,1,0:T(8,128)(2,1)S(1)}, u32[]{:S(2)}, u32[]{:S(2)}) async-start(bf16[4,256,768]{2,1,0:T(8,128)(2,1)} %get-tuple-element.31), calls=%async_computation.2 | async-start | bytes 3145728 | tf_op jit(solution)/shard_map/all_to_all | solution.py:444
  106.7 50.2 %collective-permute-start.4 = (bf16[4,4,4,2,32,128]{5,4,3,2,1,0:T(8,128)(2,1)S(1)}, bf16[4,4,4,2,32,128]{5,4,3,2,1,0:T(8,128)(2,1)S(1)}, u32[]{:S(2)}, u32[]{:S(2)}) collective-permute-start(bf16[4,4,4,2,32,128]{5,4,3,2,1,0:T(8,128)(2,1)S(1)} %all_to_all.25.own_ref), channel_id=1, source_target_pairs={{0,1},{1,0},{2,3},{3,2},{4,5},{5,4},{6,7},{7,6},{8,9},{9,8},{10,11... | collective-permute-start | bytes 3145736 | tf_op jit(solution)/shard_map/ppermute | solution.py:487
  130.3 9.8 %collective-permute-start = (bf16[400,128]{1,0:T(8,128)(2,1)S(1)}, bf16[400,128]{1,0:T(8,128)(2,1)S(1)}, u32[]{:S(2)}, u32[]{:S(2)}) collective-permute-start(bf16[400,128]{1,0:T(8,128)(2,1)S(1)} %get-tuple-element.44), channel_id=1, source_target_pairs={{0,128},{32,160},{64,192},{96,224},{128,256},{160,288},{192,320},{... | collective-permute-start | bytes 307208 | tf_op jit(solution)/shard_map/ppermute | solution.py:482
  133.0 7.1 %collective-permute-start.1 = (bf16[400,128]{1,0:T(8,128)(2,1)S(1)}, bf16[400,128]{1,0:T(8,128)(2,1)S(1)}, u32[]{:S(2)}, u32[]{:S(2)}) collective-permute-start(bf16[400,128]{1,0:T(8,128)(2,1)S(1)} %get-tuple-element.45), channel_id=1, source_target_pairs={{0,256},{32,288},{64,320},{96,352},{128,384},{160,416},{192,448},{... | collective-permute-start | bytes 307208 | tf_op jit(solution)/shard_map/ppermute | solution.py:482
  136.6 15.6 %collective-permute-start.2 = (bf16[400,128]{1,0:T(8,128)(2,1)S(1)}, bf16[400,128]{1,0:T(8,128)(2,1)S(1)}, u32[]{:S(2)}, u32[]{:S(2)}) collective-permute-start(bf16[400,128]{1,0:T(8,128)(2,1)S(1)} %get-tuple-element.46), channel_id=1, source_target_pairs={{0,384},{32,416},{64,448},{96,480},{1,385},{33,417},{65,449},{97,4... | collective-permute-start | bytes 307208 | tf_op jit(solution)/shard_map/ppermute | solution.py:482
  153.6 3.3 %collective-permute-start.3 = (bf16[4,32,256]{2,1,0:T(8,128)(2,1)S(1)}, bf16[4,32,256]{2,1,0:T(8,128)(2,1)S(1)}, u32[]{:S(2)}, u32[]{:S(2)}) collective-permute-start(bf16[4,32,256]{2,1,0:T(8,128)(2,1)S(1)} %get-tuple-element.48), channel_id=1, source_target_pairs={{0,1},{1,0},{2,3},{3,2},{4,5},{5,4},{6,7},{7,6},{8,9},{9,8},{10,11... | collective-permute-start | bytes 196616 | tf_op jit(solution)/shard_map/ppermute | solution.py:507

commit v5 on v4

--- a/solution.py
+++ b/solution.py
@@ -1,4 +1,5 @@
 import functools
+import math
 
 import jax
 import jax.numpy as jnp
@@ -15,6 +16,8 @@
 
 epsilon = 1e-06
 log_floor = 0.05
+LOG2_E = math.log2(math.e)
+LN_2 = math.log(2.0)
 F32 = jnp.float32
 BF16 = jnp.bfloat16
 INTERPRET = False
@@ -30,7 +33,7 @@
         in_specs=[pl.BlockSpec(memory_space=space(k)) for k in range(n_in)],
         out_specs=jax.tree.map(
             lambda out: pl.BlockSpec(
-                memory_space=pltpu.SMEM if out.dtype == jnp.int32 else pltpu.VMEM
+                memory_space=pltpu.SMEM if len(out.shape) == 1 else pltpu.VMEM
             ),
             outs,
         ),
@@ -97,7 +100,7 @@
     vectors = refs[: (len(refs) - 1) // 2]
     out_ref = refs[len(vectors)]
     for k, ref in enumerate(refs[len(vectors) + 1 :]):
-        if ref.dtype == jnp.int32:
+        if len(ref.shape) == 1:
             for n in range(ref.shape[0]):
                 ref[n] = vectors[k][n]
         else:
@@ -189,15 +192,17 @@
         at += 2 * ROWS
 
 
-def chain(message_ref, start, count):
-    def step(k, carry):
-        decay_all, state = carry
+def chain(message_ref, start, count=None):
+    decay_all, state = None, None
+    for k in range(message_ref.shape[0]):
         decay = message_ref[k, start + HEAD : start + HEAD + TILE].astype(F32)[0:1]
-        return decay * decay_all, decay * state + message_ref[k, start : start + HEAD].astype(F32)
-
-    return lax.fori_loop(
-        0, count, step, (jnp.ones((1, HEAD), F32), jnp.zeros((HEAD, HEAD), F32))
-    )
+        added = message_ref[k, start : start + HEAD].astype(F32)
+        if count is not None:
+            decay = jnp.where(k < count, decay, 1.0)
+            added = jnp.where(k < count, added, 0.0)
+        state = added if state is None else decay * state + added
+        decay_all = decay if decay_all is None else decay * decay_all
+    return decay_all, state
 
 
 def attend(query, message_ref, shift, k, ahead=None):
@@ -206,16 +211,17 @@
     col = lax.broadcasted_iota(jnp.int32, (length, length), 1)
     key = message_ref[k, 0:length]
     value = message_ref[k, length : 2 * length]
-    scores = dot(query, key, ((1,), (1,))) * HEAD ** (-0.5) + shift
-    softplus = jnp.maximum(scores, 0.0) + jnp.log(1.0 + jnp.exp(-jnp.abs(scores)))
+    scores = dot(query, key, ((1,), (1,))) * (HEAD ** (-0.5) * LOG2_E) + shift * LOG2_E
+    tail = jnp.log(1.0 + jnp.exp2(-jnp.abs(scores))) * LOG2_E
+    softplus = jnp.maximum(scores, 0.0) + tail
     if ahead is not None:
         seen = row + ahead * length > col
         softplus = jnp.where(seen, softplus, 0.0)
-    spent = dot_left(softplus, (row >= col).astype(BF16))
-    weights = jnp.exp(scores - spent)
+    after = dot(softplus.astype(BF16), (row > col).astype(BF16))
+    weights = jnp.exp2(scores - softplus - after)
     if ahead is not None:
         weights = jnp.where(seen, weights, 0.0)
-    return dot(weights.astype(BF16), value), spent[:, 0:1]
+    return dot(weights.astype(BF16), value), after[:, 0:1] + softplus[:, 0:1]
 
 
 def attend_near(query, message_ref, shift, place=None):
@@ -223,9 +229,9 @@
     for k in reversed(range(message_ref.shape[0])):
         ahead = None if place is None else place - k
         more, spent = attend(query, message_ref, shift, k, ahead)
-        weighted = more if weighted is None else weighted + jnp.exp(-total) * more
+        weighted = more if weighted is None else weighted + jnp.exp2(-total) * more
         total = spent if total is None else total + spent
-    return weighted, total
+    return weighted, total * LN_2
 
 
 def as_row(total):
@@ -245,8 +251,8 @@
     length = message_ref.shape[1] - count * 2 * ROWS - HEAD - TILE
     length = length // 2
     shift = shift_ref[0]
-    near = message_ref.shape[0]
     index = lax.broadcasted_iota(jnp.int32, (TILE, HEAD), 0)
+    decay, state = chain(message_ref, 2 * length)
     for j, out_ref in enumerate(out_refs):
         wanted = places_ref[0] + j + 1 < count
 
@@ -255,7 +261,6 @@
             query = query_ref[places_ref[0] + j + 1, 0:length]
             weighted, total = attend_near(query, message_ref, shift)
             out_ref[0:length] = weighted.astype(BF16)
-            decay, state = chain(message_ref, 2 * length, near)
             high, low = parts(as_row(total))
             pieces = [
                 piece[:, k * HEAD : (k + 1) * HEAD] for piece in (high, low) for k in range(2)
@@ -415,22 +420,24 @@
         functools.partial(partial_kernel, 0), shape((fs, tokens, HEAD), BF16), 2
     )(rows, column)
     vector = shape((1, HEAD), F32)
-    second, places, floor, offset, gain_a, gain_b = vmem_call(
+    second, places, shift, floor, offset, gain_a, gain_b = vmem_call(
         functools.partial(partial_kernel, 1),
         (
             shape((fs, tokens, 6 * HEAD), BF16),
             shape((3,), jnp.int32),
+            shape((1,), F32),
             vector,
             vector,
             vector,
             vector,
         ),
-        7,
-        (2,),
+        8,
+        (2, 3),
     )(
         rows,
         column,
         jnp.stack((rank // NEAR, rank % NEAR, lax.axis_index("tp").astype(jnp.int32) % 2)),
+        score_offset,
         forget_floor.reshape(1, HEAD),
         forget_offset.reshape(1, HEAD),
         attention_norm_gain.reshape(1, HEAD),
@@ -475,14 +482,14 @@
         tuple(shape((tokens + TILE + HEAD, HEAD), BF16) for _ in range(count - 1)),
         4,
         (0, 1),
-    )(places, score_offset, gathered, across)
+    )(places, shift, gathered, across)
     outside = []
     for j in range(1, count):
         moves = [(k, k + NEAR * j) for k in range(sp - NEAR * j)]
         outside.append(lax.ppermute(far[j - 1], "sp", moves))
     weighted, spent, decay, state = vmem_call(
         near_kernel, (small, small, vector, shape((HEAD, HEAD), F32)), 4, (0, 1)
-    )(places, score_offset, own, gathered)
+    )(places, shift, own, gathered)
     pairs = [(k, k ^ 1) for k in range(tp)]
     out_other = lax.ppermute(out_weights, "tp", pairs)
     half_rows = (tp // 2, tokens // tp, 2 * HEAD)

time: 172 us -> 172 us (level)
  no operation moved by 1% of the time
where the time goes in v5:
time: 172 us
  blocking collectives  93.2 us (54%)
  starting transfers between devices  42.3 us (25%)
  Pallas kernels  19.1 us (11%)
  waiting for transfers between devices  14.7 us (9%)
    all_gather x1, blocking collectives, on_device(): column = lax.all_gather(packed, 'sp')  34 us
    all_gather x1, blocking collectives, on_device(): across = lax.all_gather(own, 'sp', axis_index_groups=strided)  18.5 us
    ppermute x1, starting transfers between devices, on_device(): out_other = lax.ppermute(out_weights, 'tp', pairs)  17.3 us
    all_gather x1, blocking collectives, on_device(): gathered = lax.all_gather(message, 'sp', axis_index_groups=groups)  14.3 us
    all_to_all x1, blocking collectives, on_device(): lax.all_to_all(projected, 'tp', 0, 0, tiled=True, axis_index_groups=chips)  13.5 us
    all_to_all x1, blocking collectives, on_device(): lax.all_to_all(copies(gathered[:, start:].reshape(NEAR, count, 2, ROWS, H...  12.9 us
    ppermute x3, waiting for transfers between devices, on_device(): outside.append(lax.ppermute(far[j - 1], 'sp', moves))  11.7 us
    ppermute x3, starting transfers between devices, on_device(): outside.append(lax.ppermute(far[j - 1], 'sp', moves))  9 us
  transfers between devices with their start and end apart: 8, of which 3 were waited for; matrix products, arithmetic and copies ran while one was open for 0% of the time, Pallas kernels for 7%

profile of v5, /device:TPU:1, one launch (start us, length us, event | category | flops | bytes accessed | tf_op | source)
XLA Modules:
  0.0 171.8 jit_solution(10725719072301737938)
XLA Ops:
  0.6 3.3 %shard_map.176 = (bf16[4,256,512]{2,1,0:T(8,128)(2,1)}, bf16[224,128]{1,0:T(8,128)(2,1)}, bf16[64,128]{1,0:T(8,128)(2,1)}) custom-call(bf16[256,2048]{1,0:T(8,128)(2,1)} %bitcast.29, f32[1,2048]{1,0:T(1,128)} %bitcast.31, bf16[32,128]{1,0:T(8,128)(2,1)} %refs_0_.1, bf16[32,128]{1,0:T(8,128)(2,1)} %refs_1_.2, bf16[32,128]{1,0:T(8,128)(2,1)} %refs_2_.1, ...), custom_call_target="tpu_custom_call" | custom-call | tf_op jit(solution)/shard_map/pallas_call | solution.py:389
  3.9 0.0 copy-start.6
  4.0 5.2 %all-to-all-start = ((bf16[4,256,512]{2,1,0:T(8,128)(2,1)}), bf16[4,256,512]{2,1,0:T(8,128)(2,1)S(1)}, u32[]{:S(2)}, u32[]{:S(2)}) async-start(bf16[4,256,512]{2,1,0:T(8,128)(2,1)} %get-tuple-element.27), calls=%async_computation | async-start | bytes 2097152 | tf_op jit(solution)/shard_map/all_to_all | solution.py:417
  9.1 0.0 copy-done.6
  9.1 34.0 %all-gather = bf16[3584,128]{1,0:T(8,128)(2,1)S(1)} all-gather(bf16[224,128]{1,0:T(8,128)(2,1)S(1)} %copy-done.6), channel_id=2, replica_groups=mesh['sp'=16,'fs'=4,'tp'=8] {'sp'}, dimensions={0}, use_global_device_ids=true | all-gather | bytes 974848 | tf_op jit(solution)/shard_map/all_gather | solution.py:418
  43.1 0.0 copy-start.2
  43.1 0.0 copy-start.3
  43.1 0.0 copy-start.4
  43.1 0.0 copy-start.5
  43.1 0.0 all-to-all-done.rows_ref
  43.1 1.1 shard_map.178
  44.2 0.0 copy-start.1
  44.2 4.8 %all-to-all-start.1 = ((bf16[4,256,128]{2,1,0:T(8,128)(2,1)}), bf16[4,256,128]{2,1,0:T(8,128)(2,1)S(1)}, u32[]{:S(2)}, u32[]{:S(2)}) async-start(bf16[4,256,128]{2,1,0:T(8,128)(2,1)} %shard_map.178), calls=%async_computation.1 | async-start | bytes 524288 | tf_op jit(solution)/shard_map/all_to_all | solution.py:446
  49.7 0.1 pad_add_fusion.refs_0_
  49.8 0.0 copy-done.2
  49.8 0.0 copy-done.3
  49.8 0.0 copy-done.4
  49.8 0.0 copy-done.5
  49.8 2.7 %shard_map.177 = (bf16[4,256,768]{2,1,0:T(8,128)(2,1)}, s32[3]{0:T(128)S(1)}, f32[1]{0:T(128)}, f32[1,128]{1,0:T(1,128)S(1)}, f32[1,128]{1,0:T(1,128)S(1)}, /*index=5*/f32[1,128]{1,0:T(1,128)S(1)}, f32[1,128]{1,0:T(1,128)S(1)}) custom-call(bf16[4,256,512]{2,1,0:T(8,128)(2,1)S(1)} %all-to-all-done.rows_ref, bf16[16,224,128]{2,1,0:T(8,128)(2,1)S(1)} %bitcast.20, ...), custom_call_target="tpu_custom_call" | custom-call | tf_op jit(solution)/shard_map/pallas_call | solution.py:423
  52.6 2.0 %all-to-all-done.1.products_ref = bf16[4,256,128]{2,1,0:T(8,128)(2,1)S(1)} async-done(((bf16[4,256,128]{2,1,0:T(8,128)(2,1)}), bf16[4,256,128]{2,1,0:T(8,128)(2,1)S(1)}, u32[]{:S(2)}, u32[]{:S(2)}) %all-to-all-start.1) | async-done | bytes 262176 | tf_op jit(solution)/shard_map/all_to_all | solution.py:446
  54.6 0.0 copy-done.1
  54.7 0.0 copy-start
  54.7 3.7 %all-to-all-start.2 = ((bf16[4,256,768]{2,1,0:T(8,128)(2,1)}), bf16[4,256,768]{2,1,0:T(8,128)(2,1)S(1)}, u32[]{:S(2)}, u32[]{:S(2)}) async-start(bf16[4,256,768]{2,1,0:T(8,128)(2,1)} %get-tuple-element.33), calls=%async_computation.2 | async-start | bytes 3145728 | tf_op jit(solution)/shard_map/all_to_all | solution.py:451
  58.4 18.5 %all-gather.1 = bf16[1280,128]{1,0:T(8,128)(2,1)S(1)} all-gather(bf16[320,128]{1,0:T(8,128)(2,1)S(1)} %shard_map.179.query_ref), channel_id=3, replica_groups={{0,128,256,384},{32,160,288,416},{64,192,320,448},{96,224,352,480},{1,1..., dimensions={0}, use_global_device_ids=true | all-gather | bytes 409600 | tf_op jit(solution)/shard_map/all_gather | solution.py:453
  76.9 0.0 all-to-all-done.2.refs_0_
  76.9 0.0 copy-done
  76.9 2.3 %shard_map.180 = (bf16[912,128]{1,0:T(8,128)(2,1)S(1)}, f32[256,128]{1,0:T(8,128)S(1)}, f32[256,128]{1,0:T(8,128)S(1)}, f32[256,128]{1,0:T(8,128)S(1)}) custom-call(bf16[4,256,768]{2,1,0:T(8,128)(2,1)S(1)} %all-to-all-done.2.refs_0_, f32[1,128]{1,0:T(1,128)S(1)} %get-tuple-element.34.refs_1_, f32[1,128]{1,0:T(1,128)S(1)} %get-tuple-element.35.refs_2_, ...), custom_call_target="tpu_custom_call" | custom-call | tf_op jit(solution)/shard_map/pallas_call | solution.py:457
  79.2 14.3 %all-gather.2 = bf16[3648,128]{1,0:T(8,128)(2,1)S(1)} all-gather(bf16[912,128]{1,0:T(8,128)(2,1)S(1)} %get-tuple-element.36), channel_id=4, replica_groups={{0,32,64,96},{128,160,192,224},{256,288,320,352},{384,416,448,480},{1,3..., dimensions={0}, use_global_device_ids=true | all-gather | bytes 1167360 | tf_op jit(solution)/shard_map/all_gather | solution.py:472
  93.5 0.2 broadcast_in_dim.14
  93.8 12.9 %all_to_all.25.own_ref = bf16[4,4,4,2,32,128]{5,4,3,2,1,0:T(8,128)(2,1)S(1)} all-to-all(bf16[4,4,4,2,32,128]{5,4,3,2,1,0:T(8,128)(2,1)S(1)} %broadcast_in_dim.14), channel_id=1, replica_groups=mesh['sp'=16,'fs'=4,'tp'=8] {'fs'}, dimensions={0} | all-to-all | bytes 2097152 | tf_op jit(solution)/shard_map/all_to_all | solution.py:473
  106.7 17.3 %collective-permute-start.4 = (bf16[4,4,4,2,32,128]{5,4,3,2,1,0:T(8,128)(2,1)S(1)}, bf16[4,4,4,2,32,128]{5,4,3,2,1,0:T(8,128)(2,1)S(1)}, u32[]{:S(2)}, u32[]{:S(2)}) collective-permute-start(bf16[4,4,4,2,32,128]{5,4,3,2,1,0:T(8,128)(2,1)S(1)} %all_to_all.25.own_ref), channel_id=1, source_target_pairs={{0,1},{1,0},{2,3},{3,2},{4,5},{5,4},{6,7},{7,6},{8,9},{9,8},{10,11... | collective-permute-start | bytes 3145736 | tf_op jit(solution)/shard_map/ppermute | solution.py:494
  123.9 4.9 %shard_map.182 = (bf16[400,128]{1,0:T(8,128)(2,1)S(1)}, bf16[400,128]{1,0:T(8,128)(2,1)S(1)}, bf16[400,128]{1,0:T(8,128)(2,1)S(1)}) custom-call(s32[3]{0:T(128)S(1)} %get-tuple-element.29.places_ref, f32[1]{0:T(128)} %get-tuple-element.30.shift_ref, bf16[4,912,128]{2,1,0:T(8,128)(2,1)S(1)} %bitcast.17, bf16[4,320,128]{2,1,0:T(8,128)(2,1)S(1)} %bitcast.22), custom_call_target="tpu_custom_call" | custom-call | tf_op jit(solution)/shard_map/pallas_call | solution.py:480
  128.9 3.2 %collective-permute-start = (bf16[400,128]{1,0:T(8,128)(2,1)S(1)}, bf16[400,128]{1,0:T(8,128)(2,1)S(1)}, u32[]{:S(2)}, u32[]{:S(2)}) collective-permute-start(bf16[400,128]{1,0:T(8,128)(2,1)S(1)} %get-tuple-element.46), channel_id=1, source_target_pairs={{0,128},{32,160},{64,192},{96,224},{128,256},{160,288},{192,320},{... | collective-permute-start | bytes 307208 | tf_op jit(solution)/shard_map/ppermute | solution.py:489
  132.1 4.5 %collective-permute-start.1 = (bf16[400,128]{1,0:T(8,128)(2,1)S(1)}, bf16[400,128]{1,0:T(8,128)(2,1)S(1)}, u32[]{:S(2)}, u32[]{:S(2)}) collective-permute-start(bf16[400,128]{1,0:T(8,128)(2,1)S(1)} %get-tuple-element.47), channel_id=1, source_target_pairs={{0,256},{32,288},{64,320},{96,352},{128,384},{160,416},{192,448},{... | collective-permute-start | bytes 307208 | tf_op jit(solution)/shard_map/ppermute | solution.py:489
  136.6 1.3 collective-permute-start.2
  137.9 2.5 %shard_map.181 = (f32[256,128]{1,0:T(8,128)S(1)}, f32[256,128]{1,0:T(8,128)S(1)}, f32[1,128]{1,0:T(1,128)S(1)}, f32[128,128]{1,0:T(8,128)S(1)}) custom-call(s32[3]{0:T(128)S(1)} %get-tuple-element.29.places_ref, f32[1]{0:T(128)} %get-tuple-element.30.shift_ref, bf16[320,128]{1,0:T(8,128)(2,1)S(1)} %shard_map.179.query_ref, bf16[4,912,128]{2,1,0:T(8,128)(2,1)S(1)} %bitcast.18), custom_call_target="tpu_custom_call" | custom-call | tf_op jit(solution)/shard_map/pallas_call | solution.py:490
  140.4 0.0 collective-permute-done.refs_0_
  140.4 0.0 collective-permute-done.1.refs_1_
  140.4 11.7 %collective-permute-done.2.refs_2_ = bf16[400,128]{1,0:T(8,128)(2,1)S(1)} collective-permute-done((bf16[400,128]{1,0:T(8,128)(2,1)S(1)}, bf16[400,128]{1,0:T(8,128)(2,1)S(1)}, u32[]{:S(2)}, u32[]{:S(2)}) %collective-permute-start.2) | collective-permute-done | bytes 102432 | tf_op jit(solution)/shard_map/ppermute | solution.py:489
  152.1 1.5 shard_map.183
  153.6 2.4 %collective-permute-start.3 = (bf16[4,32,256]{2,1,0:T(8,128)(2,1)S(1)}, bf16[4,32,256]{2,1,0:T(8,128)(2,1)S(1)}, u32[]{:S(2)}, u32[]{:S(2)}) collective-permute-start(bf16[4,32,256]{2,1,0:T(8,128)(2,1)S(1)} %get-tuple-element.50), channel_id=1, source_target_pairs={{0,1},{1,0},{2,3},{3,2},{4,5},{5,4},{6,7},{7,6},{8,9},{9,8},{10,11... | collective-permute-start | bytes 196616 | tf_op jit(solution)/shard_map/ppermute | solution.py:514
  156.0 0.9 collective-permute-done.3.other_ref
  156.9 0.0 collective-permute-done.4.pair_ref
  156.9 0.7 shard_map.184
  157.6 13.5 %all_to_all.26 = bf16[4,32,2048]{2,1,0:T(8,128)(2,1)S(1)} all-to-all(bf16[4,32,2048]{2,1,0:T(8,128)(2,1)S(1)} %shard_map.184), channel_id=1, replica_groups={{0,2,4,6},{1,3,5,7},{8,10,12,14},{9,11,13,15},{16,18,20,22},{17,19,21,2..., dimensions={0} | all-to-all | bytes 1048576 | tf_op jit(solution)/shard_map/all_to_all | solution.py:519
  171.1 0.7 reduce_sum.12
  (2 shorter events, 0.1 us)
Async XLA Ops:
  3.9 5.2 %copy-start.6 = (bf16[224,128]{1,0:T(8,128)(2,1)S(1)}, bf16[224,128]{1,0:T(8,128)(2,1)}, u32[]{:S(2)}) copy-start(bf16[224,128]{1,0:T(8,128)(2,1)} %get-tuple-element.28) | copy-start | bytes 172036
  4.0 39.2 %all-to-all-start = ((bf16[4,256,512]{2,1,0:T(8,128)(2,1)}), bf16[4,256,512]{2,1,0:T(8,128)(2,1)S(1)}, u32[]{:S(2)}, u32[]{:S(2)}) async-start(bf16[4,256,512]{2,1,0:T(8,128)(2,1)} %get-tuple-element.27), calls=%async_computation | async-start | bytes 2097152 | tf_op jit(solution)/shard_map/all_to_all | solution.py:417
  43.1 6.7 %copy-start.2 = (f32[128]{0:T(128)S(1)}, f32[128]{0:T(128)}, u32[]{:S(2)}) copy-start(f32[128]{0:T(128)} %param.31) | copy-start | bytes 1540
  43.1 6.7 %copy-start.3 = (f32[128]{0:T(128)S(1)}, f32[128]{0:T(128)}, u32[]{:S(2)}) copy-start(f32[128]{0:T(128)} %param.32) | copy-start | bytes 1540
  43.1 6.7 %copy-start.4 = (f32[128]{0:T(128)S(1)}, f32[128]{0:T(128)}, u32[]{:S(2)}) copy-start(f32[128]{0:T(128)} %param.29) | copy-start | bytes 1540
  43.1 6.7 %copy-start.5 = (f32[128]{0:T(128)S(1)}, f32[128]{0:T(128)}, u32[]{:S(2)}) copy-start(f32[128]{0:T(128)} %param.30) | copy-start | bytes 1540
  44.2 10.4 %copy-start.1 = (bf16[64,128]{1,0:T(8,128)(2,1)S(1)}, bf16[64,128]{1,0:T(8,128)(2,1)}, u32[]{:S(2)}) copy-start(bf16[64,128]{1,0:T(8,128)(2,1)} %get-tuple-element.31.own_ref) | copy-start | bytes 49156
  44.2 10.4 %all-to-all-start.1 = ((bf16[4,256,128]{2,1,0:T(8,128)(2,1)}), bf16[4,256,128]{2,1,0:T(8,128)(2,1)S(1)}, u32[]{:S(2)}, u32[]{:S(2)}) async-start(bf16[4,256,128]{2,1,0:T(8,128)(2,1)} %shard_map.178), calls=%async_computation.1 | async-start | bytes 524288 | tf_op jit(solution)/shard_map/all_to_all | solution.py:446
  54.7 22.3 %copy-start = (f32[1,256,128]{2,1,0:T(8,128)S(1)}, f32[1,256,128]{2,1,0:T(8,128)}, u32[]{:S(2)}) copy-start(f32[1,256,128]{2,1,0:T(8,128)} %param.33) | copy-start | bytes 393220
  54.7 22.3 %all-to-all-start.2 = ((bf16[4,256,768]{2,1,0:T(8,128)(2,1)}), bf16[4,256,768]{2,1,0:T(8,128)(2,1)S(1)}, u32[]{:S(2)}, u32[]{:S(2)}) async-start(bf16[4,256,768]{2,1,0:T(8,128)(2,1)} %get-tuple-element.33), calls=%async_computation.2 | async-start | bytes 3145728 | tf_op jit(solution)/shard_map/all_to_all | solution.py:451
  106.7 50.2 %collective-permute-start.4 = (bf16[4,4,4,2,32,128]{5,4,3,2,1,0:T(8,128)(2,1)S(1)}, bf16[4,4,4,2,32,128]{5,4,3,2,1,0:T(8,128)(2,1)S(1)}, u32[]{:S(2)}, u32[]{:S(2)}) collective-permute-start(bf16[4,4,4,2,32,128]{5,4,3,2,1,0:T(8,128)(2,1)S(1)} %all_to_all.25.own_ref), channel_id=1, source_target_pairs={{0,1},{1,0},{2,3},{3,2},{4,5},{5,4},{6,7},{7,6},{8,9},{9,8},{10,11... | collective-permute-start | bytes 3145736 | tf_op jit(solution)/shard_map/ppermute | solution.py:494
  128.9 11.5 %collective-permute-start = (bf16[400,128]{1,0:T(8,128)(2,1)S(1)}, bf16[400,128]{1,0:T(8,128)(2,1)S(1)}, u32[]{:S(2)}, u32[]{:S(2)}) collective-permute-start(bf16[400,128]{1,0:T(8,128)(2,1)S(1)} %get-tuple-element.46), channel_id=1, source_target_pairs={{0,128},{32,160},{64,192},{96,224},{128,256},{160,288},{192,320},{... | collective-permute-start | bytes 307208 | tf_op jit(solution)/shard_map/ppermute | solution.py:489
  132.1 8.3 %collective-permute-start.1 = (bf16[400,128]{1,0:T(8,128)(2,1)S(1)}, bf16[400,128]{1,0:T(8,128)(2,1)S(1)}, u32[]{:S(2)}, u32[]{:S(2)}) collective-permute-start(bf16[400,128]{1,0:T(8,128)(2,1)S(1)} %get-tuple-element.47), channel_id=1, source_target_pairs={{0,256},{32,288},{64,320},{96,352},{128,384},{160,416},{192,448},{... | collective-permute-start | bytes 307208 | tf_op jit(solution)/shard_map/ppermute | solution.py:489
  136.6 15.6 %collective-permute-start.2 = (bf16[400,128]{1,0:T(8,128)(2,1)S(1)}, bf16[400,128]{1,0:T(8,128)(2,1)S(1)}, u32[]{:S(2)}, u32[]{:S(2)}) collective-permute-start(bf16[400,128]{1,0:T(8,128)(2,1)S(1)} %get-tuple-element.48), channel_id=1, source_target_pairs={{0,384},{32,416},{64,448},{96,480},{1,385},{33,417},{65,449},{97,4... | collective-permute-start | bytes 307208 | tf_op jit(solution)/shard_map/ppermute | solution.py:489
  153.6 3.3 %collective-permute-start.3 = (bf16[4,32,256]{2,1,0:T(8,128)(2,1)S(1)}, bf16[4,32,256]{2,1,0:T(8,128)(2,1)S(1)}, u32[]{:S(2)}, u32[]{:S(2)}) collective-permute-start(bf16[4,32,256]{2,1,0:T(8,128)(2,1)S(1)} %get-tuple-element.50), channel_id=1, source_target_pairs={{0,1},{1,0},{2,3},{3,2},{4,5},{5,4},{6,7},{7,6},{8,9},{9,8},{10,11... | collective-permute-start | bytes 196616 | tf_op jit(solution)/shard_map/ppermute | solution.py:514

commit v6 on v5

--- a/solution.py
+++ b/solution.py
@@ -1,4 +1,3 @@
-import functools
 import math
 
 import jax
@@ -96,23 +95,27 @@
             slices_ref[k, :, b * HEAD : (b + 1) * HEAD] = moved[:, k * HEAD : (k + 1) * HEAD]
 
 
-def partial_kernel(first, rows_ref, weight_ref, *refs):
-    vectors = refs[: (len(refs) - 1) // 2]
-    out_ref = refs[len(vectors)]
-    for k, ref in enumerate(refs[len(vectors) + 1 :]):
-        if len(ref.shape) == 1:
-            for n in range(ref.shape[0]):
-                ref[n] = vectors[k][n]
-        else:
-            ref[...] = vectors[k][...]
-    sp = weight_ref.shape[0]
-    pieces = [
-        weight_ref[:, k * ROWS : (k + 1) * ROWS].reshape(sp * ROWS, HEAD)
-        for k in range(first, first + out_ref.shape[2] // HEAD)
-    ]
-    weight = jnp.concatenate(pieces, axis=1)
+def partial_kernel(rows_ref, weight_ref, out_ref):
+    sp, depth = weight_ref.shape[:2]
+    weight = jnp.concatenate(
+        [
+            weight_ref[:, at : at + ROWS].reshape(sp * ROWS, HEAD)
+            for at in range(0, depth, ROWS)
+        ],
+        axis=1,
+    )
     for k in range(rows_ref.shape[0]):
         out_ref[k] = dot(rows_ref[k], weight).astype(BF16)
+
+
+def forward_kernel(*refs):
+    half = len(refs) // 2
+    for taken, given in zip(refs[:half], refs[half:]):
+        if len(taken.shape) == 1:
+            for n in range(taken.shape[0]):
+                given[n] = taken[n]
+        else:
+            given[...] = taken[...]
 
 
 def sum_of(products_ref):
@@ -122,25 +125,20 @@
     return total.astype(BF16)
 
 
-def attention_inputs_kernel(products_ref, own_ref, far_ref):
-    length = products_ref.shape[1]
-    far_ref[0:length] = sum_of(products_ref)
-    far_ref[length : length + 2 * ROWS] = own_ref[...]
-
-
 def local_recurrence_kernel(*refs):
     products_ref, floor_ref, offset_ref, extra_hbm, slots_ref = refs[:5]
-    message_ref, inner_ref, query_decayed_ref, gate_ref, extra_ref, arrived = refs[5:]
+    message_ref, query_ref, inner_ref, query_decayed_ref, gate_ref, extra_ref, arrived = refs[5:]
     copy = pltpu.make_async_copy(extra_hbm, extra_ref, arrived)
     copy.start()
     total = sum_of(products_ref)
-    columns = [total[:, k * HEAD : (k + 1) * HEAD] for k in range(6)]
-    query_b = columns[2].astype(F32)
+    columns = [total[:, k * HEAD : (k + 1) * HEAD] for k in range(7)]
+    query_ref[...] = columns[0]
+    query_b = columns[3].astype(F32)
     query = query_b / (1.0 + jnp.exp(-query_b))
-    value = columns[4]
-    gate_b = columns[5].astype(F32)
+    value = columns[5]
+    gate_b = columns[6].astype(F32)
     gate_ref[...] = gate_b / (1.0 + jnp.exp(-gate_b))
-    u = columns[3].astype(F32) + offset_ref[...]
+    u = columns[4].astype(F32) + offset_ref[...]
     key = (1.0 - floor_ref[...]) / (1.0 + jnp.exp(u))
     copy.wait()
     log_forget = jnp.log(1.0 - key) + extra_ref[...]
@@ -184,11 +182,11 @@
     state = dot(value, key_high, ((0,), (0,))) + dot(value, key_low, ((0,), (0,)))
     at = 0
     vector = jnp.broadcast_to(jnp.exp(final), (TILE, HEAD)).astype(BF16)
-    for piece in (columns[0], columns[1], state.astype(BF16), vector):
+    for piece in (columns[1], columns[2], state.astype(BF16), vector):
         message_ref[at : at + piece.shape[0]] = piece
         at += piece.shape[0]
     for k in range(slots_ref.shape[0]):
-        message_ref[at : at + 2 * ROWS] = slots_ref[k, slots_ref.shape[1] - 2 * ROWS :]
+        message_ref[at : at + 2 * ROWS] = slots_ref[k]
         at += 2 * ROWS
 
 
@@ -246,21 +244,19 @@
     return jnp.concatenate(pieces, axis=0)
 
 
-def far_kernel(places_ref, shift_ref, message_ref, query_ref, *out_refs):
-    count = query_ref.shape[0]
-    length = message_ref.shape[1] - count * 2 * ROWS - HEAD - TILE
-    length = length // 2
+def far_kernel(places_ref, shift_ref, message_ref, *refs):
+    count = len(refs) // 2
     shift = shift_ref[0]
+    length = refs[0].shape[0]
     index = lax.broadcasted_iota(jnp.int32, (TILE, HEAD), 0)
-    decay, state = chain(message_ref, 2 * length)
-    for j, out_ref in enumerate(out_refs):
-        wanted = places_ref[0] + j + 1 < count
+    for j, query_ref, out_ref in zip(range(count), refs[:count], refs[count:]):
+        wanted = places_ref[0] + j < count
 
         @pl.when(wanted)
-        def _(j=j, out_ref=out_ref):
-            query = query_ref[places_ref[0] + j + 1, 0:length]
-            weighted, total = attend_near(query, message_ref, shift)
+        def _(query_ref=query_ref, out_ref=out_ref):
+            weighted, total = attend_near(query_ref[...], message_ref, shift)
             out_ref[0:length] = weighted.astype(BF16)
+            decay, state = chain(message_ref, 2 * length)
             high, low = parts(as_row(total))
             pieces = [
                 piece[:, k * HEAD : (k + 1) * HEAD] for piece in (high, low) for k in range(2)
@@ -281,7 +277,7 @@
 ):
     place = places_ref[1]
     length = weighted_ref.shape[0]
-    weighted, total = attend_near(query_ref[0:length], message_ref, shift_ref[0], place)
+    weighted, total = attend_near(query_ref[...], message_ref, shift_ref[0], place)
     weighted_ref[...] = weighted
     total_ref[...] = jnp.broadcast_to(total, total_ref.shape)
     decay_ref[...], state_ref[...] = chain(message_ref, 2 * length, place)
@@ -416,26 +412,15 @@
     )
     rows = lax.all_to_all(slices, "fs", 0, 0, tiled=True)
     column = lax.all_gather(packed, "sp")
-    first = vmem_call(
-        functools.partial(partial_kernel, 0), shape((fs, tokens, HEAD), BF16), 2
-    )(rows, column)
+    products = vmem_call(partial_kernel, shape((fs, tokens, 7 * HEAD), BF16), 2)(rows, column)
+    products = lax.all_to_all(products, "fs", 0, 0, tiled=True)
     vector = shape((1, HEAD), F32)
-    second, places, shift, floor, offset, gain_a, gain_b = vmem_call(
-        functools.partial(partial_kernel, 1),
-        (
-            shape((fs, tokens, 6 * HEAD), BF16),
-            shape((3,), jnp.int32),
-            shape((1,), F32),
-            vector,
-            vector,
-            vector,
-            vector,
-        ),
-        8,
-        (2, 3),
+    places, shift, floor, offset, gain_a, gain_b = vmem_call(
+        forward_kernel,
+        (shape((3,), jnp.int32), shape((1,), F32), vector, vector, vector, vector),
+        6,
+        (0, 1),
     )(
-        rows,
-        column,
         jnp.stack((rank // NEAR, rank % NEAR, lax.axis_index("tp").astype(jnp.int32) % 2)),
         score_offset,
         forget_floor.reshape(1, HEAD),
@@ -443,31 +428,36 @@
         attention_norm_gain.reshape(1, HEAD),
         recurrence_norm_gain.reshape(1, HEAD),
     )
-    first = lax.all_to_all(first, "fs", 0, 0, tiled=True)
-    own = vmem_call(attention_inputs_kernel, shape((tokens + 2 * ROWS, HEAD), BF16), 2)(
-        first, out_own
-    )
-    second, _ = lax.optimization_barrier((second, own))
-    second = lax.all_to_all(second, "fs", 0, 0, tiled=True)
     strided = [list(range(k, sp, NEAR)) for k in range(NEAR)]
-    across = lax.all_gather(own, "sp", axis_index_groups=strided)
+    across = lax.all_gather(out_own, "sp", axis_index_groups=strided)
 
     small = shape((tokens, HEAD), F32)
     start = 2 * tokens + HEAD + TILE
-    message, inner, query_decayed, gate = vmem_call(
+    message, query, inner, query_decayed, gate = vmem_call(
         local_recurrence_kernel,
-        (shape((start + count * 2 * ROWS, HEAD), BF16), small, small, small),
+        (
+            shape((start + count * 2 * ROWS, HEAD), BF16),
+            shape((tokens, HEAD), BF16),
+            small,
+            small,
+            small,
+        ),
         5,
         (),
         (3,),
         (pltpu.VMEM((tokens, HEAD), F32), pltpu.SemaphoreType.DMA(())),
     )(
-        second,
+        products,
         floor,
         offset,
         extra_log_decay[0],
         across,
     )
+    queries = []
+    for j in (2, 1, 3):
+        moves = [(k, k - NEAR * j) for k in range(NEAR * j, sp)]
+        queries.append((j, lax.ppermute(query, "sp", moves)))
+    queries = [array for _, array in sorted(queries, key=lambda pair: pair[0])]
     groups = [list(range(NEAR * k, NEAR * (k + 1))) for k in range(count)]
     gathered = lax.all_gather(message, "sp", axis_index_groups=groups)
     out_weights = lax.all_to_all(
@@ -480,16 +470,16 @@
     far = vmem_call(
         far_kernel,
         tuple(shape((tokens + TILE + HEAD, HEAD), BF16) for _ in range(count - 1)),
-        4,
+        3 + len(queries),
         (0, 1),
-    )(places, shift, gathered, across)
+    )(places, shift, gathered, *queries)
     outside = []
     for j in range(1, count):
         moves = [(k, k + NEAR * j) for k in range(sp - NEAR * j)]
         outside.append(lax.ppermute(far[j - 1], "sp", moves))
     weighted, spent, decay, state = vmem_call(
         near_kernel, (small, small, vector, shape((HEAD, HEAD), F32)), 4, (0, 1)
-    )(places, shift, own, gathered)
+    )(places, shift, query, gathered)
     pairs = [(k, k ^ 1) for k in range(tp)]
     out_other = lax.ppermute(out_weights, "tp", pairs)
     half_rows = (tp // 2, tokens // tp, 2 * HEAD)

time: 172 us -> 181 us (1.052)
  waiting for transfers between devices: 14.7 us -> 30.1 us
  blocking collectives: 93.2 us -> 88 us
    ppermute x0 -> x3, waiting for transfers between devices: none -> 14.7 us  [on_device(): queries.append((j, lax.ppermute(query, 'sp', moves)))]
    all_gather x1, blocking collectives: 18.5 us -> 14.4 us  [on_device(): across = lax.all_gather(out_own, 'sp', axis_index_groups=strided)]
    ppermute x0 -> x3, starting transfers between devices: none -> 3.88 us  [on_device(): queries.append((j, lax.ppermute(query, 'sp', moves)))]
    all_to_all x2 -> x1, starting transfers between devices: 8.54 us -> 4.85 us  [on_device(): products = lax.all_to_all(products, 'fs', 0, 0, tiled=True)]
    ppermute x3, waiting for transfers between devices: 11.7 us -> 14.5 us  [on_device(): outside.append(lax.ppermute(far[j - 1], 'sp', moves))]
    ppermute x3, starting transfers between devices: 9 us -> 6.93 us  [on_device(): outside.append(lax.ppermute(far[j - 1], 'sp', moves))]
    all_to_all x2 -> x1, waiting for transfers between devices: 2.05 us -> 0.01 us  [on_device(): products = lax.all_to_all(products, 'fs', 0, 0, tiled=True)]
    pallas_call x3 -> x2, Pallas kernels: 3.87 us -> 2.41 us  [the longest x1 1.26 us: on_device(): vmem_call(partial_kernel, shape((fs, tokens, 7 * HEAD), BF16), 2)]
  transfers between devices with their start and end apart: 8 -> 10, of which waited for: 3 -> 5; matrix products, arithmetic and copies ran while one was open for 0% -> 0% of each run, Pallas kernels for 7% -> 6%
where the time goes in v6:
time: 181 us
  blocking collectives  88 us (49%)
  starting transfers between devices  41 us (23%)
  waiting for transfers between devices  30.1 us (17%)
  Pallas kernels  17.6 us (10%)
    all_gather x1, blocking collectives, on_device(): column = lax.all_gather(packed, 'sp')  34 us
    ppermute x1, starting transfers between devices, on_device(): out_other = lax.ppermute(out_weights, 'tp', pairs)  17.8 us
    ppermute x3, waiting for transfers between devices, on_device(): queries.append((j, lax.ppermute(query, 'sp', moves)))  14.7 us
    ppermute x3, waiting for transfers between devices, on_device(): outside.append(lax.ppermute(far[j - 1], 'sp', moves))  14.5 us
    all_gather x1, blocking collectives, on_device(): across = lax.all_gather(out_own, 'sp', axis_index_groups=strided)  14.4 us
    all_to_all x1, blocking collectives, on_device(): lax.all_to_all(copies(gathered[:, start:].reshape(NEAR, count, 2, ROWS, H...  13.5 us
    all_gather x1, blocking collectives, on_device(): gathered = lax.all_gather(message, 'sp', axis_index_groups=groups)  13.5 us
    all_to_all x1, blocking collectives, on_device(): lax.all_to_all(projected, 'tp', 0, 0, tiled=True, axis_index_groups=chips)  12.5 us
  transfers between devices with their start and end apart: 10, of which 5 were waited for; matrix products, arithmetic and copies ran while one was open for 0% of the time, Pallas kernels for 6%

profile of v6, /device:TPU:1, one launch (start us, length us, event | category | flops | bytes accessed | tf_op | source)
XLA Modules:
  0.0 180.6 jit_solution(647826773206303283)
XLA Ops:
  0.6 3.3 %shard_map.177 = (bf16[4,256,512]{2,1,0:T(8,128)(2,1)}, bf16[224,128]{1,0:T(8,128)(2,1)}, bf16[64,128]{1,0:T(8,128)(2,1)}) custom-call(bf16[256,2048]{1,0:T(8,128)(2,1)} %bitcast.27, f32[1,2048]{1,0:T(1,128)} %bitcast.29, bf16[32,128]{1,0:T(8,128)(2,1)} %refs_0_.1, bf16[32,128]{1,0:T(8,128)(2,1)} %refs_1_.2, bf16[32,128]{1,0:T(8,128)(2,1)} %refs_2_.1, ...), custom_call_target="tpu_custom_call" | custom-call | tf_op jit(solution)/shard_map/pallas_call | solution.py:385
  4.0 0.0 copy-start.6
  4.0 5.2 %all-to-all-start = ((bf16[4,256,512]{2,1,0:T(8,128)(2,1)}), bf16[4,256,512]{2,1,0:T(8,128)(2,1)S(1)}, u32[]{:S(2)}, u32[]{:S(2)}) async-start(bf16[4,256,512]{2,1,0:T(8,128)(2,1)} %get-tuple-element.28), calls=%async_computation | async-start | bytes 2097152 | tf_op jit(solution)/shard_map/all_to_all | solution.py:413
  9.1 0.0 copy-done.6
  9.1 34.0 %all-gather = bf16[3584,128]{1,0:T(8,128)(2,1)S(1)} all-gather(bf16[224,128]{1,0:T(8,128)(2,1)S(1)} %copy-done.6), channel_id=2, replica_groups=mesh['sp'=16,'fs'=4,'tp'=8] {'sp'}, dimensions={0}, use_global_device_ids=true | all-gather | bytes 974848 | tf_op jit(solution)/shard_map/all_gather | solution.py:414
  43.1 0.0 all-to-all-done.rows_ref
  43.1 1.3 shard_map.178
  44.4 0.0 copy-start
  44.4 1.3 copy-done
  45.7 0.0 copy-start.2
  45.7 0.0 copy-start.3
  45.7 0.0 copy-start.4
  45.7 0.0 copy-start.5
  45.7 0.0 copy-start.7
  45.7 0.0 copy-start.1
  45.7 4.8 %all-to-all-start.1 = ((bf16[4,256,896]{2,1,0:T(8,128)(2,1)}), bf16[4,256,896]{2,1,0:T(8,128)(2,1)S(1)}, u32[]{:S(2)}, u32[]{:S(2)}) async-start(bf16[4,256,896]{2,1,0:T(8,128)(2,1)} %copy-done), calls=%async_computation.1 | async-start | bytes 3670016 | tf_op jit(solution)/shard_map/all_to_all | solution.py:416
  51.2 0.1 pad_add_fusion.refs_0_
  51.3 0.0 copy-done.2
  51.3 0.0 copy-done.3
  51.3 0.0 copy-done.4
  51.3 0.0 copy-done.5
  51.3 1.1 shard_map.176
  52.5 0.0 copy-done.7
  52.5 14.4 %all-gather.1 = bf16[256,128]{1,0:T(8,128)(2,1)S(1)} all-gather(bf16[64,128]{1,0:T(8,128)(2,1)S(1)} %copy-done.7), channel_id=3, replica_groups={{0,128,256,384},{32,160,288,416},{64,192,320,448},{96,224,352,480},{1,1..., dimensions={0}, use_global_device_ids=true | all-gather | bytes 81920 | tf_op jit(solution)/shard_map/all_gather | solution.py:432
  66.9 0.0 all-to-all-done.1.refs_0_
  66.9 0.0 copy-done.1
  66.9 2.3 %shard_map.179 = (bf16[912,128]{1,0:T(8,128)(2,1)S(1)}, bf16[256,128]{1,0:T(8,128)(2,1)S(1)}, f32[256,128]{1,0:T(8,128)S(1)}, f32[256,128]{1,0:T(8,128)S(1)}, f32[256,128]{1,0:T(8,128)S(1)}) custom-call(bf16[4,256,896]{2,1,0:T(8,128)(2,1)S(1)} %all-to-all-done.1.refs_0_, f32[1,128]{1,0:T(1,128)S(1)} %get-tuple-element.30.refs_1_, ...), custom_call_target="tpu_custom_call" | custom-call | tf_op jit(solution)/shard_map/pallas_call | solution.py:436
  69.2 13.5 %all-gather.2 = bf16[3648,128]{1,0:T(8,128)(2,1)S(1)} all-gather(bf16[912,128]{1,0:T(8,128)(2,1)S(1)} %get-tuple-element.34), channel_id=4, replica_groups={{0,32,64,96},{128,160,192,224},{256,288,320,352},{384,416,448,480},{1,3..., dimensions={0}, use_global_device_ids=true | all-gather | bytes 1167360 | tf_op jit(solution)/shard_map/all_gather | solution.py:462
  82.8 0.2 broadcast_in_dim.14
  83.1 13.5 %all_to_all.20.own_ref = bf16[4,4,4,2,32,128]{5,4,3,2,1,0:T(8,128)(2,1)S(1)} all-to-all(bf16[4,4,4,2,32,128]{5,4,3,2,1,0:T(8,128)(2,1)S(1)} %broadcast_in_dim.14), channel_id=1, replica_groups=mesh['sp'=16,'fs'=4,'tp'=8] {'fs'}, dimensions={0} | all-to-all | bytes 2097152 | tf_op jit(solution)/shard_map/all_to_all | solution.py:463
  96.6 17.8 %collective-permute-start.7 = (bf16[4,4,4,2,32,128]{5,4,3,2,1,0:T(8,128)(2,1)S(1)}, bf16[4,4,4,2,32,128]{5,4,3,2,1,0:T(8,128)(2,1)S(1)}, u32[]{:S(2)}, u32[]{:S(2)}) collective-permute-start(bf16[4,4,4,2,32,128]{5,4,3,2,1,0:T(8,128)(2,1)S(1)} %all_to_all.20.own_ref), channel_id=1, source_target_pairs={{0,1},{1,0},{2,3},{3,2},{4,5},{5,4},{6,7},{7,6},{8,9},{9,8},{10,11... | collective-permute-start | bytes 3145736 | tf_op jit(solution)/shard_map/ppermute | solution.py:484
  114.4 1.3 collective-permute-start
  115.7 1.3 collective-permute-start.1
  117.0 1.3 collective-permute-start.2
  118.3 6.4 %collective-permute-done.refs_0_ = bf16[256,128]{1,0:T(8,128)(2,1)S(1)} collective-permute-done((bf16[256,128]{1,0:T(8,128)(2,1)S(1)}, bf16[256,128]{1,0:T(8,128)(2,1)S(1)}, u32[]{:S(2)}, u32[]{:S(2)}) %collective-permute-start) | collective-permute-done | bytes 65568 | tf_op jit(solution)/shard_map/ppermute | solution.py:459
  124.7 5.3 %collective-permute-done.1.refs_1_ = bf16[256,128]{1,0:T(8,128)(2,1)S(1)} collective-permute-done((bf16[256,128]{1,0:T(8,128)(2,1)S(1)}, bf16[256,128]{1,0:T(8,128)(2,1)S(1)}, u32[]{:S(2)}, u32[]{:S(2)}) %collective-permute-start.1) | collective-permute-done | bytes 65568 | tf_op jit(solution)/shard_map/ppermute | solution.py:459
  129.9 3.1 %collective-permute-done.2.refs_2_ = bf16[256,128]{1,0:T(8,128)(2,1)S(1)} collective-permute-done((bf16[256,128]{1,0:T(8,128)(2,1)S(1)}, bf16[256,128]{1,0:T(8,128)(2,1)S(1)}, u32[]{:S(2)}, u32[]{:S(2)}) %collective-permute-start.2) | collective-permute-done | bytes 65568 | tf_op jit(solution)/shard_map/ppermute | solution.py:459
  133.0 4.9 %shard_map.181 = (bf16[400,128]{1,0:T(8,128)(2,1)S(1)}, bf16[400,128]{1,0:T(8,128)(2,1)S(1)}, bf16[400,128]{1,0:T(8,128)(2,1)S(1)}) custom-call(s32[3]{0:T(128)S(1)} %get-tuple-element.26.places_ref, f32[1]{0:T(128)} %get-tuple-element.27.shift_ref, bf16[4,912,128]{2,1,0:T(8,128)(2,1)S(1)} %bitcast.17, bf16[256,128]{1,0:T(8,128)(2,1)S(1)} %collective-permute-done.refs_0_, ...), custom_call_target="tpu_custom_call" | custom-call | tf_op jit(solution)/shard_map/pallas_call | solution.py:470
  137.9 4.3 %collective-permute-start.3 = (bf16[400,128]{1,0:T(8,128)(2,1)S(1)}, bf16[400,128]{1,0:T(8,128)(2,1)S(1)}, u32[]{:S(2)}, u32[]{:S(2)}) collective-permute-start(bf16[400,128]{1,0:T(8,128)(2,1)S(1)} %get-tuple-element.44), channel_id=1, source_target_pairs={{0,128},{32,160},{64,192},{96,224},{128,256},{160,288},{192,320},{... | collective-permute-start | bytes 307208 | tf_op jit(solution)/shard_map/ppermute | solution.py:479
  142.3 1.3 collective-permute-start.4
  143.6 1.3 collective-permute-start.5
  144.9 2.5 %shard_map.180 = (f32[256,128]{1,0:T(8,128)S(1)}, f32[256,128]{1,0:T(8,128)S(1)}, f32[1,128]{1,0:T(1,128)S(1)}, f32[128,128]{1,0:T(8,128)S(1)}) custom-call(s32[3]{0:T(128)S(1)} %get-tuple-element.26.places_ref, f32[1]{0:T(128)} %get-tuple-element.27.shift_ref, bf16[256,128]{1,0:T(8,128)(2,1)S(1)} %get-tuple-element.33.query_ref, ...), custom_call_target="tpu_custom_call" | custom-call | tf_op jit(solution)/shard_map/pallas_call | solution.py:480
  147.4 0.0 collective-permute-done.3.refs_0_
  147.4 0.0 collective-permute-done.4.refs_1_
  147.4 14.5 %collective-permute-done.5.refs_2_ = bf16[400,128]{1,0:T(8,128)(2,1)S(1)} collective-permute-done((bf16[400,128]{1,0:T(8,128)(2,1)S(1)}, bf16[400,128]{1,0:T(8,128)(2,1)S(1)}, u32[]{:S(2)}, u32[]{:S(2)}) %collective-permute-start.5) | collective-permute-done | bytes 102432 | tf_op jit(solution)/shard_map/ppermute | solution.py:479
  161.9 1.5 shard_map.182
  163.4 2.4 %collective-permute-start.6 = (bf16[4,32,256]{2,1,0:T(8,128)(2,1)S(1)}, bf16[4,32,256]{2,1,0:T(8,128)(2,1)S(1)}, u32[]{:S(2)}, u32[]{:S(2)}) collective-permute-start(bf16[4,32,256]{2,1,0:T(8,128)(2,1)S(1)} %get-tuple-element.48), channel_id=1, source_target_pairs={{0,1},{1,0},{2,3},{3,2},{4,5},{5,4},{6,7},{7,6},{8,9},{9,8},{10,11... | collective-permute-start | bytes 196616 | tf_op jit(solution)/shard_map/ppermute | solution.py:504
  165.8 0.9 collective-permute-done.6.other_ref
  166.7 0.0 collective-permute-done.7.pair_ref
  166.7 0.7 shard_map.183
  167.4 12.5 %all_to_all.21 = bf16[4,32,2048]{2,1,0:T(8,128)(2,1)S(1)} all-to-all(bf16[4,32,2048]{2,1,0:T(8,128)(2,1)S(1)} %shard_map.183), channel_id=1, replica_groups={{0,2,4,6},{1,3,5,7},{8,10,12,14},{9,11,13,15},{16,18,20,22},{17,19,21,2..., dimensions={0} | all-to-all | bytes 1048576 | tf_op jit(solution)/shard_map/all_to_all | solution.py:509
  179.9 0.7 reduce_sum.12
  (1 shorter events, 0.0 us)
Async XLA Ops:
  4.0 5.2 %copy-start.6 = (bf16[224,128]{1,0:T(8,128)(2,1)S(1)}, bf16[224,128]{1,0:T(8,128)(2,1)}, u32[]{:S(2)}) copy-start(bf16[224,128]{1,0:T(8,128)(2,1)} %get-tuple-element.29) | copy-start | bytes 172036
  4.0 39.2 %all-to-all-start = ((bf16[4,256,512]{2,1,0:T(8,128)(2,1)}), bf16[4,256,512]{2,1,0:T(8,128)(2,1)S(1)}, u32[]{:S(2)}, u32[]{:S(2)}) async-start(bf16[4,256,512]{2,1,0:T(8,128)(2,1)} %get-tuple-element.28), calls=%async_computation | async-start | bytes 2097152 | tf_op jit(solution)/shard_map/all_to_all | solution.py:413
  44.4 1.3 copy-start
  45.7 5.6 %copy-start.2 = (f32[128]{0:T(128)S(1)}, f32[128]{0:T(128)}, u32[]{:S(2)}) copy-start(f32[128]{0:T(128)} %param.31) | copy-start | bytes 1540
  45.7 5.6 %copy-start.3 = (f32[128]{0:T(128)S(1)}, f32[128]{0:T(128)}, u32[]{:S(2)}) copy-start(f32[128]{0:T(128)} %param.32) | copy-start | bytes 1540
  45.7 5.6 %copy-start.4 = (f32[128]{0:T(128)S(1)}, f32[128]{0:T(128)}, u32[]{:S(2)}) copy-start(f32[128]{0:T(128)} %param.29) | copy-start | bytes 1540
  45.7 5.6 %copy-start.5 = (f32[128]{0:T(128)S(1)}, f32[128]{0:T(128)}, u32[]{:S(2)}) copy-start(f32[128]{0:T(128)} %param.30) | copy-start | bytes 1540
  45.7 6.8 %copy-start.7 = (bf16[64,128]{1,0:T(8,128)(2,1)S(1)}, bf16[64,128]{1,0:T(8,128)(2,1)}, u32[]{:S(2)}) copy-start(bf16[64,128]{1,0:T(8,128)(2,1)} %get-tuple-element.32) | copy-start | bytes 49156
  45.7 21.2 %copy-start.1 = (f32[1,256,128]{2,1,0:T(8,128)S(1)}, f32[1,256,128]{2,1,0:T(8,128)}, u32[]{:S(2)}) copy-start(f32[1,256,128]{2,1,0:T(8,128)} %param.33) | copy-start | bytes 393220
  45.7 21.2 %all-to-all-start.1 = ((bf16[4,256,896]{2,1,0:T(8,128)(2,1)}), bf16[4,256,896]{2,1,0:T(8,128)(2,1)S(1)}, u32[]{:S(2)}, u32[]{:S(2)}) async-start(bf16[4,256,896]{2,1,0:T(8,128)(2,1)} %copy-done), calls=%async_computation.1 | async-start | bytes 3670016 | tf_op jit(solution)/shard_map/all_to_all | solution.py:416
  96.6 70.1 %collective-permute-start.7 = (bf16[4,4,4,2,32,128]{5,4,3,2,1,0:T(8,128)(2,1)S(1)}, bf16[4,4,4,2,32,128]{5,4,3,2,1,0:T(8,128)(2,1)S(1)}, u32[]{:S(2)}, u32[]{:S(2)}) collective-permute-start(bf16[4,4,4,2,32,128]{5,4,3,2,1,0:T(8,128)(2,1)S(1)} %all_to_all.20.own_ref), channel_id=1, source_target_pairs={{0,1},{1,0},{2,3},{3,2},{4,5},{5,4},{6,7},{7,6},{8,9},{9,8},{10,11... | collective-permute-start | bytes 3145736 | tf_op jit(solution)/shard_map/ppermute | solution.py:484
  114.4 10.3 %collective-permute-start = (bf16[256,128]{1,0:T(8,128)(2,1)S(1)}, bf16[256,128]{1,0:T(8,128)(2,1)S(1)}, u32[]{:S(2)}, u32[]{:S(2)}) collective-permute-start(bf16[256,128]{1,0:T(8,128)(2,1)S(1)} %get-tuple-element.33.query_ref), channel_id=1, source_target_pairs={{128,0},{160,32},{192,64},{224,96},{256,128},{288,160},{320,192},{... | collective-permute-start | bytes 196616 | tf_op jit(solution)/shard_map/ppermute | solution.py:459
  115.7 14.2 %collective-permute-start.1 = (bf16[256,128]{1,0:T(8,128)(2,1)S(1)}, bf16[256,128]{1,0:T(8,128)(2,1)S(1)}, u32[]{:S(2)}, u32[]{:S(2)}) collective-permute-start(bf16[256,128]{1,0:T(8,128)(2,1)S(1)} %get-tuple-element.33.query_ref), channel_id=1, source_target_pairs={{256,0},{288,32},{320,64},{352,96},{384,128},{416,160},{448,192},{... | collective-permute-start | bytes 196616 | tf_op jit(solution)/shard_map/ppermute | solution.py:459
  117.0 16.0 %collective-permute-start.2 = (bf16[256,128]{1,0:T(8,128)(2,1)S(1)}, bf16[256,128]{1,0:T(8,128)(2,1)S(1)}, u32[]{:S(2)}, u32[]{:S(2)}) collective-permute-start(bf16[256,128]{1,0:T(8,128)(2,1)S(1)} %get-tuple-element.33.query_ref), channel_id=1, source_target_pairs={{384,0},{416,32},{448,64},{480,96},{385,1},{417,33},{449,65},{481,... | collective-permute-start | bytes 196616 | tf_op jit(solution)/shard_map/ppermute | solution.py:459
  137.9 9.5 %collective-permute-start.3 = (bf16[400,128]{1,0:T(8,128)(2,1)S(1)}, bf16[400,128]{1,0:T(8,128)(2,1)S(1)}, u32[]{:S(2)}, u32[]{:S(2)}) collective-permute-start(bf16[400,128]{1,0:T(8,128)(2,1)S(1)} %get-tuple-element.44), channel_id=1, source_target_pairs={{0,128},{32,160},{64,192},{96,224},{128,256},{160,288},{192,320},{... | collective-permute-start | bytes 307208 | tf_op jit(solution)/shard_map/ppermute | solution.py:479
  142.3 5.1 %collective-permute-start.4 = (bf16[400,128]{1,0:T(8,128)(2,1)S(1)}, bf16[400,128]{1,0:T(8,128)(2,1)S(1)}, u32[]{:S(2)}, u32[]{:S(2)}) collective-permute-start(bf16[400,128]{1,0:T(8,128)(2,1)S(1)} %get-tuple-element.45), channel_id=1, source_target_pairs={{0,256},{32,288},{64,320},{96,352},{128,384},{160,416},{192,448},{... | collective-permute-start | bytes 307208 | tf_op jit(solution)/shard_map/ppermute | solution.py:479
  143.6 18.3 %collective-permute-start.5 = (bf16[400,128]{1,0:T(8,128)(2,1)S(1)}, bf16[400,128]{1,0:T(8,128)(2,1)S(1)}, u32[]{:S(2)}, u32[]{:S(2)}) collective-permute-start(bf16[400,128]{1,0:T(8,128)(2,1)S(1)} %get-tuple-element.46), channel_id=1, source_target_pairs={{0,384},{32,416},{64,448},{96,480},{1,385},{33,417},{65,449},{97,4... | collective-permute-start | bytes 307208 | tf_op jit(solution)/shard_map/ppermute | solution.py:479
  163.4 3.3 %collective-permute-start.6 = (bf16[4,32,256]{2,1,0:T(8,128)(2,1)S(1)}, bf16[4,32,256]{2,1,0:T(8,128)(2,1)S(1)}, u32[]{:S(2)}, u32[]{:S(2)}) collective-permute-start(bf16[4,32,256]{2,1,0:T(8,128)(2,1)S(1)} %get-tuple-element.48), channel_id=1, source_target_pairs={{0,1},{1,0},{2,3},{3,2},{4,5},{5,4},{6,7},{7,6},{8,9},{9,8},{10,11... | collective-permute-start | bytes 196616 | tf_op jit(solution)/shard_map/ppermute | solution.py:504

commit v7 on v5

--- a/solution.py
+++ b/solution.py
@@ -31,12 +31,7 @@
         kernel,
         out_shape=outs,
         in_specs=[pl.BlockSpec(memory_space=space(k)) for k in range(n_in)],
-        out_specs=jax.tree.map(
-            lambda out: pl.BlockSpec(
-                memory_space=pltpu.SMEM if len(out.shape) == 1 else pltpu.VMEM
-            ),
-            outs,
-        ),
+        out_specs=jax.tree.map(lambda _: pl.BlockSpec(memory_space=pltpu.VMEM), outs),
         scratch_shapes=list(scratch),
         compiler_params=pltpu.CompilerParams(vmem_limit_bytes=mib << 20),
         interpret=INTERPRET,
@@ -100,9 +95,8 @@
     vectors = refs[: (len(refs) - 1) // 2]
     out_ref = refs[len(vectors)]
     for k, ref in enumerate(refs[len(vectors) + 1 :]):
-        if len(ref.shape) == 1:
-            for n in range(ref.shape[0]):
-                ref[n] = vectors[k][n]
+        if len(vectors[k].shape) == 1:
+            ref[...] = jnp.full(ref.shape, vectors[k][0])
         else:
             ref[...] = vectors[k][...]
     sp = weight_ref.shape[0]
@@ -246,21 +240,22 @@
     return jnp.concatenate(pieces, axis=0)
 
 
-def far_kernel(places_ref, shift_ref, message_ref, query_ref, *out_refs):
+def far_kernel(position_ref, shift_ref, message_ref, query_ref, *out_refs):
     count = query_ref.shape[0]
     length = message_ref.shape[1] - count * 2 * ROWS - HEAD - TILE
     length = length // 2
-    shift = shift_ref[0]
+    shift = shift_ref[...]
+    group = position_ref[0] // message_ref.shape[0] % count
     index = lax.broadcasted_iota(jnp.int32, (TILE, HEAD), 0)
-    decay, state = chain(message_ref, 2 * length)
     for j, out_ref in enumerate(out_refs):
-        wanted = places_ref[0] + j + 1 < count
+        wanted = group + j + 1 < count
 
         @pl.when(wanted)
         def _(j=j, out_ref=out_ref):
-            query = query_ref[places_ref[0] + j + 1, 0:length]
+            query = query_ref[group + j + 1, 0:length]
             weighted, total = attend_near(query, message_ref, shift)
             out_ref[0:length] = weighted.astype(BF16)
+            decay, state = chain(message_ref, 2 * length)
             high, low = parts(as_row(total))
             pieces = [
                 piece[:, k * HEAD : (k + 1) * HEAD] for piece in (high, low) for k in range(2)
@@ -277,18 +272,19 @@
 
 
 def near_kernel(
-    places_ref, shift_ref, query_ref, message_ref, weighted_ref, total_ref, decay_ref, state_ref
+    position_ref, shift_ref, query_ref, message_ref, weighted_ref, total_ref, decay_ref, state_ref
 ):
-    place = places_ref[1]
+    place = position_ref[0] % message_ref.shape[0]
     length = weighted_ref.shape[0]
-    weighted, total = attend_near(query_ref[0:length], message_ref, shift_ref[0], place)
+    weighted, total = attend_near(query_ref[0:length], message_ref, shift_ref[...], place)
     weighted_ref[...] = weighted
     total_ref[...] = jnp.broadcast_to(total, total_ref.shape)
     decay_ref[...], state_ref[...] = chain(message_ref, 2 * length, place)
 
 
 def mixed_kernel(
-    places_ref,
+    sp,
+    position_ref,
     weighted_ref,
     spent_ref,
     decay_ref,
@@ -329,7 +325,7 @@
     mixed_a = (weighted * lax.rsqrt(square_mean + epsilon) * gain_a_ref[...]).astype(BF16)
     mixed = jnp.concatenate([mixed_a, mixed_b], axis=1)
     blocks = mixed.reshape(keep_ref.shape[0], 2, *keep_ref.shape[1:])
-    first = places_ref[2] == 0
+    first = position_ref[0] < sp
     keep_ref[...] = jnp.where(first, blocks[:, 0], blocks[:, 1])
     give_ref[...] = jnp.where(first, blocks[:, 1], blocks[:, 0])
 
@@ -384,6 +380,8 @@
     sp, fs, tp = (lax.axis_size(name) for name in ("sp", "fs", "tp"))
     count = sp // NEAR
     rank = lax.axis_index("sp").astype(jnp.int32)
+    core = lax.axis_index("tp").astype(jnp.int32) & 1
+    position = (rank + sp * core).reshape(1)
     shape = jax.ShapeDtypeStruct
 
     slices, packed, out_own = vmem_call(
@@ -420,23 +418,21 @@
         functools.partial(partial_kernel, 0), shape((fs, tokens, HEAD), BF16), 2
     )(rows, column)
     vector = shape((1, HEAD), F32)
-    second, places, shift, floor, offset, gain_a, gain_b = vmem_call(
+    second, shift, floor, offset, gain_a, gain_b = vmem_call(
         functools.partial(partial_kernel, 1),
         (
             shape((fs, tokens, 6 * HEAD), BF16),
-            shape((3,), jnp.int32),
-            shape((1,), F32),
+            shape((1, tokens), F32),
             vector,
             vector,
             vector,
             vector,
         ),
-        8,
-        (2, 3),
+        7,
+        (2,),
     )(
         rows,
         column,
-        jnp.stack((rank // NEAR, rank % NEAR, lax.axis_index("tp").astype(jnp.int32) % 2)),
         score_offset,
         forget_floor.reshape(1, HEAD),
         forget_offset.reshape(1, HEAD),
@@ -481,25 +477,25 @@
         far_kernel,
         tuple(shape((tokens + TILE + HEAD, HEAD), BF16) for _ in range(count - 1)),
         4,
-        (0, 1),
-    )(places, shift, gathered, across)
+        (0,),
+    )(position, shift, gathered, across)
     outside = []
     for j in range(1, count):
         moves = [(k, k + NEAR * j) for k in range(sp - NEAR * j)]
         outside.append(lax.ppermute(far[j - 1], "sp", moves))
     weighted, spent, decay, state = vmem_call(
-        near_kernel, (small, small, vector, shape((HEAD, HEAD), F32)), 4, (0, 1)
-    )(places, shift, own, gathered)
+        near_kernel, (small, small, vector, shape((HEAD, HEAD), F32)), 4, (0,)
+    )(position, shift, own, gathered)
     pairs = [(k, k ^ 1) for k in range(tp)]
     out_other = lax.ppermute(out_weights, "tp", pairs)
     half_rows = (tp // 2, tokens // tp, 2 * HEAD)
     keep, give, row_log_total = vmem_call(
-        mixed_kernel,
+        functools.partial(mixed_kernel, sp),
         (shape(half_rows, BF16), shape(half_rows, BF16), shape((1, tokens), F32)),
         9 + count,
         (0,),
     )(
-        places,
+        position,
         weighted,
         spent,
         decay,

time: 172 us -> 171 us (level)
  Pallas kernels: 19.1 us -> 15.7 us
  transfers between devices with their start and end apart: 8 -> 8, of which waited for: 3 -> 3; matrix products, arithmetic and copies ran while one was open for 0% -> 0% of each run, Pallas kernels for 7% -> 5%
where the time goes in v7:
time: 171 us; the launch traced here: 170 us
  blocking collectives  93.2 us (55%)
  starting transfers between devices  42.5 us (25%)
  waiting for transfers between devices  16.4 us (10%)
  Pallas kernels  15.7 us (9%)
    all_gather x1, blocking collectives, on_device(): column = lax.all_gather(packed, 'sp')  34 us
    all_gather x1, blocking collectives, on_device(): across = lax.all_gather(own, 'sp', axis_index_groups=strided)  18.5 us
    ppermute x1, starting transfers between devices, on_device(): out_other = lax.ppermute(out_weights, 'tp', pairs)  17 us
    all_gather x1, blocking collectives, on_device(): gathered = lax.all_gather(message, 'sp', axis_index_groups=groups)  14.3 us
    all_to_all x1, blocking collectives, on_device(): lax.all_to_all(projected, 'tp', 0, 0, tiled=True, axis_index_groups=chips)  13.5 us
    ppermute x3, waiting for transfers between devices, on_device(): outside.append(lax.ppermute(far[j - 1], 'sp', moves))  12.9 us
    all_to_all x1, blocking collectives, on_device(): lax.all_to_all(copies(gathered[:, start:].reshape(NEAR, count, 2, ROWS, H...  12.9 us
    ppermute x3, starting transfers between devices, on_device(): outside.append(lax.ppermute(far[j - 1], 'sp', moves))  9.45 us
  transfers between devices with their start and end apart: 8, of which 3 were waited for; matrix products, arithmetic and copies ran while one was open for 0% of the time, Pallas kernels for 5%

profile of v7, /device:TPU:1, one launch (start us, length us, event | category | flops | bytes accessed | tf_op | source)
XLA Modules:
  0.0 170.4 jit_solution(7732231772340152748)
XLA Ops:
  0.6 3.3 %shard_map.176 = (bf16[4,256,512]{2,1,0:T(8,128)(2,1)}, bf16[224,128]{1,0:T(8,128)(2,1)}, bf16[64,128]{1,0:T(8,128)(2,1)}) custom-call(bf16[256,2048]{1,0:T(8,128)(2,1)} %bitcast.27, f32[1,2048]{1,0:T(1,128)} %bitcast.29, bf16[32,128]{1,0:T(8,128)(2,1)} %refs_0_.2, bf16[32,128]{1,0:T(8,128)(2,1)} %refs_1_.1, bf16[32,128]{1,0:T(8,128)(2,1)} %refs_2_.1, ...), custom_call_target="tpu_custom_call" | custom-call | tf_op jit(solution)/shard_map/pallas_call | solution.py:387
  4.0 0.0 copy-start.12
  4.0 5.2 %all-to-all-start = ((bf16[4,256,512]{2,1,0:T(8,128)(2,1)}), bf16[4,256,512]{2,1,0:T(8,128)(2,1)S(1)}, u32[]{:S(2)}, u32[]{:S(2)}) async-start(bf16[4,256,512]{2,1,0:T(8,128)(2,1)} %get-tuple-element.26), calls=%async_computation | async-start | bytes 2097152 | tf_op jit(solution)/shard_map/all_to_all | solution.py:415
  9.1 0.0 copy-done.12
  9.1 34.0 %all-gather = bf16[3584,128]{1,0:T(8,128)(2,1)S(1)} all-gather(bf16[224,128]{1,0:T(8,128)(2,1)S(1)} %copy-done.12), channel_id=2, replica_groups=mesh['sp'=16,'fs'=4,'tp'=8] {'sp'}, dimensions={0}, use_global_device_ids=true | all-gather | bytes 974848 | tf_op jit(solution)/shard_map/all_gather | solution.py:416
  43.1 0.0 copy-start.8
  43.1 0.0 copy-start.9
  43.1 0.0 copy-start.10
  43.1 0.0 copy-start.11
  43.1 0.0 all-to-all-done.rows_ref
  43.2 1.1 shard_map.178
  44.3 0.0 copy-start.7
  44.3 4.8 %all-to-all-start.1 = ((bf16[4,256,128]{2,1,0:T(8,128)(2,1)}), bf16[4,256,128]{2,1,0:T(8,128)(2,1)S(1)}, u32[]{:S(2)}, u32[]{:S(2)}) async-start(bf16[4,256,128]{2,1,0:T(8,128)(2,1)} %shard_map.178), calls=%async_computation.1 | async-start | bytes 524288 | tf_op jit(solution)/shard_map/all_to_all | solution.py:442
  49.8 0.0 copy-done.8
  49.8 0.0 copy-done.9
  49.8 0.0 copy-done.10
  49.8 0.0 copy-done.11
  49.8 2.2 %shard_map.177 = (bf16[4,256,768]{2,1,0:T(8,128)(2,1)}, f32[1,256]{1,0:T(1,128)S(1)}, f32[1,128]{1,0:T(1,128)S(1)}, f32[1,128]{1,0:T(1,128)S(1)}, f32[1,128]{1,0:T(1,128)S(1)}, /*index=5*/f32[1,128]{1,0:T(1,128)S(1)}) custom-call(bf16[4,256,512]{2,1,0:T(8,128)(2,1)S(1)} %all-to-all-done.rows_ref, bf16[16,224,128]{2,1,0:T(8,128)(2,1)S(1)} %bitcast.18, ...), custom_call_target="tpu_custom_call" | custom-call | tf_op jit(solution)/shard_map/pallas_call | solution.py:421
  52.0 2.7 %all-to-all-done.1.products_ref = bf16[4,256,128]{2,1,0:T(8,128)(2,1)S(1)} async-done(((bf16[4,256,128]{2,1,0:T(8,128)(2,1)}), bf16[4,256,128]{2,1,0:T(8,128)(2,1)S(1)}, u32[]{:S(2)}, u32[]{:S(2)}) %all-to-all-start.1) | async-done | bytes 262176 | tf_op jit(solution)/shard_map/all_to_all | solution.py:442
  54.7 0.0 copy-done.7
  54.7 0.0 copy-start
  54.7 3.7 %all-to-all-start.2 = ((bf16[4,256,768]{2,1,0:T(8,128)(2,1)}), bf16[4,256,768]{2,1,0:T(8,128)(2,1)S(1)}, u32[]{:S(2)}, u32[]{:S(2)}) async-start(bf16[4,256,768]{2,1,0:T(8,128)(2,1)} %get-tuple-element.31), calls=%async_computation.2 | async-start | bytes 3145728 | tf_op jit(solution)/shard_map/all_to_all | solution.py:447
  58.4 18.5 %all-gather.1 = bf16[1280,128]{1,0:T(8,128)(2,1)S(1)} all-gather(bf16[320,128]{1,0:T(8,128)(2,1)S(1)} %shard_map.179.query_ref), channel_id=3, replica_groups={{0,128,256,384},{32,160,288,416},{64,192,320,448},{96,224,352,480},{1,1..., dimensions={0}, use_global_device_ids=true | all-gather | bytes 409600 | tf_op jit(solution)/shard_map/all_gather | solution.py:449
  77.0 0.0 all-to-all-done.2.refs_0_
  77.0 0.0 copy-done
  77.0 2.3 %shard_map.180 = (bf16[912,128]{1,0:T(8,128)(2,1)S(1)}, f32[256,128]{1,0:T(8,128)S(1)}, f32[256,128]{1,0:T(8,128)S(1)}, f32[256,128]{1,0:T(8,128)S(1)}) custom-call(bf16[4,256,768]{2,1,0:T(8,128)(2,1)S(1)} %all-to-all-done.2.refs_0_, f32[1,128]{1,0:T(1,128)S(1)} %get-tuple-element.32.refs_1_, f32[1,128]{1,0:T(1,128)S(1)} %get-tuple-element.33.refs_2_, ...), custom_call_target="tpu_custom_call" | custom-call | tf_op jit(solution)/shard_map/pallas_call | solution.py:453
  79.3 0.0 copy-start.1
  79.3 0.0 copy-start.3
  79.3 0.0 copy-start.5
  79.3 14.3 %all-gather.2 = bf16[3648,128]{1,0:T(8,128)(2,1)S(1)} all-gather(bf16[912,128]{1,0:T(8,128)(2,1)S(1)} %get-tuple-element.34), channel_id=4, replica_groups={{0,32,64,96},{128,160,192,224},{256,288,320,352},{384,416,448,480},{1,3..., dimensions={0}, use_global_device_ids=true | all-gather | bytes 1167360 | tf_op jit(solution)/shard_map/all_gather | solution.py:468
  93.6 0.2 broadcast_in_dim.14
  93.9 0.0 copy-done.1
  93.9 0.0 copy-done.3
  93.9 0.0 copy-done.5
  93.9 12.9 %all_to_all.25.own_ref = bf16[4,4,4,2,32,128]{5,4,3,2,1,0:T(8,128)(2,1)S(1)} all-to-all(bf16[4,4,4,2,32,128]{5,4,3,2,1,0:T(8,128)(2,1)S(1)} %broadcast_in_dim.14), channel_id=1, replica_groups=mesh['sp'=16,'fs'=4,'tp'=8] {'fs'}, dimensions={0} | all-to-all | bytes 2097152 | tf_op jit(solution)/shard_map/all_to_all | solution.py:469
  106.7 17.0 %collective-permute-start.4 = (bf16[4,4,4,2,32,128]{5,4,3,2,1,0:T(8,128)(2,1)S(1)}, bf16[4,4,4,2,32,128]{5,4,3,2,1,0:T(8,128)(2,1)S(1)}, u32[]{:S(2)}, u32[]{:S(2)}) collective-permute-start(bf16[4,4,4,2,32,128]{5,4,3,2,1,0:T(8,128)(2,1)S(1)} %all_to_all.25.own_ref), channel_id=1, source_target_pairs={{0,1},{1,0},{2,3},{3,2},{4,5},{5,4},{6,7},{7,6},{8,9},{9,8},{10,11... | collective-permute-start | bytes 3145736 | tf_op jit(solution)/shard_map/ppermute | solution.py:490
  123.7 0.0 copy-start.2
  123.7 0.0 copy-start.4
  123.8 0.0 copy-start.6
  123.8 3.7 %shard_map.182 = (bf16[400,128]{1,0:T(8,128)(2,1)S(1)}, bf16[400,128]{1,0:T(8,128)(2,1)S(1)}, bf16[400,128]{1,0:T(8,128)(2,1)S(1)}) custom-call(s32[1]{0:T(128)} %bitcast.position_ref, f32[1,256]{1,0:T(1,128)S(1)} %get-tuple-element.28.shift_ref, bf16[4,912,128]{2,1,0:T(8,128)(2,1)S(1)} %bitcast.15, bf16[4,320,128]{2,1,0:T(8,128)(2,1)S(1)} %bitcast.20), custom_call_target="tpu_custom_call" | custom-call | tf_op jit(solution)/shard_map/pallas_call | solution.py:476
  127.5 3.5 %collective-permute-start = (bf16[400,128]{1,0:T(8,128)(2,1)S(1)}, bf16[400,128]{1,0:T(8,128)(2,1)S(1)}, u32[]{:S(2)}, u32[]{:S(2)}) collective-permute-start(bf16[400,128]{1,0:T(8,128)(2,1)S(1)} %get-tuple-element.44), channel_id=1, source_target_pairs={{0,128},{32,160},{64,192},{96,224},{128,256},{160,288},{192,320},{... | collective-permute-start | bytes 307208 | tf_op jit(solution)/shard_map/ppermute | solution.py:485
  131.0 4.6 %collective-permute-start.1 = (bf16[400,128]{1,0:T(8,128)(2,1)S(1)}, bf16[400,128]{1,0:T(8,128)(2,1)S(1)}, u32[]{:S(2)}, u32[]{:S(2)}) collective-permute-start(bf16[400,128]{1,0:T(8,128)(2,1)S(1)} %get-tuple-element.45), channel_id=1, source_target_pairs={{0,256},{32,288},{64,320},{96,352},{128,384},{160,416},{192,448},{... | collective-permute-start | bytes 307208 | tf_op jit(solution)/shard_map/ppermute | solution.py:485
  135.7 1.3 collective-permute-start.2
  137.0 1.3 shard_map.181
  138.3 0.0 collective-permute-done.refs_0_
  138.3 0.0 collective-permute-done.1.refs_1_
  138.3 12.9 %collective-permute-done.2.refs_2_ = bf16[400,128]{1,0:T(8,128)(2,1)S(1)} collective-permute-done((bf16[400,128]{1,0:T(8,128)(2,1)S(1)}, bf16[400,128]{1,0:T(8,128)(2,1)S(1)}, u32[]{:S(2)}, u32[]{:S(2)}) %collective-permute-start.2) | collective-permute-done | bytes 102432 | tf_op jit(solution)/shard_map/ppermute | solution.py:485
  151.2 0.0 copy-done.2
  151.2 0.0 copy-done.4
  151.2 0.0 copy-done.6
  151.2 0.9 shard_map.183
  152.2 2.4 %collective-permute-start.3 = (bf16[4,32,256]{2,1,0:T(8,128)(2,1)S(1)}, bf16[4,32,256]{2,1,0:T(8,128)(2,1)S(1)}, u32[]{:S(2)}, u32[]{:S(2)}) collective-permute-start(bf16[4,32,256]{2,1,0:T(8,128)(2,1)S(1)} %get-tuple-element.48), channel_id=1, source_target_pairs={{0,1},{1,0},{2,3},{3,2},{4,5},{5,4},{6,7},{7,6},{8,9},{9,8},{10,11... | collective-permute-start | bytes 196616 | tf_op jit(solution)/shard_map/ppermute | solution.py:510
  154.5 0.9 collective-permute-done.3.other_ref
  155.4 0.0 collective-permute-done.4.pair_ref
  155.4 0.7 shard_map.184
  156.1 13.5 %all_to_all.26 = bf16[4,32,2048]{2,1,0:T(8,128)(2,1)S(1)} all-to-all(bf16[4,32,2048]{2,1,0:T(8,128)(2,1)S(1)} %shard_map.184), channel_id=1, replica_groups={{0,2,4,6},{1,3,5,7},{8,10,12,14},{9,11,13,15},{16,18,20,22},{17,19,21,2..., dimensions={0} | all-to-all | bytes 1048576 | tf_op jit(solution)/shard_map/all_to_all | solution.py:515
  169.6 0.7 reduce_sum.12
  (2 shorter events, 0.1 us)
Async XLA Ops:
  4.0 5.2 %copy-start.12 = (bf16[224,128]{1,0:T(8,128)(2,1)S(1)}, bf16[224,128]{1,0:T(8,128)(2,1)}, u32[]{:S(2)}) copy-start(bf16[224,128]{1,0:T(8,128)(2,1)} %get-tuple-element.27) | copy-start | bytes 172036
  4.0 39.2 %all-to-all-start = ((bf16[4,256,512]{2,1,0:T(8,128)(2,1)}), bf16[4,256,512]{2,1,0:T(8,128)(2,1)S(1)}, u32[]{:S(2)}, u32[]{:S(2)}) async-start(bf16[4,256,512]{2,1,0:T(8,128)(2,1)} %get-tuple-element.26), calls=%async_computation | async-start | bytes 2097152 | tf_op jit(solution)/shard_map/all_to_all | solution.py:415
  43.1 6.7 %copy-start.8 = (f32[128]{0:T(128)S(1)}, f32[128]{0:T(128)}, u32[]{:S(2)}) copy-start(f32[128]{0:T(128)} %param.31) | copy-start | bytes 1540
  43.1 6.7 %copy-start.9 = (f32[128]{0:T(128)S(1)}, f32[128]{0:T(128)}, u32[]{:S(2)}) copy-start(f32[128]{0:T(128)} %param.32) | copy-start | bytes 1540
  43.1 6.7 %copy-start.10 = (f32[128]{0:T(128)S(1)}, f32[128]{0:T(128)}, u32[]{:S(2)}) copy-start(f32[128]{0:T(128)} %param.29) | copy-start | bytes 1540
  43.1 6.7 %copy-start.11 = (f32[128]{0:T(128)S(1)}, f32[128]{0:T(128)}, u32[]{:S(2)}) copy-start(f32[128]{0:T(128)} %param.30) | copy-start | bytes 1540
  44.3 10.4 %copy-start.7 = (bf16[64,128]{1,0:T(8,128)(2,1)S(1)}, bf16[64,128]{1,0:T(8,128)(2,1)}, u32[]{:S(2)}) copy-start(bf16[64,128]{1,0:T(8,128)(2,1)} %get-tuple-element.29.own_ref) | copy-start | bytes 49156
  44.3 10.4 %all-to-all-start.1 = ((bf16[4,256,128]{2,1,0:T(8,128)(2,1)}), bf16[4,256,128]{2,1,0:T(8,128)(2,1)S(1)}, u32[]{:S(2)}, u32[]{:S(2)}) async-start(bf16[4,256,128]{2,1,0:T(8,128)(2,1)} %shard_map.178), calls=%async_computation.1 | async-start | bytes 524288 | tf_op jit(solution)/shard_map/all_to_all | solution.py:442
  54.7 22.3 %copy-start = (f32[1,256,128]{2,1,0:T(8,128)S(1)}, f32[1,256,128]{2,1,0:T(8,128)}, u32[]{:S(2)}) copy-start(f32[1,256,128]{2,1,0:T(8,128)} %param.33) | copy-start | bytes 393220
  54.7 22.3 %all-to-all-start.2 = ((bf16[4,256,768]{2,1,0:T(8,128)(2,1)}), bf16[4,256,768]{2,1,0:T(8,128)(2,1)S(1)}, u32[]{:S(2)}, u32[]{:S(2)}) async-start(bf16[4,256,768]{2,1,0:T(8,128)(2,1)} %get-tuple-element.31), calls=%async_computation.2 | async-start | bytes 3145728 | tf_op jit(solution)/shard_map/all_to_all | solution.py:447
  79.3 14.6 %copy-start.1 = (f32[256,128]{1,0:T(8,128)}, f32[256,128]{1,0:T(8,128)S(1)}, u32[]{:S(2)}) copy-start(f32[256,128]{1,0:T(8,128)S(1)} %get-tuple-element.39.inner_ref) | copy-start | bytes 393220
  79.3 14.6 %copy-start.3 = (f32[256,128]{1,0:T(8,128)}, f32[256,128]{1,0:T(8,128)S(1)}, u32[]{:S(2)}) copy-start(f32[256,128]{1,0:T(8,128)S(1)} %get-tuple-element.40.query_decayed_ref) | copy-start | bytes 393220
  79.3 14.6 %copy-start.5 = (f32[256,128]{1,0:T(8,128)}, f32[256,128]{1,0:T(8,128)S(1)}, u32[]{:S(2)}) copy-start(f32[256,128]{1,0:T(8,128)S(1)} %get-tuple-element.41.gate_ref) | copy-start | bytes 393220
  106.7 48.7 %collective-permute-start.4 = (bf16[4,4,4,2,32,128]{5,4,3,2,1,0:T(8,128)(2,1)S(1)}, bf16[4,4,4,2,32,128]{5,4,3,2,1,0:T(8,128)(2,1)S(1)}, u32[]{:S(2)}, u32[]{:S(2)}) collective-permute-start(bf16[4,4,4,2,32,128]{5,4,3,2,1,0:T(8,128)(2,1)S(1)} %all_to_all.25.own_ref), channel_id=1, source_target_pairs={{0,1},{1,0},{2,3},{3,2},{4,5},{5,4},{6,7},{7,6},{8,9},{9,8},{10,11... | collective-permute-start | bytes 3145736 | tf_op jit(solution)/shard_map/ppermute | solution.py:490
  123.7 27.5 %copy-start.2 = (f32[256,128]{1,0:T(8,128)S(1)}, f32[256,128]{1,0:T(8,128)}, u32[]{:S(2)}) copy-start(f32[256,128]{1,0:T(8,128)} %copy-done.1) | copy-start | bytes 393220
  123.7 27.5 %copy-start.4 = (f32[256,128]{1,0:T(8,128)S(1)}, f32[256,128]{1,0:T(8,128)}, u32[]{:S(2)}) copy-start(f32[256,128]{1,0:T(8,128)} %copy-done.3) | copy-start | bytes 393220
  123.8 27.5 %copy-start.6 = (f32[256,128]{1,0:T(8,128)S(1)}, f32[256,128]{1,0:T(8,128)}, u32[]{:S(2)}) copy-start(f32[256,128]{1,0:T(8,128)} %copy-done.5) | copy-start | bytes 393220
  127.5 10.8 %collective-permute-start = (bf16[400,128]{1,0:T(8,128)(2,1)S(1)}, bf16[400,128]{1,0:T(8,128)(2,1)S(1)}, u32[]{:S(2)}, u32[]{:S(2)}) collective-permute-start(bf16[400,128]{1,0:T(8,128)(2,1)S(1)} %get-tuple-element.44), channel_id=1, source_target_pairs={{0,128},{32,160},{64,192},{96,224},{128,256},{160,288},{192,320},{... | collective-permute-start | bytes 307208 | tf_op jit(solution)/shard_map/ppermute | solution.py:485
  131.0 7.3 %collective-permute-start.1 = (bf16[400,128]{1,0:T(8,128)(2,1)S(1)}, bf16[400,128]{1,0:T(8,128)(2,1)S(1)}, u32[]{:S(2)}, u32[]{:S(2)}) collective-permute-start(bf16[400,128]{1,0:T(8,128)(2,1)S(1)} %get-tuple-element.45), channel_id=1, source_target_pairs={{0,256},{32,288},{64,320},{96,352},{128,384},{160,416},{192,448},{... | collective-permute-start | bytes 307208 | tf_op jit(solution)/shard_map/ppermute | solution.py:485
  135.7 15.6 %collective-permute-start.2 = (bf16[400,128]{1,0:T(8,128)(2,1)S(1)}, bf16[400,128]{1,0:T(8,128)(2,1)S(1)}, u32[]{:S(2)}, u32[]{:S(2)}) collective-permute-start(bf16[400,128]{1,0:T(8,128)(2,1)S(1)} %get-tuple-element.46), channel_id=1, source_target_pairs={{0,384},{32,416},{64,448},{96,480},{1,385},{33,417},{65,449},{97,4... | collective-permute-start | bytes 307208 | tf_op jit(solution)/shard_map/ppermute | solution.py:485
  152.2 3.2 %collective-permute-start.3 = (bf16[4,32,256]{2,1,0:T(8,128)(2,1)S(1)}, bf16[4,32,256]{2,1,0:T(8,128)(2,1)S(1)}, u32[]{:S(2)}, u32[]{:S(2)}) collective-permute-start(bf16[4,32,256]{2,1,0:T(8,128)(2,1)S(1)} %get-tuple-element.48), channel_id=1, source_target_pairs={{0,1},{1,0},{2,3},{3,2},{4,5},{5,4},{6,7},{7,6},{8,9},{9,8},{10,11... | collective-permute-start | bytes 196616 | tf_op jit(solution)/shard_map/ppermute | solution.py:510

commit v8 on v7

--- a/solution.py
+++ b/solution.py
@@ -148,7 +148,8 @@
     low = (rest - middle.astype(F32)).astype(BF16)
     running = dot(lower, high) + (dot(lower, middle) + dot(lower, low))
     position = lax.broadcasted_iota(jnp.int32, (length, 1), 0)
-    pairwise = jnp.where(row == col, dot_both(query, key, ((1,), (1,))), 0.0)
+    products = dot(query.astype(BF16), key.astype(BF16), ((1,), (1,)))
+    pairwise = jnp.where(row == col, products, 0.0)
     half = 1
     while half < length:
         block = 2 * half
@@ -169,7 +170,8 @@
         after = jnp.where(second, query * jnp.exp(running - boundary), 0.0)
         before = jnp.where(second, 0.0, key * jnp.exp(boundary - running))
         chosen = (row // block == col // block) & (row // half != col // half) & (row > col)
-        pairwise = jnp.where(chosen, dot_both(after, before, ((1,), (1,))), pairwise)
+        products = dot(after.astype(BF16), before.astype(BF16), ((1,), (1,)))
+        pairwise = jnp.where(chosen, products, pairwise)
         half = block
     inner_ref[...] = dot_left(pairwise, value)
     final = running[length - 1 : length]

time: 171 us -> 170 us (level)
  no operation moved by 1% of the time
where the time goes in v8:
time: 170 us
  blocking collectives  92.7 us (55%)
  starting transfers between devices  42.6 us (25%)
  waiting for transfers between devices  16.8 us (10%)
  Pallas kernels  15.1 us (9%)
    all_gather x1, blocking collectives, on_device(): column = lax.all_gather(packed, 'sp')  34 us
    all_gather x1, blocking collectives, on_device(): across = lax.all_gather(own, 'sp', axis_index_groups=strided)  18.5 us
    ppermute x1, starting transfers between devices, on_device(): out_other = lax.ppermute(out_weights, 'tp', pairs)  17.5 us
    all_gather x1, blocking collectives, on_device(): gathered = lax.all_gather(message, 'sp', axis_index_groups=groups)  14.4 us
    ppermute x3, waiting for transfers between devices, on_device(): outside.append(lax.ppermute(far[j - 1], 'sp', moves))  13.3 us
    all_to_all x1, blocking collectives, on_device(): lax.all_to_all(projected, 'tp', 0, 0, tiled=True, axis_index_groups=chips)  13 us
    all_to_all x1, blocking collectives, on_device(): lax.all_to_all(copies(gathered[:, start:].reshape(NEAR, count, 2, ROWS, H...  12.7 us
    ppermute x3, starting transfers between devices, on_device(): outside.append(lax.ppermute(far[j - 1], 'sp', moves))  8.98 us
  transfers between devices with their start and end apart: 8, of which 3 were waited for; matrix products, arithmetic and copies ran while one was open for 0% of the time, Pallas kernels for 5%

profile of v8, /device:TPU:1, one launch (start us, length us, event | category | flops | bytes accessed | tf_op | source)
XLA Modules:
  0.0 169.8 jit_solution(6101515521615732592)
XLA Ops:
  0.6 3.3 %shard_map.176 = (bf16[4,256,512]{2,1,0:T(8,128)(2,1)}, bf16[224,128]{1,0:T(8,128)(2,1)}, bf16[64,128]{1,0:T(8,128)(2,1)}) custom-call(bf16[256,2048]{1,0:T(8,128)(2,1)} %bitcast.27, f32[1,2048]{1,0:T(1,128)} %bitcast.29, bf16[32,128]{1,0:T(8,128)(2,1)} %refs_0_.2, bf16[32,128]{1,0:T(8,128)(2,1)} %refs_1_.1, bf16[32,128]{1,0:T(8,128)(2,1)} %refs_2_.1, ...), custom_call_target="tpu_custom_call" | custom-call | tf_op jit(solution)/shard_map/pallas_call | solution.py:389
  4.0 0.0 copy-start.12
  4.0 5.2 %all-to-all-start = ((bf16[4,256,512]{2,1,0:T(8,128)(2,1)}), bf16[4,256,512]{2,1,0:T(8,128)(2,1)S(1)}, u32[]{:S(2)}, u32[]{:S(2)}) async-start(bf16[4,256,512]{2,1,0:T(8,128)(2,1)} %get-tuple-element.26), calls=%async_computation | async-start | bytes 2097152 | tf_op jit(solution)/shard_map/all_to_all | solution.py:417
  9.1 0.0 copy-done.12
  9.1 34.0 %all-gather = bf16[3584,128]{1,0:T(8,128)(2,1)S(1)} all-gather(bf16[224,128]{1,0:T(8,128)(2,1)S(1)} %copy-done.12), channel_id=2, replica_groups=mesh['sp'=16,'fs'=4,'tp'=8] {'sp'}, dimensions={0}, use_global_device_ids=true | all-gather | bytes 974848 | tf_op jit(solution)/shard_map/all_gather | solution.py:418
  43.1 0.0 copy-start.8
  43.1 0.0 copy-start.9
  43.1 0.0 copy-start.10
  43.1 0.0 copy-start.11
  43.1 0.0 all-to-all-done.rows_ref
  43.2 1.1 shard_map.178
  44.3 0.0 copy-start.7
  44.3 4.8 %all-to-all-start.1 = ((bf16[4,256,128]{2,1,0:T(8,128)(2,1)}), bf16[4,256,128]{2,1,0:T(8,128)(2,1)S(1)}, u32[]{:S(2)}, u32[]{:S(2)}) async-start(bf16[4,256,128]{2,1,0:T(8,128)(2,1)} %shard_map.178), calls=%async_computation.1 | async-start | bytes 524288 | tf_op jit(solution)/shard_map/all_to_all | solution.py:444
  49.8 0.0 copy-done.8
  49.8 0.0 copy-done.9
  49.8 0.0 copy-done.10
  49.8 0.0 copy-done.11
  49.8 2.2 %shard_map.177 = (bf16[4,256,768]{2,1,0:T(8,128)(2,1)}, f32[1,256]{1,0:T(1,128)S(1)}, f32[1,128]{1,0:T(1,128)S(1)}, f32[1,128]{1,0:T(1,128)S(1)}, f32[1,128]{1,0:T(1,128)S(1)}, /*index=5*/f32[1,128]{1,0:T(1,128)S(1)}) custom-call(bf16[4,256,512]{2,1,0:T(8,128)(2,1)S(1)} %all-to-all-done.rows_ref, bf16[16,224,128]{2,1,0:T(8,128)(2,1)S(1)} %bitcast.18, ...), custom_call_target="tpu_custom_call" | custom-call | tf_op jit(solution)/shard_map/pallas_call | solution.py:423
  52.0 2.7 %all-to-all-done.1.products_ref = bf16[4,256,128]{2,1,0:T(8,128)(2,1)S(1)} async-done(((bf16[4,256,128]{2,1,0:T(8,128)(2,1)}), bf16[4,256,128]{2,1,0:T(8,128)(2,1)S(1)}, u32[]{:S(2)}, u32[]{:S(2)}) %all-to-all-start.1) | async-done | bytes 262176 | tf_op jit(solution)/shard_map/all_to_all | solution.py:444
  54.7 0.0 copy-done.7
  54.7 0.0 copy-start
  54.7 3.7 %all-to-all-start.2 = ((bf16[4,256,768]{2,1,0:T(8,128)(2,1)}), bf16[4,256,768]{2,1,0:T(8,128)(2,1)S(1)}, u32[]{:S(2)}, u32[]{:S(2)}) async-start(bf16[4,256,768]{2,1,0:T(8,128)(2,1)} %get-tuple-element.31), calls=%async_computation.2 | async-start | bytes 3145728 | tf_op jit(solution)/shard_map/all_to_all | solution.py:449
  58.4 18.5 %all-gather.1 = bf16[1280,128]{1,0:T(8,128)(2,1)S(1)} all-gather(bf16[320,128]{1,0:T(8,128)(2,1)S(1)} %shard_map.179.query_ref), channel_id=3, replica_groups={{0,128,256,384},{32,160,288,416},{64,192,320,448},{96,224,352,480},{1,1..., dimensions={0}, use_global_device_ids=true | all-gather | bytes 409600 | tf_op jit(solution)/shard_map/all_gather | solution.py:451
  77.0 0.0 all-to-all-done.2.refs_0_
  77.0 0.0 copy-done
  77.0 1.7 %shard_map.180 = (bf16[912,128]{1,0:T(8,128)(2,1)S(1)}, f32[256,128]{1,0:T(8,128)S(1)}, f32[256,128]{1,0:T(8,128)S(1)}, f32[256,128]{1,0:T(8,128)S(1)}) custom-call(bf16[4,256,768]{2,1,0:T(8,128)(2,1)S(1)} %all-to-all-done.2.refs_0_, f32[1,128]{1,0:T(1,128)S(1)} %get-tuple-element.32.refs_1_, f32[1,128]{1,0:T(1,128)S(1)} %get-tuple-element.33.refs_2_, ...), custom_call_target="tpu_custom_call" | custom-call | tf_op jit(solution)/shard_map/pallas_call | solution.py:455
  78.7 0.0 copy-start.1
  78.7 0.0 copy-start.3
  78.8 0.0 copy-start.5
  78.8 14.4 %all-gather.2 = bf16[3648,128]{1,0:T(8,128)(2,1)S(1)} all-gather(bf16[912,128]{1,0:T(8,128)(2,1)S(1)} %get-tuple-element.34), channel_id=4, replica_groups={{0,32,64,96},{128,160,192,224},{256,288,320,352},{384,416,448,480},{1,3..., dimensions={0}, use_global_device_ids=true | all-gather | bytes 1167360 | tf_op jit(solution)/shard_map/all_gather | solution.py:470
  93.2 0.2 broadcast_in_dim.14
  93.5 0.0 copy-done.1
  93.5 0.0 copy-done.3
  93.5 0.0 copy-done.5
  93.5 12.7 %all_to_all.25.own_ref = bf16[4,4,4,2,32,128]{5,4,3,2,1,0:T(8,128)(2,1)S(1)} all-to-all(bf16[4,4,4,2,32,128]{5,4,3,2,1,0:T(8,128)(2,1)S(1)} %broadcast_in_dim.14), channel_id=1, replica_groups=mesh['sp'=16,'fs'=4,'tp'=8] {'fs'}, dimensions={0} | all-to-all | bytes 2097152 | tf_op jit(solution)/shard_map/all_to_all | solution.py:471
  106.2 17.5 %collective-permute-start.4 = (bf16[4,4,4,2,32,128]{5,4,3,2,1,0:T(8,128)(2,1)S(1)}, bf16[4,4,4,2,32,128]{5,4,3,2,1,0:T(8,128)(2,1)S(1)}, u32[]{:S(2)}, u32[]{:S(2)}) collective-permute-start(bf16[4,4,4,2,32,128]{5,4,3,2,1,0:T(8,128)(2,1)S(1)} %all_to_all.25.own_ref), channel_id=1, source_target_pairs={{0,1},{1,0},{2,3},{3,2},{4,5},{5,4},{6,7},{7,6},{8,9},{9,8},{10,11... | collective-permute-start | bytes 3145736 | tf_op jit(solution)/shard_map/ppermute | solution.py:492
  123.8 0.0 copy-start.2
  123.8 0.0 copy-start.4
  123.8 0.0 copy-start.6
  123.8 3.7 %shard_map.182 = (bf16[400,128]{1,0:T(8,128)(2,1)S(1)}, bf16[400,128]{1,0:T(8,128)(2,1)S(1)}, bf16[400,128]{1,0:T(8,128)(2,1)S(1)}) custom-call(s32[1]{0:T(128)} %bitcast.position_ref, f32[1,256]{1,0:T(1,128)S(1)} %get-tuple-element.28.shift_ref, bf16[4,912,128]{2,1,0:T(8,128)(2,1)S(1)} %bitcast.15, bf16[4,320,128]{2,1,0:T(8,128)(2,1)S(1)} %bitcast.20), custom_call_target="tpu_custom_call" | custom-call | tf_op jit(solution)/shard_map/pallas_call | solution.py:478
  127.6 3.1 %collective-permute-start = (bf16[400,128]{1,0:T(8,128)(2,1)S(1)}, bf16[400,128]{1,0:T(8,128)(2,1)S(1)}, u32[]{:S(2)}, u32[]{:S(2)}) collective-permute-start(bf16[400,128]{1,0:T(8,128)(2,1)S(1)} %get-tuple-element.44), channel_id=1, source_target_pairs={{0,128},{32,160},{64,192},{96,224},{128,256},{160,288},{192,320},{... | collective-permute-start | bytes 307208 | tf_op jit(solution)/shard_map/ppermute | solution.py:487
  130.7 4.6 %collective-permute-start.1 = (bf16[400,128]{1,0:T(8,128)(2,1)S(1)}, bf16[400,128]{1,0:T(8,128)(2,1)S(1)}, u32[]{:S(2)}, u32[]{:S(2)}) collective-permute-start(bf16[400,128]{1,0:T(8,128)(2,1)S(1)} %get-tuple-element.45), channel_id=1, source_target_pairs={{0,256},{32,288},{64,320},{96,352},{128,384},{160,416},{192,448},{... | collective-permute-start | bytes 307208 | tf_op jit(solution)/shard_map/ppermute | solution.py:487
  135.3 1.3 collective-permute-start.2
  136.6 1.3 shard_map.181
  137.9 0.0 collective-permute-done.refs_0_
  137.9 0.0 collective-permute-done.1.refs_1_
  137.9 13.3 %collective-permute-done.2.refs_2_ = bf16[400,128]{1,0:T(8,128)(2,1)S(1)} collective-permute-done((bf16[400,128]{1,0:T(8,128)(2,1)S(1)}, bf16[400,128]{1,0:T(8,128)(2,1)S(1)}, u32[]{:S(2)}, u32[]{:S(2)}) %collective-permute-start.2) | collective-permute-done | bytes 102432 | tf_op jit(solution)/shard_map/ppermute | solution.py:487
  151.2 0.0 copy-done.2
  151.2 0.0 copy-done.4
  151.2 0.0 copy-done.6
  151.2 0.9 shard_map.183
  152.2 2.4 %collective-permute-start.3 = (bf16[4,32,256]{2,1,0:T(8,128)(2,1)S(1)}, bf16[4,32,256]{2,1,0:T(8,128)(2,1)S(1)}, u32[]{:S(2)}, u32[]{:S(2)}) collective-permute-start(bf16[4,32,256]{2,1,0:T(8,128)(2,1)S(1)} %get-tuple-element.48), channel_id=1, source_target_pairs={{0,1},{1,0},{2,3},{3,2},{4,5},{5,4},{6,7},{7,6},{8,9},{9,8},{10,11... | collective-permute-start | bytes 196616 | tf_op jit(solution)/shard_map/ppermute | solution.py:512
  154.5 0.9 collective-permute-done.3.other_ref
  155.4 0.0 collective-permute-done.4.pair_ref
  155.4 0.7 shard_map.184
  156.1 13.0 %all_to_all.26 = bf16[4,32,2048]{2,1,0:T(8,128)(2,1)S(1)} all-to-all(bf16[4,32,2048]{2,1,0:T(8,128)(2,1)S(1)} %shard_map.184), channel_id=1, replica_groups={{0,2,4,6},{1,3,5,7},{8,10,12,14},{9,11,13,15},{16,18,20,22},{17,19,21,2..., dimensions={0} | all-to-all | bytes 1048576 | tf_op jit(solution)/shard_map/all_to_all | solution.py:517
  169.1 0.7 reduce_sum.12
  (2 shorter events, 0.1 us)
Async XLA Ops:
  4.0 5.2 %copy-start.12 = (bf16[224,128]{1,0:T(8,128)(2,1)S(1)}, bf16[224,128]{1,0:T(8,128)(2,1)}, u32[]{:S(2)}) copy-start(bf16[224,128]{1,0:T(8,128)(2,1)} %get-tuple-element.27) | copy-start | bytes 172036
  4.0 39.2 %all-to-all-start = ((bf16[4,256,512]{2,1,0:T(8,128)(2,1)}), bf16[4,256,512]{2,1,0:T(8,128)(2,1)S(1)}, u32[]{:S(2)}, u32[]{:S(2)}) async-start(bf16[4,256,512]{2,1,0:T(8,128)(2,1)} %get-tuple-element.26), calls=%async_computation | async-start | bytes 2097152 | tf_op jit(solution)/shard_map/all_to_all | solution.py:417
  43.1 6.7 %copy-start.8 = (f32[128]{0:T(128)S(1)}, f32[128]{0:T(128)}, u32[]{:S(2)}) copy-start(f32[128]{0:T(128)} %param.31) | copy-start | bytes 1540
  43.1 6.7 %copy-start.9 = (f32[128]{0:T(128)S(1)}, f32[128]{0:T(128)}, u32[]{:S(2)}) copy-start(f32[128]{0:T(128)} %param.32) | copy-start | bytes 1540
  43.1 6.7 %copy-start.10 = (f32[128]{0:T(128)S(1)}, f32[128]{0:T(128)}, u32[]{:S(2)}) copy-start(f32[128]{0:T(128)} %param.29) | copy-start | bytes 1540
  43.1 6.7 %copy-start.11 = (f32[128]{0:T(128)S(1)}, f32[128]{0:T(128)}, u32[]{:S(2)}) copy-start(f32[128]{0:T(128)} %param.30) | copy-start | bytes 1540
  44.3 10.4 %copy-start.7 = (bf16[64,128]{1,0:T(8,128)(2,1)S(1)}, bf16[64,128]{1,0:T(8,128)(2,1)}, u32[]{:S(2)}) copy-start(bf16[64,128]{1,0:T(8,128)(2,1)} %get-tuple-element.29.own_ref) | copy-start | bytes 49156
  44.3 10.4 %all-to-all-start.1 = ((bf16[4,256,128]{2,1,0:T(8,128)(2,1)}), bf16[4,256,128]{2,1,0:T(8,128)(2,1)S(1)}, u32[]{:S(2)}, u32[]{:S(2)}) async-start(bf16[4,256,128]{2,1,0:T(8,128)(2,1)} %shard_map.178), calls=%async_computation.1 | async-start | bytes 524288 | tf_op jit(solution)/shard_map/all_to_all | solution.py:444
  54.7 22.3 %copy-start = (f32[1,256,128]{2,1,0:T(8,128)S(1)}, f32[1,256,128]{2,1,0:T(8,128)}, u32[]{:S(2)}) copy-start(f32[1,256,128]{2,1,0:T(8,128)} %param.33) | copy-start | bytes 393220
  54.7 22.3 %all-to-all-start.2 = ((bf16[4,256,768]{2,1,0:T(8,128)(2,1)}), bf16[4,256,768]{2,1,0:T(8,128)(2,1)S(1)}, u32[]{:S(2)}, u32[]{:S(2)}) async-start(bf16[4,256,768]{2,1,0:T(8,128)(2,1)} %get-tuple-element.31), calls=%async_computation.2 | async-start | bytes 3145728 | tf_op jit(solution)/shard_map/all_to_all | solution.py:449
  78.7 14.7 %copy-start.1 = (f32[256,128]{1,0:T(8,128)}, f32[256,128]{1,0:T(8,128)S(1)}, u32[]{:S(2)}) copy-start(f32[256,128]{1,0:T(8,128)S(1)} %get-tuple-element.39.inner_ref) | copy-start | bytes 393220
  78.7 14.7 %copy-start.3 = (f32[256,128]{1,0:T(8,128)}, f32[256,128]{1,0:T(8,128)S(1)}, u32[]{:S(2)}) copy-start(f32[256,128]{1,0:T(8,128)S(1)} %get-tuple-element.40.query_decayed_ref) | copy-start | bytes 393220
  78.8 14.7 %copy-start.5 = (f32[256,128]{1,0:T(8,128)}, f32[256,128]{1,0:T(8,128)S(1)}, u32[]{:S(2)}) copy-start(f32[256,128]{1,0:T(8,128)S(1)} %get-tuple-element.41.gate_ref) | copy-start | bytes 393220
  106.2 49.2 %collective-permute-start.4 = (bf16[4,4,4,2,32,128]{5,4,3,2,1,0:T(8,128)(2,1)S(1)}, bf16[4,4,4,2,32,128]{5,4,3,2,1,0:T(8,128)(2,1)S(1)}, u32[]{:S(2)}, u32[]{:S(2)}) collective-permute-start(bf16[4,4,4,2,32,128]{5,4,3,2,1,0:T(8,128)(2,1)S(1)} %all_to_all.25.own_ref), channel_id=1, source_target_pairs={{0,1},{1,0},{2,3},{3,2},{4,5},{5,4},{6,7},{7,6},{8,9},{9,8},{10,11... | collective-permute-start | bytes 3145736 | tf_op jit(solution)/shard_map/ppermute | solution.py:492
  123.8 27.4 %copy-start.2 = (f32[256,128]{1,0:T(8,128)S(1)}, f32[256,128]{1,0:T(8,128)}, u32[]{:S(2)}) copy-start(f32[256,128]{1,0:T(8,128)} %copy-done.1) | copy-start | bytes 393220
  123.8 27.4 %copy-start.4 = (f32[256,128]{1,0:T(8,128)S(1)}, f32[256,128]{1,0:T(8,128)}, u32[]{:S(2)}) copy-start(f32[256,128]{1,0:T(8,128)} %copy-done.3) | copy-start | bytes 393220
  123.8 27.4 %copy-start.6 = (f32[256,128]{1,0:T(8,128)S(1)}, f32[256,128]{1,0:T(8,128)}, u32[]{:S(2)}) copy-start(f32[256,128]{1,0:T(8,128)} %copy-done.5) | copy-start | bytes 393220
  127.6 10.4 %collective-permute-start = (bf16[400,128]{1,0:T(8,128)(2,1)S(1)}, bf16[400,128]{1,0:T(8,128)(2,1)S(1)}, u32[]{:S(2)}, u32[]{:S(2)}) collective-permute-start(bf16[400,128]{1,0:T(8,128)(2,1)S(1)} %get-tuple-element.44), channel_id=1, source_target_pairs={{0,128},{32,160},{64,192},{96,224},{128,256},{160,288},{192,320},{... | collective-permute-start | bytes 307208 | tf_op jit(solution)/shard_map/ppermute | solution.py:487
  130.7 7.2 %collective-permute-start.1 = (bf16[400,128]{1,0:T(8,128)(2,1)S(1)}, bf16[400,128]{1,0:T(8,128)(2,1)S(1)}, u32[]{:S(2)}, u32[]{:S(2)}) collective-permute-start(bf16[400,128]{1,0:T(8,128)(2,1)S(1)} %get-tuple-element.45), channel_id=1, source_target_pairs={{0,256},{32,288},{64,320},{96,352},{128,384},{160,416},{192,448},{... | collective-permute-start | bytes 307208 | tf_op jit(solution)/shard_map/ppermute | solution.py:487
  135.3 16.0 %collective-permute-start.2 = (bf16[400,128]{1,0:T(8,128)(2,1)S(1)}, bf16[400,128]{1,0:T(8,128)(2,1)S(1)}, u32[]{:S(2)}, u32[]{:S(2)}) collective-permute-start(bf16[400,128]{1,0:T(8,128)(2,1)S(1)} %get-tuple-element.46), channel_id=1, source_target_pairs={{0,384},{32,416},{64,448},{96,480},{1,385},{33,417},{65,449},{97,4... | collective-permute-start | bytes 307208 | tf_op jit(solution)/shard_map/ppermute | solution.py:487
  152.2 3.2 %collective-permute-start.3 = (bf16[4,32,256]{2,1,0:T(8,128)(2,1)S(1)}, bf16[4,32,256]{2,1,0:T(8,128)(2,1)S(1)}, u32[]{:S(2)}, u32[]{:S(2)}) collective-permute-start(bf16[4,32,256]{2,1,0:T(8,128)(2,1)S(1)} %get-tuple-element.48), channel_id=1, source_target_pairs={{0,1},{1,0},{2,3},{3,2},{4,5},{5,4},{6,7},{7,6},{8,9},{9,8},{10,11... | collective-permute-start | bytes 196616 | tf_op jit(solution)/shard_map/ppermute | solution.py:512

commit v9 on v8

--- a/solution.py
+++ b/solution.py
@@ -73,7 +73,8 @@
         copies.append(pltpu.make_async_copy(weights[7 + k], place, arrived.at[9 + k]))
     for copy in copies:
         copy.start()
-    for copy in copies:
+    packed_ref[7 * ROWS :] = jnp.zeros((1, HEAD), BF16)
+    for copy in copies[:2]:
         copy.wait()
     values = x_ref[...].astype(F32)
     square_mean = jnp.mean(values * values, axis=-1, keepdims=True)
@@ -89,6 +90,8 @@
         moved = dot(normed[:, b * wide : (b + 1) * wide], pick).astype(BF16)
         for k in range(count):
             slices_ref[k, :, b * HEAD : (b + 1) * HEAD] = moved[:, k * HEAD : (k + 1) * HEAD]
+    for copy in copies[2:]:
+        copy.wait()
 
 
 def partial_kernel(first, rows_ref, weight_ref, *refs):
@@ -390,7 +393,7 @@
         start_kernel,
         (
             shape((fs, tokens, width // fs), BF16),
-            shape((7 * ROWS, HEAD), BF16),
+            shape((7 * ROWS + 1, HEAD), BF16),
             shape((2 * ROWS, HEAD), BF16),
         ),
         11,

time: 170 us -> 170 us (level)
  transfers between devices with their start and end apart: 8 -> 8, of which waited for: 3 -> 3; matrix products, arithmetic and copies ran while one was open for 0% -> 0% of each run, Pallas kernels for 5% -> 4%
where the time goes in v9:
time: 170 us
  blocking collectives  92.1 us (54%)
  starting transfers between devices  42.9 us (25%)
  waiting for transfers between devices  17 us (10%)
  Pallas kernels  14 us (8%)
    all_gather x1, blocking collectives, on_device(): column = lax.all_gather(packed, 'sp')  34.2 us
    all_gather x1, blocking collectives, on_device(): across = lax.all_gather(own, 'sp', axis_index_groups=strided)  18.6 us
    ppermute x1, starting transfers between devices, on_device(): out_other = lax.ppermute(out_weights, 'tp', pairs)  17.1 us
    all_gather x1, blocking collectives, on_device(): gathered = lax.all_gather(message, 'sp', axis_index_groups=groups)  14.4 us
    ppermute x3, waiting for transfers between devices, on_device(): outside.append(lax.ppermute(far[j - 1], 'sp', moves))  13.4 us
    all_to_all x1, blocking collectives, on_device(): lax.all_to_all(copies(gathered[:, start:].reshape(NEAR, count, 2, ROWS, H...  12.9 us
    all_to_all x1, blocking collectives, on_device(): lax.all_to_all(projected, 'tp', 0, 0, tiled=True, axis_index_groups=chips)  12.1 us
    ppermute x3, starting transfers between devices, on_device(): outside.append(lax.ppermute(far[j - 1], 'sp', moves))  9.83 us
  transfers between devices with their start and end apart: 8, of which 3 were waited for; matrix products, arithmetic and copies ran while one was open for 0% of the time, Pallas kernels for 4%

profile of v9, /device:TPU:1, one launch (start us, length us, event | category | flops | bytes accessed | tf_op | source)
XLA Modules:
  0.0 169.8 jit_solution(18042615810288916409)
XLA Ops:
  0.6 3.4 %shard_map.176 = (bf16[4,256,512]{2,1,0:T(8,128)(2,1)}, bf16[225,128]{1,0:T(8,128)(2,1)}, bf16[64,128]{1,0:T(8,128)(2,1)}) custom-call(bf16[256,2048]{1,0:T(8,128)(2,1)} %bitcast.25, f32[1,2048]{1,0:T(1,128)} %bitcast.28, bf16[32,128]{1,0:T(8,128)(2,1)} %refs_0_.2, bf16[32,128]{1,0:T(8,128)(2,1)} %refs_1_.1, bf16[32,128]{1,0:T(8,128)(2,1)} %refs_2_.1, ...), custom_call_target="tpu_custom_call" | custom-call | tf_op jit(solution)/shard_map/pallas_call | solution.py:392
  4.0 0.0 copy-start.13
  4.0 5.1 %all-to-all-start = ((bf16[4,256,512]{2,1,0:T(8,128)(2,1)}), bf16[4,256,512]{2,1,0:T(8,128)(2,1)S(1)}, u32[]{:S(2)}, u32[]{:S(2)}) async-start(bf16[4,256,512]{2,1,0:T(8,128)(2,1)} %get-tuple-element.26), calls=%async_computation | async-start | bytes 2097152 | tf_op jit(solution)/shard_map/all_to_all | solution.py:420
  9.2 0.0 copy-done.13
  9.2 34.2 %all-gather.3.weight_ref = bf16[16,225,128]{2,1,0:T(8,128)(2,1)S(1)} all-gather(bf16[1,225,128]{2,1,0:T(8,128)(2,1)S(1)} %bitcast.27), channel_id=2, replica_groups=mesh['sp'=16,'fs'=4,'tp'=8] {'sp'}, dimensions={0}, use_global_device_ids=true | all-gather | bytes 979200 | tf_op jit(solution)/shard_map/all_gather | solution.py:421
  43.4 0.0 copy-start.9
  43.4 0.0 copy-start.10
  43.4 0.0 copy-start.11
  43.4 0.0 copy-start.12
  43.4 0.0 all-to-all-done.rows_ref
  43.4 1.2 shard_map.178
  44.5 0.0 copy-start.8
  44.5 4.8 %all-to-all-start.1 = ((bf16[4,256,128]{2,1,0:T(8,128)(2,1)}), bf16[4,256,128]{2,1,0:T(8,128)(2,1)S(1)}, u32[]{:S(2)}, u32[]{:S(2)}) async-start(bf16[4,256,128]{2,1,0:T(8,128)(2,1)} %shard_map.178), calls=%async_computation.1 | async-start | bytes 524288 | tf_op jit(solution)/shard_map/all_to_all | solution.py:447
  50.0 0.0 copy-done.9
  50.0 0.0 copy-done.10
  50.1 0.0 copy-done.11
  50.1 0.0 copy-done.12
  50.1 1.0 shard_map.177
  51.1 0.0 copy-start
  51.1 1.2 copy-done
  52.2 2.7 %all-to-all-done.1.products_ref = bf16[4,256,128]{2,1,0:T(8,128)(2,1)S(1)} async-done(((bf16[4,256,128]{2,1,0:T(8,128)(2,1)}), bf16[4,256,128]{2,1,0:T(8,128)(2,1)S(1)}, u32[]{:S(2)}, u32[]{:S(2)}) %all-to-all-start.1) | async-done | bytes 262176 | tf_op jit(solution)/shard_map/all_to_all | solution.py:447
  54.9 0.0 copy-done.8
  55.0 0.0 copy-start.1
  55.0 3.7 %all-to-all-start.2 = ((bf16[4,256,768]{2,1,0:T(8,128)(2,1)}), bf16[4,256,768]{2,1,0:T(8,128)(2,1)S(1)}, u32[]{:S(2)}, u32[]{:S(2)}) async-start(bf16[4,256,768]{2,1,0:T(8,128)(2,1)} %copy-done), calls=%async_computation.2 | async-start | bytes 3145728 | tf_op jit(solution)/shard_map/all_to_all | solution.py:452
  58.7 18.6 %all-gather.1 = bf16[1280,128]{1,0:T(8,128)(2,1)S(1)} all-gather(bf16[320,128]{1,0:T(8,128)(2,1)S(1)} %shard_map.179.query_ref), channel_id=3, replica_groups={{0,128,256,384},{32,160,288,416},{64,192,320,448},{96,224,352,480},{1,1..., dimensions={0}, use_global_device_ids=true | all-gather | bytes 409600 | tf_op jit(solution)/shard_map/all_gather | solution.py:454
  77.3 0.0 all-to-all-done.2.refs_0_
  77.3 0.0 copy-done.1
  77.3 1.7 %shard_map.180 = (bf16[912,128]{1,0:T(8,128)(2,1)S(1)}, f32[256,128]{1,0:T(8,128)S(1)}, f32[256,128]{1,0:T(8,128)S(1)}, f32[256,128]{1,0:T(8,128)S(1)}) custom-call(bf16[4,256,768]{2,1,0:T(8,128)(2,1)S(1)} %all-to-all-done.2.refs_0_, f32[1,128]{1,0:T(1,128)S(1)} %get-tuple-element.32.refs_1_, f32[1,128]{1,0:T(1,128)S(1)} %get-tuple-element.33.refs_2_, ...), custom_call_target="tpu_custom_call" | custom-call | tf_op jit(solution)/shard_map/pallas_call | solution.py:458
  79.0 0.0 copy-start.2
  79.0 0.0 copy-start.4
  79.0 0.0 copy-start.6
  79.0 14.4 %all-gather.2 = bf16[3648,128]{1,0:T(8,128)(2,1)S(1)} all-gather(bf16[912,128]{1,0:T(8,128)(2,1)S(1)} %get-tuple-element.34), channel_id=4, replica_groups={{0,32,64,96},{128,160,192,224},{256,288,320,352},{384,416,448,480},{1,3..., dimensions={0}, use_global_device_ids=true | all-gather | bytes 1167360 | tf_op jit(solution)/shard_map/all_gather | solution.py:473
  93.5 0.2 broadcast_in_dim.14
  93.7 12.9 %all_to_all.25.own_ref = bf16[4,4,4,2,32,128]{5,4,3,2,1,0:T(8,128)(2,1)S(1)} all-to-all(bf16[4,4,4,2,32,128]{5,4,3,2,1,0:T(8,128)(2,1)S(1)} %broadcast_in_dim.14), channel_id=1, replica_groups=mesh['sp'=16,'fs'=4,'tp'=8] {'fs'}, dimensions={0} | all-to-all | bytes 2097152 | tf_op jit(solution)/shard_map/all_to_all | solution.py:474
  106.6 0.0 copy-done.2
  106.6 0.0 copy-done.4
  106.6 0.0 copy-done.6
  106.6 17.1 %collective-permute-start.4 = (bf16[4,4,4,2,32,128]{5,4,3,2,1,0:T(8,128)(2,1)S(1)}, bf16[4,4,4,2,32,128]{5,4,3,2,1,0:T(8,128)(2,1)S(1)}, u32[]{:S(2)}, u32[]{:S(2)}) collective-permute-start(bf16[4,4,4,2,32,128]{5,4,3,2,1,0:T(8,128)(2,1)S(1)} %all_to_all.25.own_ref), channel_id=1, source_target_pairs={{0,1},{1,0},{2,3},{3,2},{4,5},{5,4},{6,7},{7,6},{8,9},{9,8},{10,11... | collective-permute-start | bytes 3145736 | tf_op jit(solution)/shard_map/ppermute | solution.py:495
  123.7 0.0 copy-start.3
  123.7 0.0 copy-start.5
  123.7 0.0 copy-start.7
  123.7 3.7 %shard_map.182 = (bf16[400,128]{1,0:T(8,128)(2,1)S(1)}, bf16[400,128]{1,0:T(8,128)(2,1)S(1)}, bf16[400,128]{1,0:T(8,128)(2,1)S(1)}) custom-call(s32[1]{0:T(128)} %bitcast.position_ref, f32[1,256]{1,0:T(1,128)S(1)} %get-tuple-element.28.shift_ref, bf16[4,912,128]{2,1,0:T(8,128)(2,1)S(1)} %bitcast.15, bf16[4,320,128]{2,1,0:T(8,128)(2,1)S(1)} %bitcast.18), custom_call_target="tpu_custom_call" | custom-call | tf_op jit(solution)/shard_map/pallas_call | solution.py:481
  127.5 3.8 %collective-permute-start = (bf16[400,128]{1,0:T(8,128)(2,1)S(1)}, bf16[400,128]{1,0:T(8,128)(2,1)S(1)}, u32[]{:S(2)}, u32[]{:S(2)}) collective-permute-start(bf16[400,128]{1,0:T(8,128)(2,1)S(1)} %get-tuple-element.44), channel_id=1, source_target_pairs={{0,128},{32,160},{64,192},{96,224},{128,256},{160,288},{192,320},{... | collective-permute-start | bytes 307208 | tf_op jit(solution)/shard_map/ppermute | solution.py:490
  131.3 4.7 %collective-permute-start.1 = (bf16[400,128]{1,0:T(8,128)(2,1)S(1)}, bf16[400,128]{1,0:T(8,128)(2,1)S(1)}, u32[]{:S(2)}, u32[]{:S(2)}) collective-permute-start(bf16[400,128]{1,0:T(8,128)(2,1)S(1)} %get-tuple-element.45), channel_id=1, source_target_pairs={{0,256},{32,288},{64,320},{96,352},{128,384},{160,416},{192,448},{... | collective-permute-start | bytes 307208 | tf_op jit(solution)/shard_map/ppermute | solution.py:490
  136.0 1.3 collective-permute-start.2
  137.3 1.3 shard_map.181
  138.7 0.0 collective-permute-done.refs_0_
  138.7 0.0 collective-permute-done.1.refs_1_
  138.7 13.4 %collective-permute-done.2.refs_2_ = bf16[400,128]{1,0:T(8,128)(2,1)S(1)} collective-permute-done((bf16[400,128]{1,0:T(8,128)(2,1)S(1)}, bf16[400,128]{1,0:T(8,128)(2,1)S(1)}, u32[]{:S(2)}, u32[]{:S(2)}) %collective-permute-start.2) | collective-permute-done | bytes 102432 | tf_op jit(solution)/shard_map/ppermute | solution.py:490
  152.1 0.0 copy-done.3
  152.1 0.0 copy-done.5
  152.1 0.0 copy-done.7
  152.1 0.9 shard_map.183
  153.0 2.4 %collective-permute-start.3 = (bf16[4,32,256]{2,1,0:T(8,128)(2,1)S(1)}, bf16[4,32,256]{2,1,0:T(8,128)(2,1)S(1)}, u32[]{:S(2)}, u32[]{:S(2)}) collective-permute-start(bf16[4,32,256]{2,1,0:T(8,128)(2,1)S(1)} %get-tuple-element.48), channel_id=1, source_target_pairs={{0,1},{1,0},{2,3},{3,2},{4,5},{5,4},{6,7},{7,6},{8,9},{9,8},{10,11... | collective-permute-start | bytes 196616 | tf_op jit(solution)/shard_map/ppermute | solution.py:515
  155.4 0.9 collective-permute-done.3.other_ref
  156.3 0.0 collective-permute-done.4.pair_ref
  156.3 0.7 shard_map.184
  157.0 12.1 %all_to_all.26 = bf16[4,32,2048]{2,1,0:T(8,128)(2,1)S(1)} all-to-all(bf16[4,32,2048]{2,1,0:T(8,128)(2,1)S(1)} %shard_map.184), channel_id=1, replica_groups={{0,2,4,6},{1,3,5,7},{8,10,12,14},{9,11,13,15},{16,18,20,22},{17,19,21,2..., dimensions={0} | all-to-all | bytes 1048576 | tf_op jit(solution)/shard_map/all_to_all | solution.py:520
  169.1 0.7 reduce_sum.12
  (2 shorter events, 0.1 us)
Async XLA Ops:
  4.0 5.2 %copy-start.13 = (bf16[225,128]{1,0:T(8,128)(2,1)S(1)}, bf16[225,128]{1,0:T(8,128)(2,1)}, u32[]{:S(2)}) copy-start(bf16[225,128]{1,0:T(8,128)(2,1)} %get-tuple-element.27) | copy-start | bytes 172804
  4.0 39.4 %all-to-all-start = ((bf16[4,256,512]{2,1,0:T(8,128)(2,1)}), bf16[4,256,512]{2,1,0:T(8,128)(2,1)S(1)}, u32[]{:S(2)}, u32[]{:S(2)}) async-start(bf16[4,256,512]{2,1,0:T(8,128)(2,1)} %get-tuple-element.26), calls=%async_computation | async-start | bytes 2097152 | tf_op jit(solution)/shard_map/all_to_all | solution.py:420
  43.4 6.7 %copy-start.9 = (f32[128]{0:T(128)S(1)}, f32[128]{0:T(128)}, u32[]{:S(2)}) copy-start(f32[128]{0:T(128)} %param.31) | copy-start | bytes 1540
  43.4 6.7 %copy-start.10 = (f32[128]{0:T(128)S(1)}, f32[128]{0:T(128)}, u32[]{:S(2)}) copy-start(f32[128]{0:T(128)} %param.32) | copy-start | bytes 1540
  43.4 6.7 %copy-start.11 = (f32[128]{0:T(128)S(1)}, f32[128]{0:T(128)}, u32[]{:S(2)}) copy-start(f32[128]{0:T(128)} %param.29) | copy-start | bytes 1540
  43.4 6.7 %copy-start.12 = (f32[128]{0:T(128)S(1)}, f32[128]{0:T(128)}, u32[]{:S(2)}) copy-start(f32[128]{0:T(128)} %param.30) | copy-start | bytes 1540
  44.5 10.4 %copy-start.8 = (bf16[64,128]{1,0:T(8,128)(2,1)S(1)}, bf16[64,128]{1,0:T(8,128)(2,1)}, u32[]{:S(2)}) copy-start(bf16[64,128]{1,0:T(8,128)(2,1)} %get-tuple-element.29.own_ref) | copy-start | bytes 49156
  44.5 10.4 %all-to-all-start.1 = ((bf16[4,256,128]{2,1,0:T(8,128)(2,1)}), bf16[4,256,128]{2,1,0:T(8,128)(2,1)S(1)}, u32[]{:S(2)}, u32[]{:S(2)}) async-start(bf16[4,256,128]{2,1,0:T(8,128)(2,1)} %shard_map.178), calls=%async_computation.1 | async-start | bytes 524288 | tf_op jit(solution)/shard_map/all_to_all | solution.py:447
  51.1 1.2 copy-start
  55.0 22.3 %copy-start.1 = (f32[1,256,128]{2,1,0:T(8,128)S(1)}, f32[1,256,128]{2,1,0:T(8,128)}, u32[]{:S(2)}) copy-start(f32[1,256,128]{2,1,0:T(8,128)} %param.33) | copy-start | bytes 393220
  55.0 22.3 %all-to-all-start.2 = ((bf16[4,256,768]{2,1,0:T(8,128)(2,1)}), bf16[4,256,768]{2,1,0:T(8,128)(2,1)S(1)}, u32[]{:S(2)}, u32[]{:S(2)}) async-start(bf16[4,256,768]{2,1,0:T(8,128)(2,1)} %copy-done), calls=%async_computation.2 | async-start | bytes 3145728 | tf_op jit(solution)/shard_map/all_to_all | solution.py:452
  79.0 27.6 %copy-start.2 = (f32[256,128]{1,0:T(8,128)}, f32[256,128]{1,0:T(8,128)S(1)}, u32[]{:S(2)}) copy-start(f32[256,128]{1,0:T(8,128)S(1)} %get-tuple-element.39.inner_ref) | copy-start | bytes 393220
  79.0 27.6 %copy-start.4 = (f32[256,128]{1,0:T(8,128)}, f32[256,128]{1,0:T(8,128)S(1)}, u32[]{:S(2)}) copy-start(f32[256,128]{1,0:T(8,128)S(1)} %get-tuple-element.40.query_decayed_ref) | copy-start | bytes 393220
  79.0 27.6 %copy-start.6 = (f32[256,128]{1,0:T(8,128)}, f32[256,128]{1,0:T(8,128)S(1)}, u32[]{:S(2)}) copy-start(f32[256,128]{1,0:T(8,128)S(1)} %get-tuple-element.41.gate_ref) | copy-start | bytes 393220
  106.6 49.7 %collective-permute-start.4 = (bf16[4,4,4,2,32,128]{5,4,3,2,1,0:T(8,128)(2,1)S(1)}, bf16[4,4,4,2,32,128]{5,4,3,2,1,0:T(8,128)(2,1)S(1)}, u32[]{:S(2)}, u32[]{:S(2)}) collective-permute-start(bf16[4,4,4,2,32,128]{5,4,3,2,1,0:T(8,128)(2,1)S(1)} %all_to_all.25.own_ref), channel_id=1, source_target_pairs={{0,1},{1,0},{2,3},{3,2},{4,5},{5,4},{6,7},{7,6},{8,9},{9,8},{10,11... | collective-permute-start | bytes 3145736 | tf_op jit(solution)/shard_map/ppermute | solution.py:495
  123.7 28.4 %copy-start.3 = (f32[256,128]{1,0:T(8,128)S(1)}, f32[256,128]{1,0:T(8,128)}, u32[]{:S(2)}) copy-start(f32[256,128]{1,0:T(8,128)} %copy-done.2) | copy-start | bytes 393220
  123.7 28.4 %copy-start.5 = (f32[256,128]{1,0:T(8,128)S(1)}, f32[256,128]{1,0:T(8,128)}, u32[]{:S(2)}) copy-start(f32[256,128]{1,0:T(8,128)} %copy-done.4) | copy-start | bytes 393220
  123.7 28.4 %copy-start.7 = (f32[256,128]{1,0:T(8,128)S(1)}, f32[256,128]{1,0:T(8,128)}, u32[]{:S(2)}) copy-start(f32[256,128]{1,0:T(8,128)} %copy-done.6) | copy-start | bytes 393220
  127.5 11.2 %collective-permute-start = (bf16[400,128]{1,0:T(8,128)(2,1)S(1)}, bf16[400,128]{1,0:T(8,128)(2,1)S(1)}, u32[]{:S(2)}, u32[]{:S(2)}) collective-permute-start(bf16[400,128]{1,0:T(8,128)(2,1)S(1)} %get-tuple-element.44), channel_id=1, source_target_pairs={{0,128},{32,160},{64,192},{96,224},{128,256},{160,288},{192,320},{... | collective-permute-start | bytes 307208 | tf_op jit(solution)/shard_map/ppermute | solution.py:490
  131.3 7.4 %collective-permute-start.1 = (bf16[400,128]{1,0:T(8,128)(2,1)S(1)}, bf16[400,128]{1,0:T(8,128)(2,1)S(1)}, u32[]{:S(2)}, u32[]{:S(2)}) collective-permute-start(bf16[400,128]{1,0:T(8,128)(2,1)S(1)} %get-tuple-element.45), channel_id=1, source_target_pairs={{0,256},{32,288},{64,320},{96,352},{128,384},{160,416},{192,448},{... | collective-permute-start | bytes 307208 | tf_op jit(solution)/shard_map/ppermute | solution.py:490
  136.0 16.1 %collective-permute-start.2 = (bf16[400,128]{1,0:T(8,128)(2,1)S(1)}, bf16[400,128]{1,0:T(8,128)(2,1)S(1)}, u32[]{:S(2)}, u32[]{:S(2)}) collective-permute-start(bf16[400,128]{1,0:T(8,128)(2,1)S(1)} %get-tuple-element.46), channel_id=1, source_target_pairs={{0,384},{32,416},{64,448},{96,480},{1,385},{33,417},{65,449},{97,4... | collective-permute-start | bytes 307208 | tf_op jit(solution)/shard_map/ppermute | solution.py:490
  153.0 3.2 %collective-permute-start.3 = (bf16[4,32,256]{2,1,0:T(8,128)(2,1)S(1)}, bf16[4,32,256]{2,1,0:T(8,128)(2,1)S(1)}, u32[]{:S(2)}, u32[]{:S(2)}) collective-permute-start(bf16[4,32,256]{2,1,0:T(8,128)(2,1)S(1)} %get-tuple-element.48), channel_id=1, source_target_pairs={{0,1},{1,0},{2,3},{3,2},{4,5},{5,4},{6,7},{7,6},{8,9},{9,8},{10,11... | collective-permute-start | bytes 196616 | tf_op jit(solution)/shard_map/ppermute | solution.py:515
